TPU v7x, 32 devices: a whole 2x2x4 slice. The times are simulated.
32 devices in a mesh: gr: 2 (over x), sp: 4 (over z), tp: 4 (over y, core).
Axes of the slice: x: 2, y: 2, z: 4, core: 2. Of those that a mesh axis runs over, the one named last changes fastest.
Arguments:
- tokens: bfloat16 [8, 8192, 2048], P('gr', ('sp', 'tp')), parts along dimension 0, may hold values from -6 to 6
- norm_gain: float32 [2048], replicated, may hold values from 0.1 to 1.9
- w_key: bfloat16 [2048, 256], replicated, may hold values from -0.125 to 0.125
- w_value: bfloat16 [2048, 256], replicated, may hold values from -0.125 to 0.125
- new_query: bfloat16 [8, 32, 64], P('gr'), parts along dimension 0, may hold values from -360 to 360
- cum_gate: float32 [8, 4, 8192], P(('gr', 'sp'), 'tp'), parts along dimension 0, may hold values from -1025 to 0, as said below
Outputs:
- kv_cache: bfloat16 [8, 4, 8192, 128], P(('gr', 'sp'), 'tp'), parts along dimension 0
- first_read: float32 [8, 32, 64], P('gr'), parts along dimension 0
There are 2 independent parts, one for each index of `gr`. A program takes and returns all parts, laid end to end along the dimension named above; an argument that names none is the same for every part. Nothing has to cross between parts.
Inputs may be any that keep to these rules, and one draw needn't show every extreme that they name: `cum_gate`: for each sequence and key head, the running sum along the positions of the sequence of negative log forget gates; it never rises from one position to the next.
All inputs are finite; a program needn't handle non-finite values.
Results may differ from a plain program's by a relative error of at most 0.0014.
The roundings to bfloat16 on the way count: a program that leaves them out, or rounds other values in their place, can miss the bound.
Values may be sent and summed in bfloat16 or wider, within the bound.
No kernel may reach another device: no remote copies, remote signals or barrier semaphores. Data moves between devices by JAX's collectives and lax.ppermute only.
A program may use at most 64 MiB of HBM per device.

v0:
```python
import jax
import jax.numpy as jnp
from jax import lax
from jax.sharding import PartitionSpec as P

HD = 64


NORM_FLOOR = 0.05
SCORE_FLOOR = -1e30


def joined(value, axis, join):
    pieces = jax.tree.map(lambda part: lax.all_gather(part, axis), value)
    head = jax.tree.map(lambda part: part[0], pieces)
    tail = jax.tree.map(lambda part: part[1:], pieces)
    subtotal, _ = lax.scan(lambda subtotal, slab: (join(subtotal, slab), None), head, tail)
    return subtotal


def combine(left_side, right_side):
    out_left, top_left, sum_left = left_side
    out_right, top_right, sum_right = right_side
    merged_top = jnp.maximum(top_left, top_right)
    factor_left = jnp.exp(top_left - merged_top)
    factor_right = jnp.exp(top_right - merged_top)
    merged_out = out_left * factor_left[..., None] + out_right * factor_right[..., None]
    merged_sum = sum_left * factor_left + sum_right * factor_right
    return (merged_out, merged_top, merged_sum)


def shards(tokens, norm_gain, w_key, w_value, new_query, cum_gate):
    seq_count, positions, model_width = tokens.shape
    sp_count = lax.axis_size("sp")
    tp_count = lax.axis_size("tp")
    kv_heads = w_key.shape[1] // HD
    classes = sp_count // seq_count
    halves = tp_count // kv_heads
    piece_len = positions // (classes * halves)
    widened = tokens.astype(jnp.float32)
    inverse_rms = lax.rsqrt(jnp.mean(widened * widened, axis=-1, keepdims=True) + NORM_FLOOR)
    normed = (widened * inverse_rms * norm_gain).astype(jnp.bfloat16)
    shaped = normed.reshape(seq_count, classes, halves, piece_len, model_width)
    key_heads = w_key.reshape(model_width, kv_heads, HD)
    value_heads = w_value.reshape(model_width, kv_heads, HD)
    keys_made = jnp.einsum(
        "gcbkd,dhe->gchbke", shaped, key_heads, preferred_element_type=jnp.float32
    ).astype(jnp.bfloat16)
    values_made = jnp.einsum(
        "gcbkd,dhe->gchbke", shaped, value_heads, preferred_element_type=jnp.float32
    ).astype(jnp.bfloat16)
    stacked = jnp.concatenate([keys_made, values_made], axis=-1)
    arrived = lax.all_to_all(
        stacked.reshape(sp_count * tp_count, 1, piece_len, 2 * HD),
        ("sp", "tp"),
        split_axis=0,
        concat_axis=1,
        tiled=True,
    )
    kv_cache = arrived.reshape(1, 1, sp_count * tp_count * piece_len, 2 * HD)
    query_heads = new_query.shape[1]
    group_size = query_heads // kv_heads
    seq_index = lax.axis_index("sp") // classes
    head_index = lax.axis_index("tp") // halves
    queries = lax.dynamic_slice(
        new_query, (seq_index, head_index * group_size, 0), (1, group_size, HD)
    )[0]
    keys_here = kv_cache[0, 0, :, :HD]
    values_here = kv_cache[0, 0, :, HD:]
    scores = lax.dot_general(
        queries, keys_here, (((1,), (1,)), ((), ())), preferred_element_type=jnp.float32
    )
    scores = scores * HD ** (-0.5) - cum_gate[0, 0][None, :]
    row_top = jnp.max(scores, axis=1)
    weights = jnp.exp(scores - row_top[:, None])
    row_total = jnp.sum(weights, axis=1)
    summed = jnp.dot(weights, values_here.astype(jnp.float32), precision=lax.Precision.HIGHEST)
    out_full = lax.dynamic_update_slice(
        jnp.zeros((seq_count, query_heads, HD), jnp.float32),
        summed[None],
        (seq_index, head_index * group_size, 0),
    )
    top_full = lax.dynamic_update_slice(
        jnp.full((seq_count, query_heads), SCORE_FLOOR, jnp.float32),
        row_top[None],
        (seq_index, head_index * group_size),
    )
    sum_full = lax.dynamic_update_slice(
        jnp.zeros((seq_count, query_heads), jnp.float32),
        row_total[None],
        (seq_index, head_index * group_size),
    )
    merged_out, merged_top, merged_sum = joined(
        (out_full, top_full, sum_full), ("sp", "tp"), combine
    )
    first_read = merged_out / merged_sum[..., None]
    return (kv_cache, first_read)


def solution(mesh):
    in_specs = (
        P("gr", ("sp", "tp"), None),
        P(),
        P(),
        P(),
        P("gr", None, None),
        P(("gr", "sp"), "tp", None),
    )
    out_specs = (P(("gr", "sp"), "tp", None, None), P("gr", None, None))
    return jax.shard_map(shards, mesh=mesh, in_specs=in_specs, out_specs=out_specs, check_vma=False)
```

profile of v0, /device:TPU:0, one launch (start us, length us, event | category | flops | bytes accessed | tf_op | source)
XLA Modules:
  0.0 146.3 jit_solution(3882460997390789915)
XLA Ops:
  0.6 0.0 copy-start
  0.6 0.0 copy-start.2
  0.7 0.0 copy-start.4
  0.7 1.6 %copy.18 = bf16[2048,256]{0,1:T(8,128)(2,1)S(1)} copy(bf16[2048,256]{1,0:T(8,128)(2,1)} %param.11) | data formatting | bytes 2097152 | tf_op args[3]
  2.2 5.1 %fusion.3 = f32[4,512]{1,0:T(4,128)S(1)} fusion(bf16[4,512,2048]{2,1,0:T(8,128)(2,1)} %param.8), kind=kLoop, calls=%fused_computation.10 | loop fusion | flops 12580864 | bytes 8396800 | tf_op jit(solution)/shard_map/reduce_sum | solution.py:41
  7.3 0.0 copy-done.2
  7.4 0.6 copy.17
  8.0 0.0 copy-done.4
  8.0 5.8 %fusion.19 = bf16[4,1,4,1,512,64]{4,5,2,0,3,1:T(8,128)(2,1)S(1)} fusion(bf16[2048,4,64,1]{0,2,1,3:T(8,128)(2,1)S(1)} %bitcast.90, bf16[4,512,2048]{2,1,0:T(8,128)(2,1)} %param.8, f32[2048]{0:T(1024)S(1)} %copy-done.4, f32[4,512]{1,0:T(4,128)S(1)} %add_rsqrt_fusion), kind=kOutput, calls=%fused_computation.24 | convolution fusion | flops 2164785152 | bytes 10502144 | tf_op jit(solution)/shard_map/gcbkd,dhe->gchbke/dot_general | solution.py:49
  13.9 5.8 %fusion.22 = bf16[4,1,4,1,512,64]{4,5,2,0,3,1:T(8,128)(2,1)S(1)} fusion(bf16[2048,4,64,1]{0,2,1,3:T(8,128)(2,1)S(1)} %bitcast.91, bf16[4,512,2048]{2,1,0:T(8,128)(2,1)} %param.8, f32[2048]{0:T(1024)S(1)} %copy-done.4, f32[4,512]{1,0:T(4,128)S(1)} %add_rsqrt_fusion), kind=kOutput, calls=%fused_computation.25 | convolution fusion | flops 2164785152 | bytes 10502144 | tf_op jit(solution)/shard_map/gcbkd,dhe->gchbke/dot_general | solution.py:46
  19.7 0.0 copy-start.3
  19.7 1.5 %pad_maximum_fusion = bf16[4,1,4,1,512,128]{4,5,2,0,3,1:T(8,128)(2,1)} fusion(bf16[4,1,4,1,512,64]{4,5,2,0,3,1:T(8,128)(2,1)S(1)} %fusion.19, bf16[4,1,4,1,512,64]{4,5,2,0,3,1:T(8,128)(2,1)S(1)} %fusion.22), kind=kLoop, calls=%fused_computation.21 | loop fusion | flops 4194304 | bytes 4194304 | tf_op jit(solution)/shard_map/concatenate | solution.py:52
  21.3 7.5 %all-to-all-start = ((bf16[16,1,512,128]{2,3,1,0:T(8,128)(2,1)}), bf16[16,1,512,128]{2,3,1,0:T(8,128)(2,1)}, u32[]{:S(2)}, u32[]{:S(2)}) async-start(bf16[16,1,512,128]{2,3,1,0:T(8,128)(2,1)} %bitcast.17), calls=%async_computation | async-start | bytes 4194304 | tf_op jit(solution)/shard_map/all_to_all | solution.py:53
  28.7 41.0 %all-to-all-done = bf16[16,1,512,128]{2,3,1,0:T(8,128)(2,1)} async-done(((bf16[16,1,512,128]{2,3,1,0:T(8,128)(2,1)}), bf16[16,1,512,128]{2,3,1,0:T(8,128)(2,1)}, u32[]{:S(2)}, u32[]{:S(2)}) %all-to-all-start) | async-done | bytes 2097184 | tf_op jit(solution)/shard_map/all_to_all | solution.py:53
  69.8 3.0 %copy.20 = bf16[16,1,512,128]{3,2,0,1:T(8,128)(2,1)S(1)} copy(bf16[16,1,512,128]{2,3,1,0:T(8,128)(2,1)} %all-to-all-done) | data formatting | bytes 4194304 | tf_op jit(solution)/shard_map/all_to_all | solution.py:53
  72.8 0.0 copy-start.1
  72.8 0.0 copy-done
  72.8 0.0 copy-done.3
  72.8 0.8 fusion.33
  73.6 0.2 dynamic_update_slice.13
  73.8 27.1 %all_gather.21 = f32[16,4,32]{2,1,0:T(4,128)S(1)} all-gather(f32[1,4,32]{2,1,0:T(4,128)S(1)} %dynamic_update_slice.13), channel_id=1, replica_groups=mesh['gr'=2,'sp'=4,'tp'=4] {'sp','tp'}, dimensions={0}, use_global_device_ids=true | all-gather | bytes 8704 | tf_op jit(solution)/shard_map/all_gather | solution.py:14
  100.9 0.3 fusion.27
  101.2 1.3 fusion.26
  102.5 20.5 %all_gather.19 = f32[16,4,32,64]{3,2,1,0:T(8,128)S(1)} all-gather(f32[1,4,32,64]{3,2,1,0:T(8,128)S(1)} %fusion.26), channel_id=1, replica_groups=mesh['gr'=2,'sp'=4,'tp'=4] {'sp','tp'}, dimensions={0}, use_global_device_ids=true | all-gather | bytes 557056 | tf_op jit(solution)/shard_map/all_gather | solution.py:14
  123.0 0.1 slice.38
  123.1 0.2 dynamic_update_slice.14
  123.3 19.9 %all_gather.23 = f32[16,4,32]{2,1,0:T(4,128)S(1)} all-gather(f32[1,4,32]{2,1,0:T(4,128)S(1)} %dynamic_update_slice.14), channel_id=1, replica_groups=mesh['gr'=2,'sp'=4,'tp'=4] {'sp','tp'}, dimensions={0}, use_global_device_ids=true | all-gather | bytes 8704 | tf_op jit(solution)/shard_map/all_gather | solution.py:14
  143.2 2.4 %while.14 = (s32[]{:T(128)}, f32[4,32,64]{2,1,0:T(8,128)S(1)}, f32[4,32]{1,0:T(4,128)S(1)}, f32[4,32]{1,0:T(4,128)S(1)}, f32[15,4,32]{2,1,0:T(4,128)S(1)}, /*ind...) while((s32[]{:T(128)}, f32[4,32,64]{2,1,0:T(8,128)S(1)}, f32[4,32]{1,0:T(4,128)S(1)}, ...), condition=%wide.region_4.5_spmd, body=%wide.region_3.4_spmd.sunk | while | flops 25346 | bytes 103525 | solution.py:17
  143.2 0.1 fusion.39
  143.4 0.1 fusion.39
  143.5 0.1 fusion.39
  143.7 0.1 fusion.39
  143.8 0.1 fusion.39
  144.0 0.1 fusion.39
  144.2 0.1 fusion.39
  144.3 0.1 fusion.39
  144.5 0.1 fusion.39
  144.6 0.1 fusion.39
  144.8 0.1 fusion.39
  145.0 0.1 fusion.39
  145.1 0.1 fusion.39
  145.3 0.1 fusion.39
  145.4 0.1 fusion.39
  145.6 0.7 broadcast_divide_fusion
  146.3 0.0 copy-done.1
  (24 shorter events, 0.4 us)
Async XLA Ops:
  0.6 72.2 %copy-start = (bf16[4,32,64]{2,1,0:T(8,128)(2,1)S(1)}, bf16[4,32,64]{2,1,0:T(8,128)(2,1)}, u32[]{:S(2)}) copy-start(bf16[4,32,64]{2,1,0:T(8,128)(2,1)} %param.12) | copy-start | bytes 49156
  0.6 6.7 %copy-start.2 = (bf16[2048,256]{1,0:T(8,128)(2,1)S(1)}, bf16[2048,256]{1,0:T(8,128)(2,1)}, u32[]{:S(2)}) copy-start(bf16[2048,256]{1,0:T(8,128)(2,1)} %param.10) | copy-start | bytes 3145732
  0.7 7.4 %copy-start.4 = (f32[2048]{0:T(1024)S(1)}, f32[2048]{0:T(1024)}, u32[]{:S(2)}) copy-start(f32[2048]{0:T(1024)} %param.9) | copy-start | bytes 24580
  19.7 53.1 %copy-start.3 = (f32[1,1,8192]{2,1,0:T(1,128)S(1)}, f32[1,1,8192]{2,1,0:T(1,128)}, u32[]{:S(2)}) copy-start(f32[1,1,8192]{2,1,0:T(1,128)} %param.13) | copy-start | bytes 98308
  21.3 48.5 %all-to-all-start = ((bf16[16,1,512,128]{2,3,1,0:T(8,128)(2,1)}), bf16[16,1,512,128]{2,3,1,0:T(8,128)(2,1)}, u32[]{:S(2)}, u32[]{:S(2)}) async-start(bf16[16,1,512,128]{2,3,1,0:T(8,128)(2,1)} %bitcast.17), calls=%async_computation | async-start | bytes 4194304 | tf_op jit(solution)/shard_map/all_to_all | solution.py:53
  72.8 73.5 %copy-start.1 = (bf16[16,1,512,128]{3,2,0,1:T(8,128)(2,1)}, bf16[16,1,512,128]{3,2,0,1:T(8,128)(2,1)S(1)}, u32[]{:S(2)}) copy-start(bf16[16,1,512,128]{3,2,0,1:T(8,128)(2,1)S(1)} %copy.20) | copy-start | bytes 6291460
where the time goes:
time: 147 us; the launch traced here: 146 us
  blocking collectives  67.5 us (46%)
  waiting for transfers between devices  41 us (28%)
  matrix products  13.8 us (9%)
  other arithmetic  9.65 us (7%)
  starting transfers between devices  7.46 us (5%)
  local copies, waits for them, and re-layouts  5.71 us (4%)
    all_gather x3, blocking collectives, joined(): pieces = jax.tree.map(lambda part: lax.all_gather(part, axis), value)  67.5 us
    all_to_all x1, waiting for transfers between devices, shards(): lax.all_to_all(stacked.reshape(sp_count * tp_count, 1, piece_len, 2 * HD)...  41 us
    all_to_all x1, starting transfers between devices, shards(): lax.all_to_all(stacked.reshape(sp_count * tp_count, 1, piece_len, 2 * HD)...  7.46 us
    dot_general x1, matrix products, shards(): jnp.einsum('gcbkd,dhe->gchbke', shaped, value_heads, preferred_element_ty...  5.85 us
    dot_general x1, matrix products, shards(): jnp.einsum('gcbkd,dhe->gchbke', shaped, key_heads, preferred_element_type...  5.84 us
    reduce_sum x1, other arithmetic, shards(): jnp.mean(widened * widened, axis=-1, keepdims=True) + NORM_FLOOR  5.09 us
    all_to_all x1, local copies, waits for them, and re-layouts, shards(): lax.all_to_all(stacked.reshape(sp_count * tp_count, 1, piece_len, 2 * HD)...  3.03 us
  transfers between devices with their start and end apart: 1, of which 1 were waited for; matrix products, arithmetic and copies ran while one was open for 0% of the time, Pallas kernels for 0%

commit v1 on v0

v1 whole, which is shorter than its diff:
```python
import functools

import jax
import jax.numpy as jnp
from jax import lax
from jax.experimental import pallas as pl
from jax.experimental.pallas import tpu as pltpu
from jax.sharding import PartitionSpec as P

HD = 64
NORM_FLOOR = 0.05
F32 = jnp.float32
BF16 = jnp.bfloat16


def divisor_up_to(total, limit):
    size = min(total, limit)
    while total % size:
        size -= 1
    return size


def project_kernel(heads, tokens_ref, gain_ref, key_ref, value_ref, out_ref):
    widened = tokens_ref[0].astype(F32)
    mean_square = jnp.mean(widened * widened, axis=-1, keepdims=True)
    normed = (widened * lax.rsqrt(mean_square + NORM_FLOOR) * gain_ref[...]).astype(BF16)
    keys = jnp.dot(normed, key_ref[...], preferred_element_type=F32)
    values = jnp.dot(normed, value_ref[...], preferred_element_type=F32)
    for head in range(heads):
        columns = slice(head * HD, (head + 1) * HD)
        both = jnp.concatenate([keys[:, columns], values[:, columns]], axis=-1)
        out_ref[0, head] = both.astype(BF16)


def project(tokens, norm_gain, w_key, w_value):
    seqs, positions, width = tokens.shape
    heads = w_key.shape[1] // HD
    tile = divisor_up_to(positions, 128)
    return pl.pallas_call(
        functools.partial(project_kernel, heads),
        grid=(seqs, positions // tile),
        in_specs=[
            pl.BlockSpec((1, tile, width), lambda s, i: (s, i, 0)),
            pl.BlockSpec((1, width), lambda s, i: (0, 0)),
            pl.BlockSpec(w_key.shape, lambda s, i: (0, 0)),
            pl.BlockSpec(w_value.shape, lambda s, i: (0, 0)),
        ],
        out_specs=pl.BlockSpec((1, heads, tile, 2 * HD), lambda s, i: (s, 0, i, 0)),
        out_shape=jax.ShapeDtypeStruct((seqs, heads, positions, 2 * HD), BF16),
        name="project",
    )(tokens, norm_gain.reshape(1, width), w_key, w_value)


def three_parts(value):
    high = value.astype(BF16)
    rest = value - high.astype(F32)
    middle = rest.astype(BF16)
    low = (rest - middle.astype(F32)).astype(BF16)
    return jnp.concatenate([high, middle, low], axis=0)


def read_kernel(chunks, query_ref, cache_ref, gate_ref, out_ref):
    rows = query_ref.shape[0]
    size = cache_ref.shape[0] // chunks
    tops, totals, sums = [], [], []
    for c in range(chunks):
        block = cache_ref[c * size : (c + 1) * size, :]
        scores = lax.dot_general(
            query_ref[...], block, (((1,), (1,)), ((), ())), preferred_element_type=F32
        )
        scores = scores * HD ** (-0.5) - gate_ref[:, c * size : (c + 1) * size]
        top = jnp.max(scores, axis=1, keepdims=True)
        weights = jnp.exp(scores - top)
        parts = jnp.dot(three_parts(weights), block, preferred_element_type=F32)
        tops.append(top)
        totals.append(jnp.sum(weights, axis=1, keepdims=True))
        sums.append(parts[:rows] + parts[rows : 2 * rows] + parts[2 * rows :])
    best = functools.reduce(jnp.maximum, tops)
    factors = [jnp.exp(top - best) for top in tops]
    summed = sum(s * f for s, f in zip(sums, factors))
    total = sum(t * f for t, f in zip(totals, factors))
    lane = lax.broadcasted_iota(jnp.int32, summed.shape, 1)
    out_ref[...] = jnp.where(lane >= HD, summed, jnp.where(lane == 0, best, total))


def read(queries, cache, gates):
    rows = queries.shape[0]
    padded = jnp.concatenate([queries, jnp.zeros_like(queries)], axis=-1)
    chunks = 4
    while cache.shape[0] % chunks:
        chunks -= 1
    return pl.pallas_call(
        functools.partial(read_kernel, chunks),
        out_shape=jax.ShapeDtypeStruct((rows, 2 * HD), F32),
        name="read",
    )(padded, cache, gates)


def gathered(tile, axis, size):
    stacked = tile[None]
    if size & (size - 1):
        return lax.all_gather(tile, axis)
    step = 1
    index = lax.axis_index(axis)
    while step < size:
        other = lax.ppermute(stacked, axis, [(i, i ^ step) for i in range(size)])
        low = (index & step) == 0
        first = jnp.where(low, stacked, other)
        second = jnp.where(low, other, stacked)
        stacked = jnp.concatenate([first, second], axis=0)
        step *= 2
    return stacked


def shards(tokens, norm_gain, w_key, w_value, new_query, cum_gate):
    seqs, positions, width = tokens.shape
    sp_count, tp_count = lax.axis_size("sp"), lax.axis_size("tp")
    heads = w_key.shape[1] // HD
    classes, halves = sp_count // seqs, tp_count // heads
    piece = positions // (classes * halves)
    devices = sp_count * tp_count
    made = project(tokens, norm_gain, w_key, w_value)
    if classes * halves > 1:
        made = made.reshape(seqs, heads, classes, halves, piece, 2 * HD)
        made = made.transpose(0, 2, 1, 3, 4, 5)
    arrived = lax.all_to_all(
        made.reshape(devices, piece, 2 * HD), ("sp", "tp"), split_axis=0, concat_axis=0, tiled=True
    )
    kv_cache = arrived.reshape(devices * piece, 2 * HD)
    query_heads = new_query.shape[1]
    group = query_heads // heads
    seq_index = lax.axis_index("sp") // classes
    head_index = lax.axis_index("tp") // halves
    queries = lax.dynamic_slice(new_query, (seq_index, head_index * group, 0), (1, group, HD))[0]
    partial_read = read(queries, kv_cache, cum_gate[0])
    tiles = gathered(gathered(partial_read, "tp", tp_count), "sp", sp_count)
    tiles = tiles.reshape(seqs, classes, heads, halves, group, 2 * HD)
    tops = tiles[..., :1]
    factors = jnp.exp(tops - jnp.max(tops, axis=(1, 3), keepdims=True))
    merged = jnp.sum(tiles * factors, axis=(1, 3))
    first_read = merged[..., HD:] / merged[..., 1:2]
    return kv_cache[None, None], first_read.reshape(seqs, query_heads, HD)


def solution(mesh):
    in_specs = (
        P("gr", ("sp", "tp"), None),
        P(),
        P(),
        P(),
        P("gr", None, None),
        P(("gr", "sp"), "tp", None),
    )
    out_specs = (P(("gr", "sp"), "tp", None, None), P("gr", None, None))
    return jax.shard_map(shards, mesh=mesh, in_specs=in_specs, out_specs=out_specs, check_vma=False)
```

time: 147 us -> 96.6 us (0.66)
  blocking collectives: 67.5 us -> 0 us
  Pallas kernels: 0 us -> 20.4 us
  starting transfers between devices: 7.46 us -> 21.4 us
  matrix products: 13.8 us -> 0 us
  other arithmetic: 9.65 us -> 1.67 us
  waiting for transfers between devices: 41 us -> 46.6 us
    all_gather x3 -> x0, blocking collectives: 67.5 us -> none  [joined(): pieces = jax.tree.map(lambda part: lax.all_gather(part, axis), value)]
    pallas_call x0 -> x2, Pallas kernels: none -> 20.4 us  [the longest x1 16.4 us: project(): pl.pallas_call(functools.partial(project_kernel, heads), grid=(seqs, posi...]
    ppermute x0 -> x4, starting transfers between devices: none -> 14 us  [gathered(): other = lax.ppermute(stacked, axis, [(i, i ^ step) for i in range(size)])]
    dot_general x4 -> x0, matrix products: 13.8 us -> none  [the longest x1 5.85 us: shards(): jnp.einsum('gcbkd,dhe->gchbke', shaped, value_heads, preferred_element_ty...]
    ppermute x0 -> x4, waiting for transfers between devices: none -> 6.27 us  [gathered(): other = lax.ppermute(stacked, axis, [(i, i ^ step) for i in range(size)])]
    reduce_sum x2 -> x0, other arithmetic: 5.34 us -> none  [the longest x1 5.09 us: shards(): jnp.mean(widened * widened, axis=-1, keepdims=True) + NORM_FLOOR]
    all_to_all x1 -> x0, local copies, waits for them, and re-layouts: 3.03 us -> none  [shards(): lax.all_to_all(stacked.reshape(sp_count * tp_count, 1, piece_len, 2 * HD)...]
    unnamed x12 -> x5, local copies, waits for them, and re-layouts: 2.25 us -> 4.41 us
  transfers between devices with their start and end apart: 1 -> 5, of which waited for: 1 -> 5; matrix products, arithmetic and copies ran while one was open for 0% -> 1% of each run, Pallas kernels for 0% -> 0%
where the time goes in v1:
time: 96.6 us; the launch traced here: 96 us
  waiting for transfers between devices  46.6 us (48%)
  starting transfers between devices  21.4 us (22%)
  Pallas kernels  20.4 us (21%)
  local copies, waits for them, and re-layouts  5.18 us (5%)
  other arithmetic  1.67 us (2%)
    all_to_all x1, waiting for transfers between devices, shards(): lax.all_to_all(made.reshape(devices, piece, 2 * HD), ('sp', 'tp'), split_...  40.4 us
    pallas_call x1, Pallas kernels, project(): pl.pallas_call(functools.partial(project_kernel, heads), grid=(seqs, posi...  16.4 us
    ppermute x4, starting transfers between devices, gathered(): other = lax.ppermute(stacked, axis, [(i, i ^ step) for i in range(size)])  14 us
    all_to_all x1, starting transfers between devices, shards(): lax.all_to_all(made.reshape(devices, piece, 2 * HD), ('sp', 'tp'), split_...  7.41 us
    ppermute x4, waiting for transfers between devices, gathered(): other = lax.ppermute(stacked, axis, [(i, i ^ step) for i in range(size)])  6.27 us
    unnamed x5, local copies, waits for them, and re-layouts  4.41 us
    pallas_call x1, Pallas kernels, read(): pl.pallas_call(functools.partial(read_kernel, chunks), out_shape=jax.Shap...  3.98 us
  transfers between devices with their start and end apart: 5, of which 5 were waited for; matrix products, arithmetic and copies ran while one was open for 1% of the time, Pallas kernels for 0%

profile of v1, /device:TPU:0, one launch (start us, length us, event | category | flops | bytes accessed | tf_op | source)
XLA Modules:
  0.0 96.0 jit_solution(16435974890534015757)
XLA Ops:
  0.6 0.0 copy-start
  0.6 16.4 %project.1 = bf16[4,4,512,128]{3,2,1,0:T(8,128)(2,1)} custom-call(bf16[4,512,2048]{2,1,0:T(8,128)(2,1)} %tokens_ref.1, f32[1,2048]{1,0:T(1,128)} %bitcast.25, bf16[2048,256]{1,0:T(8,128)(2,1)} %key_ref.1, bf16[2048,256]{1,0:T(8,128)(2,1)} %value_ref.1), custom_call_target="tpu_custom_call" | custom-call | tf_op jit(solution)/shard_map/project/pallas_call | solution.py:39
  17.1 7.4 %all-to-all-start = ((bf16[16,512,128]{2,1,0:T(8,128)(2,1)}), bf16[16,512,128]{2,1,0:T(8,128)(2,1)S(1)}, u32[]{:S(2)}, u32[]{:S(2)}) async-start(bf16[16,512,128]{2,1,0:T(8,128)(2,1)} %bitcast.22), calls=%async_computation | async-start | bytes 4194304 | tf_op jit(solution)/shard_map/all_to_all | solution.py:126
  24.5 0.0 copy-done
  24.5 0.6 concatenate.17.query_ref
  25.1 40.4 %all-to-all-done = bf16[16,512,128]{2,1,0:T(8,128)(2,1)S(1)} async-done(((bf16[16,512,128]{2,1,0:T(8,128)(2,1)}), bf16[16,512,128]{2,1,0:T(8,128)(2,1)S(1)}, u32[]{:S(2)}, u32[]{:S(2)}) %all-to-all-start) | async-done | bytes 2097184 | tf_op jit(solution)/shard_map/all_to_all | solution.py:126
  65.5 0.0 copy-start.1
  65.5 1.4 %copy-done.1 = bf16[16,512,128]{2,1,0:T(8,128)(2,1)} copy-done((bf16[16,512,128]{2,1,0:T(8,128)(2,1)}, bf16[16,512,128]{2,1,0:T(8,128)(2,1)S(1)}, u32[]{:S(2)}) %copy-start.1) | copy-done | bytes 2097176
  66.8 4.0 %read.1 = f32[8,128]{1,0:T(8,128)} custom-call(bf16[8,128]{1,0:T(8,128)(2,1)} %concatenate.17.query_ref, bf16[8192,128]{1,0:T(8,128)(2,1)} %bitcast.20, f32[1,8192]{1,0:T(1,128)} %bitcast.23), custom_call_target="tpu_custom_call" | custom-call | tf_op jit(solution)/shard_map/read/pallas_call | solution.py:92
  70.8 1.0 %collective-permute-start = (f32[1,8,128]{2,1,0:T(8,128)}, f32[1,8,128]{2,1,0:T(8,128)S(1)}, u32[]{:S(2)}, u32[]{:S(2)}) collective-permute-start(f32[1,8,128]{2,1,0:T(8,128)} %bitcast.24), channel_id=1, source_target_pairs={{0,1},{1,0},{2,3},{3,2},{4,5},{5,4},{6,7},{7,6},{8,9},{9,8},{10,11... | collective-permute-start | bytes 12296 | tf_op jit(solution)/shard_map/ppermute | solution.py:106
  71.8 1.0 %collective-permute-done = f32[1,8,128]{2,1,0:T(8,128)S(1)} collective-permute-done((f32[1,8,128]{2,1,0:T(8,128)}, f32[1,8,128]{2,1,0:T(8,128)S(1)}, u32[]{:S(2)}, u32[]{:S(2)}) %collective-permute-start) | collective-permute-done | bytes 4128 | tf_op jit(solution)/shard_map/ppermute | solution.py:106
  72.8 0.7 broadcast_select_fusion.7
  73.5 3.4 %collective-permute-start.1 = (f32[2,8,128]{2,1,0:T(8,128)S(1)}, f32[2,8,128]{2,1,0:T(8,128)S(1)}, u32[]{:S(2)}, u32[]{:S(2)}) collective-permute-start(f32[2,8,128]{2,1,0:T(8,128)S(1)} %pad_maximum_fusion.2), channel_id=1, source_target_pairs={{0,2},{1,3},{2,0},{3,1},{4,6},{5,7},{6,4},{7,5},{8,10},{9,11},{10,... | collective-permute-start | bytes 24584 | tf_op jit(solution)/shard_map/ppermute | solution.py:106
  76.9 1.6 %collective-permute-done.1 = f32[2,8,128]{2,1,0:T(8,128)S(1)} collective-permute-done((f32[2,8,128]{2,1,0:T(8,128)S(1)}, f32[2,8,128]{2,1,0:T(8,128)S(1)}, u32[]{:S(2)}, u32[]{:S(2)}) %collective-permute-start.1) | collective-permute-done | bytes 8224 | tf_op jit(solution)/shard_map/ppermute | solution.py:106
  78.5 5.7 %collective-permute-start.2 = (f32[1,4,8,128]{3,2,1,0:T(8,128)S(1)}, f32[1,4,8,128]{3,2,1,0:T(8,128)S(1)}, u32[]{:S(2)}, u32[]{:S(2)}) collective-permute-start(f32[1,4,8,128]{3,2,1,0:T(8,128)S(1)} %maximum_bitcast_fusion), channel_id=1, source_target_pairs={{0,4},{4,0},{8,12},{12,8},{1,5},{5,1},{9,13},{13,9},{2,6},{6,2},{1... | collective-permute-start | bytes 49160 | tf_op jit(solution)/shard_map/ppermute | solution.py:106
  84.2 1.7 %collective-permute-done.2 = f32[1,4,8,128]{3,2,1,0:T(8,128)S(1)} collective-permute-done((f32[1,4,8,128]{3,2,1,0:T(8,128)S(1)}, f32[1,4,8,128]{3,2,1,0:T(8,128)S(1)}, u32[]{:S(2)}, u32[]{:S(2)}) %collective-permute-start.2) | collective-permute-done | bytes 16416 | tf_op jit(solution)/shard_map/ppermute | solution.py:106
  85.9 4.0 %collective-permute-start.3 = (f32[2,4,8,128]{3,2,1,0:T(8,128)S(1)}, f32[2,4,8,128]{3,2,1,0:T(8,128)S(1)}, u32[]{:S(2)}, u32[]{:S(2)}) collective-permute-start(f32[2,4,8,128]{3,2,1,0:T(8,128)S(1)} %pad_maximum_fusion.1), channel_id=1, source_target_pairs={{0,8},{4,12},{8,0},{12,4},{1,9},{5,13},{9,1},{13,5},{2,10},{6,14},... | collective-permute-start | bytes 98312 | tf_op jit(solution)/shard_map/ppermute | solution.py:106
  89.9 1.9 %collective-permute-done.3 = f32[2,4,8,128]{3,2,1,0:T(8,128)S(1)} collective-permute-done((f32[2,4,8,128]{3,2,1,0:T(8,128)S(1)}, f32[2,4,8,128]{3,2,1,0:T(8,128)S(1)}, u32[]{:S(2)}, u32[]{:S(2)}) %collective-permute-start.3) | collective-permute-done | bytes 32800 | tf_op jit(solution)/shard_map/ppermute | solution.py:106
  91.8 0.1 fusion.2
  91.9 0.1 fusion.3
  92.0 0.2 slice_reduce_fusion
  92.2 0.7 fusion
  93.0 3.0 %copy.9 = bf16[1,1,8192,128]{3,2,1,0:T(8,128)(2,1)} copy(bf16[1,1,8192,128]{3,2,1,0:T(8,128)(2,1)} %bitcast.21) | data formatting | bytes 4194304
  (8 shorter events, 0.1 us)
Async XLA Ops:
  0.6 23.9 %copy-start = (bf16[4,32,64]{2,1,0:T(8,128)(2,1)S(1)}, bf16[4,32,64]{2,1,0:T(8,128)(2,1)}, u32[]{:S(2)}) copy-start(bf16[4,32,64]{2,1,0:T(8,128)(2,1)} %param.10) | copy-start | bytes 49156
  17.1 48.4 %all-to-all-start = ((bf16[16,512,128]{2,1,0:T(8,128)(2,1)}), bf16[16,512,128]{2,1,0:T(8,128)(2,1)S(1)}, u32[]{:S(2)}, u32[]{:S(2)}) async-start(bf16[16,512,128]{2,1,0:T(8,128)(2,1)} %bitcast.22), calls=%async_computation | async-start | bytes 4194304 | tf_op jit(solution)/shard_map/all_to_all | solution.py:126
  65.5 1.4 %copy-start.1 = (bf16[16,512,128]{2,1,0:T(8,128)(2,1)}, bf16[16,512,128]{2,1,0:T(8,128)(2,1)S(1)}, u32[]{:S(2)}) copy-start(bf16[16,512,128]{2,1,0:T(8,128)(2,1)S(1)} %all-to-all-done) | copy-start | bytes 6291460
  70.8 2.0 %collective-permute-start = (f32[1,8,128]{2,1,0:T(8,128)}, f32[1,8,128]{2,1,0:T(8,128)S(1)}, u32[]{:S(2)}, u32[]{:S(2)}) collective-permute-start(f32[1,8,128]{2,1,0:T(8,128)} %bitcast.24), channel_id=1, source_target_pairs={{0,1},{1,0},{2,3},{3,2},{4,5},{5,4},{6,7},{7,6},{8,9},{9,8},{10,11... | collective-permute-start | bytes 12296 | tf_op jit(solution)/shard_map/ppermute | solution.py:106
  73.5 5.0 %collective-permute-start.1 = (f32[2,8,128]{2,1,0:T(8,128)S(1)}, f32[2,8,128]{2,1,0:T(8,128)S(1)}, u32[]{:S(2)}, u32[]{:S(2)}) collective-permute-start(f32[2,8,128]{2,1,0:T(8,128)S(1)} %pad_maximum_fusion.2), channel_id=1, source_target_pairs={{0,2},{1,3},{2,0},{3,1},{4,6},{5,7},{6,4},{7,5},{8,10},{9,11},{10,... | collective-permute-start | bytes 24584 | tf_op jit(solution)/shard_map/ppermute | solution.py:106
  78.5 7.4 %collective-permute-start.2 = (f32[1,4,8,128]{3,2,1,0:T(8,128)S(1)}, f32[1,4,8,128]{3,2,1,0:T(8,128)S(1)}, u32[]{:S(2)}, u32[]{:S(2)}) collective-permute-start(f32[1,4,8,128]{3,2,1,0:T(8,128)S(1)} %maximum_bitcast_fusion), channel_id=1, source_target_pairs={{0,4},{4,0},{8,12},{12,8},{1,5},{5,1},{9,13},{13,9},{2,6},{6,2},{1... | collective-permute-start | bytes 49160 | tf_op jit(solution)/shard_map/ppermute | solution.py:106
  85.9 5.9 %collective-permute-start.3 = (f32[2,4,8,128]{3,2,1,0:T(8,128)S(1)}, f32[2,4,8,128]{3,2,1,0:T(8,128)S(1)}, u32[]{:S(2)}, u32[]{:S(2)}) collective-permute-start(f32[2,4,8,128]{3,2,1,0:T(8,128)S(1)} %pad_maximum_fusion.1), channel_id=1, source_target_pairs={{0,8},{4,12},{8,0},{12,4},{1,9},{5,13},{9,1},{13,5},{2,10},{6,14},... | collective-permute-start | bytes 98312 | tf_op jit(solution)/shard_map/ppermute | solution.py:106

commit v2 on v1

v2 whole, which is shorter than its diff:
```python
import functools

import jax
import jax.numpy as jnp
from jax import lax
from jax.experimental import pallas as pl
from jax.experimental.pallas import tpu as pltpu
from jax.sharding import PartitionSpec as P

HD = 64
LANES = 128
NORM_FLOOR = 0.05
F32 = jnp.float32
BF16 = jnp.bfloat16


def divisor_up_to(total, limit):
    size = min(total, limit)
    while total % size:
        size -= 1
    return size


def normalize(tokens, gain):
    widened = tokens.astype(F32)
    mean_square = jnp.mean(widened * widened, axis=-1, keepdims=True)
    return (widened * lax.rsqrt(mean_square + NORM_FLOOR) * gain).astype(BF16)


def keys_and_values(normed, key_ref, value_ref):
    keys = jnp.dot(normed, key_ref[...], preferred_element_type=F32)
    values = jnp.dot(normed, value_ref[...], preferred_element_type=F32)
    for head in range(key_ref.shape[1] // HD):
        columns = slice(head * HD, (head + 1) * HD)
        yield head, jnp.concatenate([keys[:, columns], values[:, columns]], axis=-1).astype(BF16)


def three_parts(value, axis=0):
    high = value.astype(BF16)
    rest = value - high.astype(F32)
    middle = rest.astype(BF16)
    low = (rest - middle.astype(F32)).astype(BF16)
    return jnp.concatenate([high, middle, low], axis=axis)


def project_kernel(tokens_ref, gain_ref, key_ref, value_ref, out_ref):
    normed = normalize(tokens_ref[0], gain_ref[...])
    for head, both in keys_and_values(normed, key_ref, value_ref):
        out_ref[0, head] = both


def project(tokens, norm_gain, w_key, w_value):
    seqs, positions, width = tokens.shape
    heads = w_key.shape[1] // HD
    tile = divisor_up_to(positions, 512)
    return pl.pallas_call(
        project_kernel,
        grid=(seqs, positions // tile),
        in_specs=[
            pl.BlockSpec((1, tile, width), lambda s, i: (s, i, 0)),
            pl.BlockSpec((1, width), lambda s, i: (0, 0)),
            pl.BlockSpec(w_key.shape, lambda s, i: (0, 0)),
            pl.BlockSpec(w_value.shape, lambda s, i: (0, 0)),
        ],
        out_specs=pl.BlockSpec((1, heads, tile, 2 * HD), lambda s, i: (s, 0, i, 0)),
        out_shape=jax.ShapeDtypeStruct((seqs, heads, positions, 2 * HD), BF16),
        name="project",
    )(tokens, norm_gain, w_key, w_value)


def softmax_part(query, block, gate):
    rows = query.shape[0]
    scores = lax.dot_general(query, block, (((1,), (1,)), ((), ())), preferred_element_type=F32)
    scores = scores * HD ** (-0.5) - gate
    top = jnp.max(scores, axis=1, keepdims=True)
    weights = jnp.exp(scores - top)
    parts = jnp.dot(three_parts(weights), block, preferred_element_type=F32)
    summed = parts[:rows] + parts[rows : 2 * rows] + parts[2 * rows :]
    return summed, top, jnp.sum(weights, axis=1, keepdims=True)


def packed(summed, top, total):
    lane = lax.broadcasted_iota(jnp.int32, summed.shape, summed.ndim - 1)
    return jnp.where(lane >= HD, summed, jnp.where(lane == 0, top, total))


def merged(tiles):
    best = functools.reduce(jnp.maximum, [tile[..., :1] for tile in tiles])
    factors = [jnp.exp(tile[..., :1] - best) for tile in tiles]
    both = sum(tile * factor for tile, factor in zip(tiles, factors))
    return both, best


def read_kernel(chunks, query_ref, cache_ref, gate_ref, out_ref):
    size = cache_ref.shape[0] // chunks
    tiles = []
    for c in range(chunks):
        rows = slice(c * size, (c + 1) * size)
        tiles.append(packed(*softmax_part(query_ref[...], cache_ref[rows, :], gate_ref[:, rows])))
    both, best = merged(tiles)
    out_ref[...] = packed(both, best, both[:, 1:2])


def read(queries, cache, gates):
    padded = jnp.concatenate([queries, jnp.zeros_like(queries)], axis=-1)
    chunks = 4
    while cache.shape[0] % chunks:
        chunks -= 1
    return pl.pallas_call(
        functools.partial(read_kernel, chunks),
        out_shape=jax.ShapeDtypeStruct((queries.shape[0], 2 * HD), F32),
        name="read",
    )(padded, cache, gates)


def read_after(sp_axes, tokens, norm_gain, w_key, w_value, new_query, cum_gate):
    seqs, positions, _ = tokens.shape
    sp_count, tp_count = lax.axis_size(sp_axes), lax.axis_size("tp")
    everyone = (sp_axes if isinstance(sp_axes, tuple) else (sp_axes,)) + ("tp",)
    heads = w_key.shape[1] // HD
    classes, halves = sp_count // seqs, tp_count // heads
    piece = positions // (classes * halves)
    devices = sp_count * tp_count
    made = project(tokens, norm_gain, w_key, w_value)
    made = made.reshape(seqs, heads, classes, halves, piece, 2 * HD).transpose(0, 2, 1, 3, 4, 5)
    arrived = lax.all_to_all(
        made.reshape(devices, piece, 2 * HD), everyone, split_axis=0, concat_axis=0, tiled=True
    )
    kv_cache = arrived.reshape(devices * piece, 2 * HD)
    query_heads = new_query.shape[1]
    group = query_heads // heads
    seq_index = lax.axis_index(sp_axes) // classes
    head_index = lax.axis_index("tp") // halves
    queries = lax.dynamic_slice(new_query, (seq_index, head_index * group, 0), (1, group, HD))[0]
    tile = read(queries, kv_cache, cum_gate[0])
    tiles = lax.all_gather(tile, everyone)
    tiles = tiles.reshape(seqs, classes, heads, halves, group, 2 * HD)
    tops = tiles[..., :1]
    factors = jnp.exp(tops - jnp.max(tops, axis=(1, 3), keepdims=True))
    both = jnp.sum(tiles * factors, axis=(1, 3))
    first_read = both[..., HD:] / both[..., 1:2]
    return kv_cache[None, None], first_read.reshape(seqs, query_heads, HD)


def heads_made(normed, key_ref, value_ref):
    return [both for _, both in keys_and_values(normed, key_ref, value_ref)]


def across_kernel(axes, flip, tokens_ref, gain_ref, key_hbm, value_hbm, *refs):
    out_refs, (token_ref, key_ref, value_ref, made_ref, semaphores) = refs[:-5], refs[-5:]
    upper, lower, column = (lax.axis_index(axis) for axis in axes)
    seq = (upper * lax.axis_size(axes[1]) + lower) ^ flip
    pieces, rows = token_ref.shape[:2]
    loads = [(tokens_ref.at[seq, pl.ds(i * rows, rows)], token_ref.at[i]) for i in range(pieces)]
    loads[1:1] = [(key_hbm, key_ref), (value_hbm, value_ref)]
    copies = [
        pltpu.make_async_copy(source, target, semaphores.at[i])
        for i, (source, target) in enumerate(loads)
    ]
    for copy in copies:
        copy.start()
    for i in range(pieces):
        copies[0 if i == 0 else i + 2].wait()
        normed = normalize(token_ref[i], gain_ref[...])
        if i == 0:
            copies[1].wait()
            copies[2].wait()
        for head, both in enumerate(heads_made(normed, key_ref, value_ref)):
            made_ref[head, i * rows : (i + 1) * rows] = both
    for j, out_ref in enumerate(out_refs):
        out_ref[...] = made_ref[column ^ j]


def make_across(axes, flip, tokens, norm_gain, w_key, w_value):
    _, positions, width = tokens.shape
    heads = w_key.shape[1] // HD
    pieces = 2
    anywhere, vmem = pl.BlockSpec(memory_space=pl.ANY), pl.BlockSpec(memory_space=pltpu.VMEM)
    return pl.pallas_call(
        functools.partial(across_kernel, axes, flip),
        in_specs=[anywhere, vmem, anywhere, anywhere],
        out_specs=[vmem] * heads,
        out_shape=[jax.ShapeDtypeStruct((positions, 2 * HD), BF16)] * heads,
        scratch_shapes=[
            pltpu.VMEM((pieces, positions // pieces, width), BF16),
            pltpu.VMEM(w_key.shape, BF16),
            pltpu.VMEM(w_value.shape, BF16),
            pltpu.VMEM((heads, positions, 2 * HD), BF16),
            pltpu.SemaphoreType.DMA((pieces + 2,)),
        ],
        name="across",
    )(tokens, norm_gain, w_key, w_value)


def planes(axes):
    upper, lower, column = (lax.axis_index(axis) for axis in axes)
    half = lax.axis_size(axes[1])
    return upper * half + lower, upper * half, column, half


def read_sequence(slots, blocks, query_ref, gate_ref, tile_ref):
    heads, group = len(blocks), query_ref.shape[1]
    lanes, queries, gates = 2 * HD, [], []
    for head, slot in enumerate(slots):
        query = query_ref[slot].astype(F32)
        pieces = [jnp.zeros((group, size), F32) for size in (head * lanes, (heads - head) * lanes - HD)]
        pieces.insert(1, query)
        queries.append(jnp.concatenate([piece for piece in pieces if piece.shape[1]], axis=1))
        lines = gate_ref[slot]
        gate = jnp.concatenate([lines[i : i + 1] for i in range(lines.shape[0])], axis=1)
        gates.append(jnp.broadcast_to(gate, (group, gate.shape[1])))
    query = jnp.concatenate(queries, axis=0).astype(BF16)
    block = jnp.concatenate(blocks, axis=1)
    summed, top, total = softmax_part(query, block, jnp.concatenate(gates, axis=0))
    for head, slot in enumerate(slots):
        rows = slice(head * group, (head + 1) * group)
        columns = slice(head * lanes, (head + 1) * lanes)
        tile_ref[slot] = packed(summed[rows, columns], top[rows], total[rows])


def rest_kernel(axes, heads, tokens_ref, gain_ref, key_ref, value_ref, query_ref, gate_ref, *refs):
    first_refs, refs = refs[:heads], refs[heads:]
    second_refs, (near_ref, tile_ref, _, made_ref) = refs[:heads], refs[heads:]
    step = pl.program_id(0)
    plane, near_first, column, half = planes(axes)
    made = heads_made(normalize(tokens_ref[0], gain_ref[...]), key_ref, value_ref)
    seq = jnp.where(step == 0, plane ^ (half + 1), near_first + step - 1)
    slots = [seq * heads + head for head in range(heads)]
    read_sequence(slots, made, query_ref, gate_ref, tile_ref)

    @pl.when(step == 0)
    def _():
        for head, both in enumerate(made):
            made_ref[head] = both
        for j in range(heads):
            second_refs[j][...] = made_ref[column ^ j]
        slots = [(plane ^ half) * heads + (column ^ j) for j in range(heads)]
        read_sequence(slots, [ref[...] for ref in first_refs], query_ref, gate_ref, tile_ref)

    @pl.when(step > 0)
    def _():
        for head, both in enumerate(made):
            near_ref[0, head] = both


def make_rest(axes, tokens, norm_gain, w_key, w_value, queries, gates, first):
    seqs, positions, width = tokens.shape
    heads = w_key.shape[1] // HD
    near = seqs // 2
    fixed = lambda rank: lambda i: (0,) * rank
    tile_shape = queries.shape[:2] + (2 * HD,)

    def sequence(i):
        plane, near_first, _, half = planes(axes)
        return jnp.where(i == 0, plane ^ (half + 1), near_first + i - 1), 0, 0

    made = pl.pallas_call(
        functools.partial(rest_kernel, axes, heads),
        grid=(near + 1,),
        in_specs=[
            pl.BlockSpec((1, positions, width), sequence),
            pl.BlockSpec((1, width), fixed(2)),
            pl.BlockSpec(w_key.shape, fixed(2)),
            pl.BlockSpec(w_value.shape, fixed(2)),
            pl.BlockSpec(queries.shape, fixed(3)),
            pl.BlockSpec(gates.shape, fixed(3)),
        ]
        + [pl.BlockSpec((positions, 2 * HD), fixed(2))] * heads,
        out_specs=[pl.BlockSpec((positions, 2 * HD), fixed(2))] * heads
        + [
            pl.BlockSpec((1, heads, positions, 2 * HD), lambda i: (jnp.maximum(i - 1, 0), 0, 0, 0)),
            pl.BlockSpec(tile_shape, fixed(3)),
            pl.BlockSpec(memory_space=pl.ANY),
        ],
        scratch_shapes=[pltpu.VMEM((heads, positions, 2 * HD), BF16)],
        out_shape=[jax.ShapeDtypeStruct((positions, 2 * HD), BF16)] * heads
        + [
            jax.ShapeDtypeStruct((near, heads, positions, 2 * HD), BF16),
            jax.ShapeDtypeStruct(tile_shape, F32),
            jax.ShapeDtypeStruct((seqs * heads * positions, 2 * HD), BF16),
        ],
        name="rest",
    )(tokens, norm_gain, w_key, w_value, queries, gates, *first)
    return made[:heads], *made[heads:]


def merge(tiles):
    both, best = merged(tiles)
    return packed(both, best, both[..., 1:2])


def after(value, *others):
    return lax.optimization_barrier((value,) + others)[0]


def read_beside(tokens, norm_gain, w_key, w_value, new_query, cum_gate):
    seqs, positions, _ = tokens.shape
    heads = w_key.shape[1] // HD
    query_heads = new_query.shape[1]
    group = query_heads // heads
    devices = seqs * heads
    half = seqs // 2
    everyone = ("hi", "lo", "tp")
    plane = lax.axis_index("hi") * half + lax.axis_index("lo")
    column = lax.axis_index("tp")
    near_first = lax.axis_index("hi") * half
    weights = (norm_gain, w_key, w_value)

    def swap(value, k, j):
        pairs = [(i, i ^ (k * heads + j)) for i in range(devices)]
        return lax.ppermute(value, everyone, pairs)

    first = make_across(everyone, half, tokens, *weights)
    arrived_first = [swap(first[0], half, 0)]
    gates = after(cum_gate.reshape(devices, positions // LANES, LANES), first[0])
    gates = lax.all_to_all(gates, everyone, split_axis=0, concat_axis=0, tiled=True)
    arrived_first += [swap(first[j], half, j) for j in range(1, heads)]
    queries = new_query.reshape(devices, group, HD)
    rest = make_rest(everyone, tokens, *weights, queries, gates, first)
    second, near, tile, cache = rest
    arrived_second = [swap(second[j], half + 1, j) for j in range(heads)]
    near = near.reshape(half * heads, positions, 2 * HD)
    arrived_near = lax.all_to_all(near, ("lo", "tp"), split_axis=0, concat_axis=0, tiled=True)
    rows = devices * positions

    def placed(cache, blocks, k, columns):
        for j in columns:
            start = ((plane ^ k) * heads + (column ^ j)) * positions
            cache = lax.dynamic_update_slice(cache, blocks[j], (start, 0))
        return cache

    columns = [1 << bit for bit in reversed(range(heads.bit_length() - 1))]
    for step, j in enumerate(columns):
        other = swap(tile, 0, j)
        if step == len(columns) - 1:
            cache = placed(cache, arrived_first, half, range(heads))
            other, cache = lax.optimization_barrier((other, cache))
        tile = merge([tile, other])
    others = [swap(tile, k, 0) for k in range(1, seqs)]
    near_rows = arrived_near.reshape(half * heads * positions, 2 * HD)
    cache = lax.dynamic_update_slice(cache, near_rows, (near_first * heads * positions, 0))
    cache = placed(cache, arrived_second, half + 1, range(heads - 1))
    others, cache = lax.optimization_barrier((others, cache))
    tile = merge([tile] + others)
    first_read = tile[..., HD:] / tile[..., 1:2]
    cache = placed(cache, arrived_second, half + 1, range(heads - 1, heads))
    return cache.reshape(1, 1, rows, 2 * HD), first_read.reshape(seqs, query_heads, HD)


def power_of_two(size):
    return size > 1 and size & (size - 1) == 0


def solution(mesh):
    groups, sp_count, tp_count = (mesh.shape[axis] for axis in ("gr", "sp", "tp"))
    sp_axes = "sp"
    halves_mesh = mesh
    if sp_count % 2 == 0:
        halves_mesh = jax.sharding.Mesh(
            mesh.devices.reshape(groups, 2, sp_count // 2, tp_count), ("gr", "hi", "lo", "tp")
        )
        sp_axes = ("hi", "lo")

    def shards(tokens, norm_gain, w_key, w_value, new_query, cum_gate):
        seqs, positions, width = tokens.shape
        heads = w_key.shape[1] // HD
        alone = sp_count == seqs and tp_count == heads
        even = power_of_two(seqs) and power_of_two(heads) and positions % LANES == 0
        body = read_beside if alone and even else functools.partial(read_after, sp_axes)
        return body(tokens, norm_gain.reshape(1, width), w_key, w_value, new_query, cum_gate)

    sp = sp_axes if isinstance(sp_axes, tuple) else (sp_axes,)
    in_specs = (
        P("gr", sp + ("tp",), None),
        P(),
        P(),
        P(),
        P("gr", None, None),
        P(("gr",) + sp, "tp", None),
    )
    out_specs = (P(("gr",) + sp, "tp", None, None), P("gr", None, None))
    return jax.shard_map(
        shards, mesh=halves_mesh, in_specs=in_specs, out_specs=out_specs, check_vma=False
    )
```

time: 96.6 us -> 75.2 us (0.78)
  waiting for transfers between devices: 46.6 us -> 9.5 us
  starting transfers between devices: 21.4 us -> 37.3 us
  local copies, waits for them, and re-layouts: 5.18 us -> 9.71 us
  Pallas kernels: 20.4 us -> 15.9 us
    all_to_all x1 -> x2, waiting for transfers between devices: 40.4 us -> 0.52 us  [the longest x1 0.52 us: read_beside(): lax.all_to_all(gates, everyone, split_axis=0, concat_axis=0, tiled=True)]
    ppermute x4 -> x13, starting transfers between devices: 14 us -> 26.3 us  [swap(): return lax.ppermute(value, everyone, pairs)]
    dynamic_update_slice x0 -> x9, local copies, waits for them, and re-layouts: none -> 6.36 us  [the longest x8 5.31 us: placed(): cache = lax.dynamic_update_slice(cache, blocks[j], (start, 0))]
    pallas_call x2, Pallas kernels: 20.4 us -> 15.9 us  [the longest x1 10.7 us: make_rest(): pl.pallas_call(functools.partial(rest_kernel, axes, heads), grid=(near +...]
    unnamed x5 -> x12, local copies, waits for them, and re-layouts: 4.41 us -> 0.63 us
    all_to_all x1 -> x2, starting transfers between devices: 7.41 us -> 11 us  [the longest x1 7.43 us: read_beside(): lax.all_to_all(gates, everyone, split_axis=0, concat_axis=0, tiled=True)]
    ppermute x4 -> x13, waiting for transfers between devices: 6.27 us -> 8.98 us  [swap(): return lax.ppermute(value, everyone, pairs)]
    mul x0 -> x8, local copies, waits for them, and re-layouts: none -> 1.3 us  [merged(): both = sum((tile * factor for tile, factor in zip(tiles, factors)))]
  transfers between devices with their start and end apart: 5 -> 15, of which waited for: 5 -> 4; matrix products, arithmetic and copies ran while one was open for 1% -> 14% of each run, Pallas kernels for 0% -> 14%
where the time goes in v2:
time: 75.2 us; the launch traced here: 74.9 us
  starting transfers between devices  37.3 us (50%)
  Pallas kernels  15.9 us (21%)
  local copies, waits for them, and re-layouts  9.71 us (13%)
  waiting for transfers between devices  9.5 us (13%)
  other arithmetic  1.7 us (2%)
  between operations  0.83 us (1%)
    ppermute x13, starting transfers between devices, swap(): return lax.ppermute(value, everyone, pairs)  26.3 us
    pallas_call x1, Pallas kernels, make_rest(): pl.pallas_call(functools.partial(rest_kernel, axes, heads), grid=(near +...  10.7 us
    ppermute x13, waiting for transfers between devices, swap(): return lax.ppermute(value, everyone, pairs)  8.98 us
    all_to_all x1, starting transfers between devices, read_beside(): lax.all_to_all(gates, everyone, split_axis=0, concat_axis=0, tiled=True)  7.43 us
    dynamic_update_slice x8, local copies, waits for them, and re-layouts, placed(): cache = lax.dynamic_update_slice(cache, blocks[j], (start, 0))  5.31 us
    pallas_call x1, Pallas kernels, make_across(): pl.pallas_call(functools.partial(across_kernel, axes, flip), in_specs=[an...  5.22 us
    all_to_all x1, starting transfers between devices, read_beside(): lax.all_to_all(near, ('lo', 'tp'), split_axis=0, concat_axis=0, tiled=True)  3.56 us
  transfers between devices with their start and end apart: 15, of which 4 were waited for; matrix products, arithmetic and copies ran while one was open for 14% of the time, Pallas kernels for 14%

profile of v2, /device:TPU:0, one launch (start us, length us, event | category | flops | bytes accessed | tf_op | source)
XLA Modules:
  0.0 74.9 jit_solution(14738627733126178190)
XLA Ops:
  0.6 5.2 %across.1 = (bf16[512,128]{1,0:T(8,128)(2,1)}, bf16[512,128]{1,0:T(8,128)(2,1)}, bf16[512,128]{1,0:T(8,128)(2,1)}, bf16[512,128]{1,0:T(8,128)(2,1)}) custom-call(bf16[4,512,2048]{2,1,0:T(8,128)(2,1)} %tokens_ref.3, f32[1,2048]{1,0:T(1,128)} %bitcast.62, bf16[2048,256]{1,0:T(8,128)(2,1)} %key_ref.1, bf16[2048,256]{1,0:T(8,128)(2,1)} %value_ref.1), custom_call_target="tpu_custom_call" | custom-call | tf_op jit(solution)/shard_map/across/pallas_call | solution.py:179
  5.9 7.4 %all-to-all-start = ((f32[16,4,128]{2,1,0:T(4,128)}), f32[16,4,128]{2,1,0:T(4,128)S(1)}, u32[]{:S(2)}, u32[]{:S(2)}) async-start(f32[16,4,128]{2,1,0:T(4,128)} %bitcast.2), calls=%async_computation | async-start | bytes 65536 | tf_op jit(solution)/shard_map/all_to_all | solution.py:316
  13.3 2.8 %collective-permute-start.2 = (bf16[512,128]{1,0:T(8,128)(2,1)}, bf16[512,128]{1,0:T(8,128)(2,1)S(1)}, u32[]{:S(2)}, u32[]{:S(2)}) collective-permute-start(bf16[512,128]{1,0:T(8,128)(2,1)} %get-tuple-element.20.refs_0_), channel_id=1, source_target_pairs={{0,8},{1,9},{2,10},{3,11},{4,12},{5,13},{6,14},{7,15},{8,0},{9,1},... | collective-permute-start | bytes 393224 | tf_op jit(solution)/shard_map/ppermute | solution.py:311
  16.1 0.0 collective-permute-start.3
  16.1 3.3 %collective-permute-start.4 = (bf16[512,128]{1,0:T(8,128)(2,1)}, bf16[512,128]{1,0:T(8,128)(2,1)S(1)}, u32[]{:S(2)}, u32[]{:S(2)}) collective-permute-start(bf16[512,128]{1,0:T(8,128)(2,1)} %get-tuple-element.23.refs_2_), channel_id=1, source_target_pairs={{0,10},{1,11},{2,8},{3,9},{4,14},{5,15},{6,12},{7,13},{8,2},{9,3},... | collective-permute-start | bytes 393224 | tf_op jit(solution)/shard_map/ppermute | solution.py:311
  19.4 0.3 collective-permute-start.5
  19.7 0.5 all-to-all-done.gate_ref
  20.2 0.6 copy-done.1
  20.8 10.7 %rest.1 = (bf16[512,128]{1,0:T(8,128)(2,1)}, bf16[512,128]{1,0:T(8,128)(2,1)}, bf16[512,128]{1,0:T(8,128)(2,1)}, bf16[512,128]{1,0:T(8,128)(2,1)}, bf16[2,4,512,...) custom-call(bf16[4,512,2048]{2,1,0:T(8,128)(2,1)} %tokens_ref.3, f32[1,2048]{1,0:T(1,128)} %bitcast.63, ...), custom_call_target="tpu_custom_call" | custom-call | tf_op jit(solution)/shard_map/rest/pallas_call | solution.py:257
  31.5 0.0 copy-start
  31.5 1.3 %collective-permute-start = (f32[16,8,128]{2,1,0:T(8,128)}, f32[16,8,128]{2,1,0:T(8,128)S(1)}, u32[]{:S(2)}, u32[]{:S(2)}) collective-permute-start(f32[16,8,128]{2,1,0:T(8,128)} %get-tuple-element.25), channel_id=1, source_target_pairs={{0,2},{1,3},{2,0},{3,1},{4,6},{5,7},{6,4},{7,5},{8,10},{9,11},{10,... | collective-permute-start | bytes 196616 | tf_op jit(solution)/shard_map/ppermute | solution.py:311
  32.8 3.6 %all-to-all-start.1 = ((bf16[8,512,128]{2,1,0:T(8,128)(2,1)}), bf16[8,512,128]{2,1,0:T(8,128)(2,1)S(1)}, u32[]{:S(2)}, u32[]{:S(2)}) async-start(bf16[8,512,128]{2,1,0:T(8,128)(2,1)} %bitcast.40), calls=%async_computation.1 | async-start | bytes 2097152 | tf_op jit(solution)/shard_map/all_to_all | solution.py:323
  36.4 5.6 %collective-permute-done = f32[16,8,128]{2,1,0:T(8,128)S(1)} collective-permute-done((f32[16,8,128]{2,1,0:T(8,128)}, f32[16,8,128]{2,1,0:T(8,128)S(1)}, u32[]{:S(2)}, u32[]{:S(2)}) %collective-permute-start) | collective-permute-done | bytes 65568 | tf_op jit(solution)/shard_map/ppermute | solution.py:311
  42.0 4.0 %collective-permute-start.9 = (bf16[512,128]{1,0:T(8,128)(2,1)S(1)}, bf16[512,128]{1,0:T(8,128)(2,1)S(1)}, u32[]{:S(2)}, u32[]{:S(2)}) collective-permute-start(bf16[512,128]{1,0:T(8,128)(2,1)S(1)} %copy-done.5), channel_id=1, source_target_pairs={{0,12},{1,13},{2,14},{3,15},{4,8},{5,9},{6,10},{7,11},{8,4},{9,5},... | collective-permute-start | bytes 393224 | tf_op jit(solution)/shard_map/ppermute | solution.py:311
  46.0 0.2 copy.70
  46.2 0.2 copy.69
  46.4 0.2 copy.68
  46.5 0.1 multiply_add_fusion.2
  46.6 0.1 slice.61
  46.7 0.2 copy.71
  46.9 0.1 select_select_fusion.2
  47.0 0.1 collective-permute-start.10
  47.1 0.7 constant_dynamic-update-slice_fusion.7
  47.8 0.0 collective-permute-done.3
  47.8 4.0 %collective-permute-start.11 = (bf16[512,128]{1,0:T(8,128)(2,1)S(1)}, bf16[512,128]{1,0:T(8,128)(2,1)S(1)}, u32[]{:S(2)}, u32[]{:S(2)}) collective-permute-start(bf16[512,128]{1,0:T(8,128)(2,1)S(1)} %copy-done.3), channel_id=1, source_target_pairs={{0,14},{1,15},{2,12},{3,13},{4,10},{5,11},{6,8},{7,9},{8,6},{9,7},... | collective-permute-start | bytes 393224 | tf_op jit(solution)/shard_map/ppermute | solution.py:311
  51.8 0.7 constant_dynamic-update-slice_fusion.6
  52.5 3.5 %collective-permute-start.12 = (bf16[512,128]{1,0:T(8,128)(2,1)S(1)}, bf16[512,128]{1,0:T(8,128)(2,1)S(1)}, u32[]{:S(2)}, u32[]{:S(2)}) collective-permute-start(bf16[512,128]{1,0:T(8,128)(2,1)S(1)} %copy-done.2), channel_id=1, source_target_pairs={{0,15},{1,14},{2,13},{3,12},{4,11},{5,10},{6,9},{7,8},{8,7},{9,6},... | collective-permute-start | bytes 393224 | tf_op jit(solution)/shard_map/ppermute | solution.py:311
  56.0 0.7 constant_dynamic-update-slice_fusion.5
  56.7 0.0 collective-permute-done.5
  56.7 0.1 collective-permute-start.1
  56.8 0.7 constant_dynamic-update-slice_fusion.4
  57.4 0.5 collective-permute-done.1
  57.9 0.2 copy.74
  58.1 0.2 copy.73
  58.3 0.2 copy.72
  58.5 0.2 multiply_add_fusion.1
  58.6 0.1 slice.63
  58.7 0.2 copy.75
  58.9 0.1 select_select_fusion.1
  59.0 0.1 collective-permute-start.6
  59.1 0.0 all-to-all-done.1
  59.1 1.0 %constant_dynamic-update-slice_fusion.3 = bf16[8192,128]{1,0:T(8,128)(2,1)} fusion(bf16[8192,128]{1,0:T(8,128)(2,1)} %constant_dynamic-update-slice_fusion.4, bf16[4096,128]{1,0:T(8,128)(2,1)S(1)} %bitcast.39, s32[]{:T(128)S(6)} %select_n.55), kind=kLoop, calls=%fused_computation.22 | loop fusion | bytes 2097156 | tf_op jit(solution)/shard_map/dynamic_update_slice | solution.py:341
  60.1 5.0 %collective-permute-start.7 = (f32[16,8,128]{2,1,0:T(8,128)S(1)}, f32[16,8,128]{2,1,0:T(8,128)S(1)}, u32[]{:S(2)}, u32[]{:S(2)}) collective-permute-start(f32[16,8,128]{2,1,0:T(8,128)S(1)} %select_select_fusion.1), channel_id=1, source_target_pairs={{0,8},{1,9},{2,10},{3,11},{4,12},{5,13},{6,14},{7,15},{8,0},{9,1},... | collective-permute-start | bytes 196616 | tf_op jit(solution)/shard_map/ppermute | solution.py:311
  65.1 0.7 constant_dynamic-update-slice_fusion.2
  65.7 1.8 %collective-permute-start.8 = (f32[16,8,128]{2,1,0:T(8,128)S(1)}, f32[16,8,128]{2,1,0:T(8,128)S(1)}, u32[]{:S(2)}, u32[]{:S(2)}) collective-permute-start(f32[16,8,128]{2,1,0:T(8,128)S(1)} %select_select_fusion.1), channel_id=1, source_target_pairs={{0,12},{1,13},{2,14},{3,15},{4,8},{5,9},{6,10},{7,11},{8,4},{9,5},... | collective-permute-start | bytes 196616 | tf_op jit(solution)/shard_map/ppermute | solution.py:311
  67.6 0.7 constant_dynamic-update-slice_fusion.1
  68.2 0.0 collective-permute-done.11
  68.2 0.7 constant_dynamic-update-slice_fusion
  68.9 0.0 collective-permute-done.6
  68.9 2.9 %collective-permute-done.8 = f32[16,8,128]{2,1,0:T(8,128)S(1)} collective-permute-done((f32[16,8,128]{2,1,0:T(8,128)S(1)}, f32[16,8,128]{2,1,0:T(8,128)S(1)}, u32[]{:S(2)}, u32[]{:S(2)}) %collective-permute-start.8) | collective-permute-done | bytes 65568 | tf_op jit(solution)/shard_map/ppermute | solution.py:311
  71.9 0.2 copy.80
  72.0 0.2 copy.77
  72.2 0.2 copy.78
  72.4 0.2 copy.79
  72.5 0.2 copy.76
  72.7 0.2 multiply_add_fusion
  72.9 0.1 slice.65
  73.0 0.2 copy.81
  73.1 0.1 select_select_fusion
  73.3 0.1 slice.67
  73.3 0.2 copy.82
  73.5 0.7 slice_divide_fusion
  74.2 0.0 collective-permute-done.12
  74.3 0.7 bitcast_dynamic-update-slice_fusion
  (22 shorter events, 0.2 us)
Async XLA Ops:
  5.9 14.3 %all-to-all-start = ((f32[16,4,128]{2,1,0:T(4,128)}), f32[16,4,128]{2,1,0:T(4,128)S(1)}, u32[]{:S(2)}, u32[]{:S(2)}) async-start(f32[16,4,128]{2,1,0:T(4,128)} %bitcast.2), calls=%async_computation | async-start | bytes 65536 | tf_op jit(solution)/shard_map/all_to_all | solution.py:316
  13.3 33.7 %collective-permute-start.2 = (bf16[512,128]{1,0:T(8,128)(2,1)}, bf16[512,128]{1,0:T(8,128)(2,1)S(1)}, u32[]{:S(2)}, u32[]{:S(2)}) collective-permute-start(bf16[512,128]{1,0:T(8,128)(2,1)} %get-tuple-element.20.refs_0_), channel_id=1, source_target_pairs={{0,8},{1,9},{2,10},{3,11},{4,12},{5,13},{6,14},{7,15},{8,0},{9,1},... | collective-permute-start | bytes 393224 | tf_op jit(solution)/shard_map/ppermute | solution.py:311
  16.1 31.7 %collective-permute-start.3 = (bf16[512,128]{1,0:T(8,128)(2,1)}, bf16[512,128]{1,0:T(8,128)(2,1)S(1)}, u32[]{:S(2)}, u32[]{:S(2)}) collective-permute-start(bf16[512,128]{1,0:T(8,128)(2,1)} %get-tuple-element.22.refs_1_), channel_id=1, source_target_pairs={{0,9},{1,8},{2,11},{3,10},{4,13},{5,12},{6,15},{7,14},{8,1},{9,0},... | collective-permute-start | bytes 393224 | tf_op jit(solution)/shard_map/ppermute | solution.py:311
  16.1 36.3 %collective-permute-start.4 = (bf16[512,128]{1,0:T(8,128)(2,1)}, bf16[512,128]{1,0:T(8,128)(2,1)S(1)}, u32[]{:S(2)}, u32[]{:S(2)}) collective-permute-start(bf16[512,128]{1,0:T(8,128)(2,1)} %get-tuple-element.23.refs_2_), channel_id=1, source_target_pairs={{0,10},{1,11},{2,8},{3,9},{4,14},{5,15},{6,12},{7,13},{8,2},{9,3},... | collective-permute-start | bytes 393224 | tf_op jit(solution)/shard_map/ppermute | solution.py:311
  19.4 37.3 %collective-permute-start.5 = (bf16[512,128]{1,0:T(8,128)(2,1)}, bf16[512,128]{1,0:T(8,128)(2,1)S(1)}, u32[]{:S(2)}, u32[]{:S(2)}) collective-permute-start(bf16[512,128]{1,0:T(8,128)(2,1)} %get-tuple-element.24.refs_3_), channel_id=1, source_target_pairs={{0,11},{1,10},{2,9},{3,8},{4,15},{5,14},{6,13},{7,12},{8,3},{9,2},... | collective-permute-start | bytes 393224 | tf_op jit(solution)/shard_map/ppermute | solution.py:311
  20.2 0.6 copy-start.1
  31.5 10.5 %copy-start.5 = (bf16[512,128]{1,0:T(8,128)(2,1)S(1)}, bf16[512,128]{1,0:T(8,128)(2,1)}, u32[]{:S(2)}) copy-start(bf16[512,128]{1,0:T(8,128)(2,1)} %get-tuple-element.30) | copy-start | bytes 393220
  31.5 14.5 %copy-start = (f32[16,8,128]{2,1,0:T(8,128)S(1)}, f32[16,8,128]{2,1,0:T(8,128)}, u32[]{:S(2)}) copy-start(f32[16,8,128]{2,1,0:T(8,128)} %get-tuple-element.25) | copy-start | bytes 196612
  31.5 15.5 %copy-start.4 = (bf16[512,128]{1,0:T(8,128)(2,1)S(1)}, bf16[512,128]{1,0:T(8,128)(2,1)}, u32[]{:S(2)}) copy-start(bf16[512,128]{1,0:T(8,128)(2,1)} %get-tuple-element.31) | copy-start | bytes 393220
  31.5 16.3 %copy-start.3 = (bf16[512,128]{1,0:T(8,128)(2,1)S(1)}, bf16[512,128]{1,0:T(8,128)(2,1)}, u32[]{:S(2)}) copy-start(bf16[512,128]{1,0:T(8,128)(2,1)} %get-tuple-element.32) | copy-start | bytes 393220
  31.5 20.9 %copy-start.2 = (bf16[512,128]{1,0:T(8,128)(2,1)S(1)}, bf16[512,128]{1,0:T(8,128)(2,1)}, u32[]{:S(2)}) copy-start(bf16[512,128]{1,0:T(8,128)(2,1)} %get-tuple-element.34) | copy-start | bytes 393220
  31.5 10.4 %collective-permute-start = (f32[16,8,128]{2,1,0:T(8,128)}, f32[16,8,128]{2,1,0:T(8,128)S(1)}, u32[]{:S(2)}, u32[]{:S(2)}) collective-permute-start(f32[16,8,128]{2,1,0:T(8,128)} %get-tuple-element.25), channel_id=1, source_target_pairs={{0,2},{1,3},{2,0},{3,1},{4,6},{5,7},{6,4},{7,5},{8,10},{9,11},{10,... | collective-permute-start | bytes 196616 | tf_op jit(solution)/shard_map/ppermute | solution.py:311
  32.8 26.2 %all-to-all-start.1 = ((bf16[8,512,128]{2,1,0:T(8,128)(2,1)}), bf16[8,512,128]{2,1,0:T(8,128)(2,1)S(1)}, u32[]{:S(2)}, u32[]{:S(2)}) async-start(bf16[8,512,128]{2,1,0:T(8,128)(2,1)} %bitcast.40), calls=%async_computation.1 | async-start | bytes 2097152 | tf_op jit(solution)/shard_map/all_to_all | solution.py:323
  42.0 18.1 %collective-permute-start.9 = (bf16[512,128]{1,0:T(8,128)(2,1)S(1)}, bf16[512,128]{1,0:T(8,128)(2,1)S(1)}, u32[]{:S(2)}, u32[]{:S(2)}) collective-permute-start(bf16[512,128]{1,0:T(8,128)(2,1)S(1)} %copy-done.5), channel_id=1, source_target_pairs={{0,12},{1,13},{2,14},{3,15},{4,8},{5,9},{6,10},{7,11},{8,4},{9,5},... | collective-permute-start | bytes 393224 | tf_op jit(solution)/shard_map/ppermute | solution.py:311
  47.0 18.7 %collective-permute-start.10 = (bf16[512,128]{1,0:T(8,128)(2,1)S(1)}, bf16[512,128]{1,0:T(8,128)(2,1)S(1)}, u32[]{:S(2)}, u32[]{:S(2)}) collective-permute-start(bf16[512,128]{1,0:T(8,128)(2,1)S(1)} %copy-done.4), channel_id=1, source_target_pairs={{0,13},{1,12},{2,15},{3,14},{4,9},{5,8},{6,11},{7,10},{8,5},{9,4},... | collective-permute-start | bytes 393224 | tf_op jit(solution)/shard_map/ppermute | solution.py:311
  47.8 20.4 %collective-permute-start.11 = (bf16[512,128]{1,0:T(8,128)(2,1)S(1)}, bf16[512,128]{1,0:T(8,128)(2,1)S(1)}, u32[]{:S(2)}, u32[]{:S(2)}) collective-permute-start(bf16[512,128]{1,0:T(8,128)(2,1)S(1)} %copy-done.3), channel_id=1, source_target_pairs={{0,14},{1,15},{2,12},{3,13},{4,10},{5,11},{6,8},{7,9},{8,6},{9,7},... | collective-permute-start | bytes 393224 | tf_op jit(solution)/shard_map/ppermute | solution.py:311
  52.5 21.8 %collective-permute-start.12 = (bf16[512,128]{1,0:T(8,128)(2,1)S(1)}, bf16[512,128]{1,0:T(8,128)(2,1)S(1)}, u32[]{:S(2)}, u32[]{:S(2)}) collective-permute-start(bf16[512,128]{1,0:T(8,128)(2,1)S(1)} %copy-done.2), channel_id=1, source_target_pairs={{0,15},{1,14},{2,13},{3,12},{4,11},{5,10},{6,9},{7,8},{8,7},{9,6},... | collective-permute-start | bytes 393224 | tf_op jit(solution)/shard_map/ppermute | solution.py:311
  56.7 1.3 %collective-permute-start.1 = (f32[16,8,128]{2,1,0:T(8,128)S(1)}, f32[16,8,128]{2,1,0:T(8,128)S(1)}, u32[]{:S(2)}, u32[]{:S(2)}) collective-permute-start(f32[16,8,128]{2,1,0:T(8,128)S(1)} %select_select_fusion.2), channel_id=1, source_target_pairs={{0,1},{1,0},{2,3},{3,2},{4,5},{5,4},{6,7},{7,6},{8,9},{9,8},{10,11... | collective-permute-start | bytes 196616 | tf_op jit(solution)/shard_map/ppermute | solution.py:311
  59.0 9.9 %collective-permute-start.6 = (f32[16,8,128]{2,1,0:T(8,128)S(1)}, f32[16,8,128]{2,1,0:T(8,128)S(1)}, u32[]{:S(2)}, u32[]{:S(2)}) collective-permute-start(f32[16,8,128]{2,1,0:T(8,128)S(1)} %select_select_fusion.1), channel_id=1, source_target_pairs={{0,4},{1,5},{2,6},{3,7},{4,0},{5,1},{6,2},{7,3},{8,12},{9,13},{10,... | collective-permute-start | bytes 196616 | tf_op jit(solution)/shard_map/ppermute | solution.py:311
  60.1 8.8 %collective-permute-start.7 = (f32[16,8,128]{2,1,0:T(8,128)S(1)}, f32[16,8,128]{2,1,0:T(8,128)S(1)}, u32[]{:S(2)}, u32[]{:S(2)}) collective-permute-start(f32[16,8,128]{2,1,0:T(8,128)S(1)} %select_select_fusion.1), channel_id=1, source_target_pairs={{0,8},{1,9},{2,10},{3,11},{4,12},{5,13},{6,14},{7,15},{8,0},{9,1},... | collective-permute-start | bytes 196616 | tf_op jit(solution)/shard_map/ppermute | solution.py:311
  65.7 6.1 %collective-permute-start.8 = (f32[16,8,128]{2,1,0:T(8,128)S(1)}, f32[16,8,128]{2,1,0:T(8,128)S(1)}, u32[]{:S(2)}, u32[]{:S(2)}) collective-permute-start(f32[16,8,128]{2,1,0:T(8,128)S(1)} %select_select_fusion.1), channel_id=1, source_target_pairs={{0,12},{1,13},{2,14},{3,15},{4,8},{5,9},{6,10},{7,11},{8,4},{9,5},... | collective-permute-start | bytes 196616 | tf_op jit(solution)/shard_map/ppermute | solution.py:311

commit v3 on v2

--- a/solution.py
+++ b/solution.py
@@ -147,28 +147,40 @@
 
 
 def across_kernel(axes, flip, tokens_ref, gain_ref, key_hbm, value_hbm, *refs):
-    out_refs, (token_ref, key_ref, value_ref, made_ref, semaphores) = refs[:-5], refs[-5:]
+    heads = len(refs) - 6
+    out_refs, (token_ref, key_ref, value_ref, made_ref, loads, stores) = refs[:heads], refs[heads:]
     upper, lower, column = (lax.axis_index(axis) for axis in axes)
     seq = (upper * lax.axis_size(axes[1]) + lower) ^ flip
     pieces, rows = token_ref.shape[:2]
-    loads = [(tokens_ref.at[seq, pl.ds(i * rows, rows)], token_ref.at[i]) for i in range(pieces)]
-    loads[1:1] = [(key_hbm, key_ref), (value_hbm, value_ref)]
+    moves = [(tokens_ref.at[seq, pl.ds(i * rows, rows)], token_ref.at[i]) for i in range(pieces)]
+    moves += [(key_hbm, key_ref), (value_hbm, value_ref)]
     copies = [
-        pltpu.make_async_copy(source, target, semaphores.at[i])
-        for i, (source, target) in enumerate(loads)
+        pltpu.make_async_copy(source, target, loads.at[i]) for i, (source, target) in enumerate(moves)
     ]
     for copy in copies:
         copy.start()
+    normed = []
     for i in range(pieces):
-        copies[0 if i == 0 else i + 2].wait()
-        normed = normalize(token_ref[i], gain_ref[...])
-        if i == 0:
-            copies[1].wait()
-            copies[2].wait()
-        for head, both in enumerate(heads_made(normed, key_ref, value_ref)):
-            made_ref[head, i * rows : (i + 1) * rows] = both
-    for j, out_ref in enumerate(out_refs):
-        out_ref[...] = made_ref[column ^ j]
+        copies[i].wait()
+        normed.append(normalize(token_ref[i], gain_ref[...]))
+    copies[pieces].wait()
+    keys = [jnp.dot(value, key_ref[...], preferred_element_type=F32) for value in normed]
+    copies[pieces + 1].wait()
+    writes = []
+    for i in range(pieces):
+        values = jnp.dot(normed[i], value_ref[...], preferred_element_type=F32)
+        part = slice(i * rows, (i + 1) * rows)
+        for head in range(heads):
+            lanes = slice(head * HD, (head + 1) * HD)
+            both = jnp.concatenate([keys[i][:, lanes], values[:, lanes]], axis=-1)
+            made_ref[head, part] = both.astype(BF16)
+        for j, out_ref in enumerate(out_refs):
+            source = made_ref.at[column ^ j, pl.ds(i * rows, rows)]
+            target = out_ref.at[pl.ds(i * rows, rows)]
+            writes.append(pltpu.make_async_copy(source, target, stores.at[i, j]))
+            writes[-1].start()
+    for write in writes:
+        write.wait()
 
 
 def make_across(axes, flip, tokens, norm_gain, w_key, w_value):
@@ -179,7 +191,7 @@
     return pl.pallas_call(
         functools.partial(across_kernel, axes, flip),
         in_specs=[anywhere, vmem, anywhere, anywhere],
-        out_specs=[vmem] * heads,
+        out_specs=[anywhere] * heads,
         out_shape=[jax.ShapeDtypeStruct((positions, 2 * HD), BF16)] * heads,
         scratch_shapes=[
             pltpu.VMEM((pieces, positions // pieces, width), BF16),
@@ -187,6 +199,7 @@
             pltpu.VMEM(w_value.shape, BF16),
             pltpu.VMEM((heads, positions, 2 * HD), BF16),
             pltpu.SemaphoreType.DMA((pieces + 2,)),
+            pltpu.SemaphoreType.DMA((pieces, heads)),
         ],
         name="across",
     )(tokens, norm_gain, w_key, w_value)
@@ -314,7 +327,9 @@
     arrived_first = [swap(first[0], half, 0)]
     gates = after(cum_gate.reshape(devices, positions // LANES, LANES), first[0])
     gates = lax.all_to_all(gates, everyone, split_axis=0, concat_axis=0, tiled=True)
-    arrived_first += [swap(first[j], half, j) for j in range(1, heads)]
+    arrived_first += [swap(first[j], half, j) for j in range(1, heads - 1)]
+    last, gates = lax.optimization_barrier((first[-1], gates))
+    arrived_first.append(swap(last, half, heads - 1))
     queries = new_query.reshape(devices, group, HD)
     rest = make_rest(everyone, tokens, *weights, queries, gates, first)
     second, near, tile, cache = rest
@@ -329,20 +344,25 @@
             cache = lax.dynamic_update_slice(cache, blocks[j], (start, 0))
         return cache
 
-    columns = [1 << bit for bit in reversed(range(heads.bit_length() - 1))]
-    for step, j in enumerate(columns):
-        other = swap(tile, 0, j)
-        if step == len(columns) - 1:
-            cache = placed(cache, arrived_first, half, range(heads))
-            other, cache = lax.optimization_barrier((other, cache))
-        tile = merge([tile, other])
+    columns = [1 << bit for bit in reversed(range(1, heads.bit_length() - 1))]
+    for j in columns:
+        tile = merge([tile, swap(tile, 0, j)])
+    odd = (column & 1) == 1
+    low, high = tile[: devices // 2], tile[devices // 2 :]
+    tile = jnp.where(odd, high, low)
+    tile = merge([tile, swap(jnp.where(odd, low, high), 0, 1)])
     others = [swap(tile, k, 0) for k in range(1, seqs)]
+    early = max(heads - 2, 0)
+    cache = placed(cache, arrived_first, half, range(heads))
+    cache = placed(cache, arrived_second, half + 1, range(early))
     near_rows = arrived_near.reshape(half * heads * positions, 2 * HD)
     cache = lax.dynamic_update_slice(cache, near_rows, (near_first * heads * positions, 0))
-    cache = placed(cache, arrived_second, half + 1, range(heads - 1))
+    cache = placed(cache, arrived_second, half + 1, range(early, heads - 1))
     others, cache = lax.optimization_barrier((others, cache))
     tile = merge([tile] + others)
-    first_read = tile[..., HD:] / tile[..., 1:2]
+    tile = tile / tile[..., 1:2]
+    other = swap(tile, 0, 1)
+    first_read = jnp.concatenate([jnp.where(odd, other, tile), jnp.where(odd, tile, other)])[..., HD:]
     cache = placed(cache, arrived_second, half + 1, range(heads - 1, heads))
     return cache.reshape(1, 1, rows, 2 * HD), first_read.reshape(seqs, query_heads, HD)
 

time: 75.2 us -> 70.1 us (0.932)
  starting transfers between devices: 37.3 us -> 28.7 us
  waiting for transfers between devices: 9.5 us -> 14 us
  local copies, waits for them, and re-layouts: 9.71 us -> 8.16 us
    ppermute x13 -> x14, starting transfers between devices: 26.3 us -> 17.6 us  [swap(): return lax.ppermute(value, everyone, pairs)]
    all_to_all x1, waiting for transfers between devices: 0.01 us -> 5.1 us  [read_beside(): lax.all_to_all(near, ('lo', 'tp'), split_axis=0, concat_axis=0, tiled=True)]
    mul x8 -> x2, local copies, waits for them, and re-layouts: 1.3 us -> 0.32 us  [merged(): both = sum((tile * factor for tile, factor in zip(tiles, factors)))]
    ppermute x13 -> x14, waiting for transfers between devices: 8.98 us -> 8.07 us  [swap(): return lax.ppermute(value, everyone, pairs)]
  transfers between devices with their start and end apart: 15 -> 16, of which waited for: 4 -> 7; matrix products, arithmetic and copies ran while one was open for 14% -> 12% of each run, Pallas kernels for 14% -> 16%
where the time goes in v3:
time: 70.1 us; the launch traced here: 69.8 us
  starting transfers between devices  28.7 us (41%)
  Pallas kernels  16.4 us (23%)
  waiting for transfers between devices  14 us (20%)
  local copies, waits for them, and re-layouts  8.16 us (12%)
  other arithmetic  1.79 us (3%)
  between operations  0.83 us (1%)
    ppermute x14, starting transfers between devices, swap(): return lax.ppermute(value, everyone, pairs)  17.6 us
    pallas_call x1, Pallas kernels, make_rest(): pl.pallas_call(functools.partial(rest_kernel, axes, heads), grid=(near +...  11.2 us
    ppermute x14, waiting for transfers between devices, swap(): return lax.ppermute(value, everyone, pairs)  8.07 us
    all_to_all x1, starting transfers between devices, read_beside(): lax.all_to_all(gates, everyone, split_axis=0, concat_axis=0, tiled=True)  7.43 us
    dynamic_update_slice x8, local copies, waits for them, and re-layouts, placed(): cache = lax.dynamic_update_slice(cache, blocks[j], (start, 0))  5.32 us
    pallas_call x1, Pallas kernels, make_across(): pl.pallas_call(functools.partial(across_kernel, axes, flip), in_specs=[an...  5.14 us
    all_to_all x1, waiting for transfers between devices, read_beside(): lax.all_to_all(near, ('lo', 'tp'), split_axis=0, concat_axis=0, tiled=True)  5.1 us
    all_to_all x1, starting transfers between devices, read_beside(): lax.all_to_all(near, ('lo', 'tp'), split_axis=0, concat_axis=0, tiled=True)  3.69 us
  transfers between devices with their start and end apart: 16, of which 7 were waited for; matrix products, arithmetic and copies ran while one was open for 12% of the time, Pallas kernels for 16%

profile of v3, /device:TPU:0, one launch (start us, length us, event | category | flops | bytes accessed | tf_op | source)
XLA Modules:
  0.0 69.8 jit_solution(4612688404906300215)
XLA Ops:
  0.6 5.1 %across.1 = (bf16[512,128]{1,0:T(8,128)(2,1)}, bf16[512,128]{1,0:T(8,128)(2,1)}, bf16[512,128]{1,0:T(8,128)(2,1)}, bf16[512,128]{1,0:T(8,128)(2,1)}) custom-call(bf16[4,512,2048]{2,1,0:T(8,128)(2,1)} %tokens_ref.3, f32[1,2048]{1,0:T(1,128)} %bitcast.25, bf16[2048,256]{1,0:T(8,128)(2,1)} %key_ref.1, bf16[2048,256]{1,0:T(8,128)(2,1)} %value_ref.1), custom_call_target="tpu_custom_call" | custom-call | tf_op jit(solution)/shard_map/across/pallas_call | solution.py:191
  5.8 7.4 %all-to-all-start = ((f32[16,4,128]{2,1,0:T(4,128)}), f32[16,4,128]{2,1,0:T(4,128)S(1)}, u32[]{:S(2)}, u32[]{:S(2)}) async-start(f32[16,4,128]{2,1,0:T(4,128)} %bitcast.2), calls=%async_computation | async-start | bytes 65536 | tf_op jit(solution)/shard_map/all_to_all | solution.py:329
  13.2 2.8 %collective-permute-start.5 = (bf16[512,128]{1,0:T(8,128)(2,1)}, bf16[512,128]{1,0:T(8,128)(2,1)S(1)}, u32[]{:S(2)}, u32[]{:S(2)}) collective-permute-start(bf16[512,128]{1,0:T(8,128)(2,1)} %get-tuple-element.21.refs_0_), channel_id=1, source_target_pairs={{0,8},{1,9},{2,10},{3,11},{4,12},{5,13},{6,14},{7,15},{8,0},{9,1},... | collective-permute-start | bytes 393224 | tf_op jit(solution)/shard_map/ppermute | solution.py:324
  16.0 0.0 collective-permute-start.6
  16.0 3.3 %collective-permute-start.7 = (bf16[512,128]{1,0:T(8,128)(2,1)}, bf16[512,128]{1,0:T(8,128)(2,1)S(1)}, u32[]{:S(2)}, u32[]{:S(2)}) collective-permute-start(bf16[512,128]{1,0:T(8,128)(2,1)} %get-tuple-element.25.refs_2_), channel_id=1, source_target_pairs={{0,10},{1,11},{2,8},{3,9},{4,14},{5,15},{6,12},{7,13},{8,2},{9,3},... | collective-permute-start | bytes 393224 | tf_op jit(solution)/shard_map/ppermute | solution.py:324
  19.3 0.8 %all-to-all-done.gate_ref = f32[16,4,128]{2,1,0:T(4,128)S(1)} async-done(((f32[16,4,128]{2,1,0:T(4,128)}), f32[16,4,128]{2,1,0:T(4,128)S(1)}, u32[]{:S(2)}, u32[]{:S(2)}) %all-to-all-start) | async-done | bytes 32800 | tf_op jit(solution)/shard_map/all_to_all | solution.py:329
  20.1 0.6 copy-done.2
  20.7 11.2 %rest.1 = (bf16[512,128]{1,0:T(8,128)(2,1)}, bf16[512,128]{1,0:T(8,128)(2,1)}, bf16[512,128]{1,0:T(8,128)(2,1)}, bf16[512,128]{1,0:T(8,128)(2,1)}, bf16[2,4,512,...) custom-call(bf16[4,512,2048]{2,1,0:T(8,128)(2,1)} %tokens_ref.3, f32[1,2048]{1,0:T(1,128)} %bitcast.26, ...), custom_call_target="tpu_custom_call" | custom-call | tf_op jit(solution)/shard_map/rest/pallas_call | solution.py:270
  32.0 0.2 collective-permute-start
  32.2 0.0 copy-done.1
  32.2 1.0 %collective-permute-start.8 = (bf16[512,128]{1,0:T(8,128)(2,1)S(1)}, bf16[512,128]{1,0:T(8,128)(2,1)S(1)}, u32[]{:S(2)}, u32[]{:S(2)}) collective-permute-start(bf16[512,128]{1,0:T(8,128)(2,1)S(1)} %copy-done.1), channel_id=1, source_target_pairs={{0,11},{1,10},{2,9},{3,8},{4,15},{5,14},{6,13},{7,12},{8,3},{9,2},... | collective-permute-start | bytes 393224 | tf_op jit(solution)/shard_map/ppermute | solution.py:324
  33.2 3.7 %all-to-all-start.1 = ((bf16[8,512,128]{2,1,0:T(8,128)(2,1)}), bf16[8,512,128]{2,1,0:T(8,128)(2,1)S(1)}, u32[]{:S(2)}, u32[]{:S(2)}) async-start(bf16[8,512,128]{2,1,0:T(8,128)(2,1)} %bitcast.18), calls=%async_computation.1 | async-start | bytes 2097152 | tf_op jit(solution)/shard_map/all_to_all | solution.py:338
  36.9 0.9 %collective-permute-done = f32[16,8,128]{2,1,0:T(8,128)S(1)} collective-permute-done((f32[16,8,128]{2,1,0:T(8,128)}, f32[16,8,128]{2,1,0:T(8,128)S(1)}, u32[]{:S(2)}, u32[]{:S(2)}) %collective-permute-start) | collective-permute-done | bytes 65568 | tf_op jit(solution)/shard_map/ppermute | solution.py:324
  37.8 2.7 %collective-permute-start.9 = (bf16[512,128]{1,0:T(8,128)(2,1)S(1)}, bf16[512,128]{1,0:T(8,128)(2,1)S(1)}, u32[]{:S(2)}, u32[]{:S(2)}) collective-permute-start(bf16[512,128]{1,0:T(8,128)(2,1)S(1)} %copy-done.6), channel_id=1, source_target_pairs={{0,12},{1,13},{2,14},{3,15},{4,8},{5,9},{6,10},{7,11},{8,4},{9,5},... | collective-permute-start | bytes 393224 | tf_op jit(solution)/shard_map/ppermute | solution.py:324
  40.6 0.2 copy.33
  40.7 0.2 copy.32
  40.9 0.1 multiply_add_fusion
  41.0 0.2 copy.34
  41.2 0.1 slice.69
  41.3 0.2 copy.35
  41.4 0.1 select_select_fusion
  41.6 0.0 collective-permute-done.5
  41.6 0.3 collective-permute-start.10
  41.8 0.7 constant_dynamic-update-slice_fusion.7
  42.5 0.0 collective-permute-done.6
  42.5 4.0 %collective-permute-start.11 = (bf16[512,128]{1,0:T(8,128)(2,1)S(1)}, bf16[512,128]{1,0:T(8,128)(2,1)S(1)}, u32[]{:S(2)}, u32[]{:S(2)}) collective-permute-start(bf16[512,128]{1,0:T(8,128)(2,1)S(1)} %copy-done.4), channel_id=1, source_target_pairs={{0,14},{1,15},{2,12},{3,13},{4,10},{5,11},{6,8},{7,9},{8,6},{9,7},... | collective-permute-start | bytes 393224 | tf_op jit(solution)/shard_map/ppermute | solution.py:324
  46.5 0.7 constant_dynamic-update-slice_fusion.6
  47.2 0.0 collective-permute-done.7
  47.2 0.4 collective-permute-start.1
  47.6 0.7 constant_dynamic-update-slice_fusion.5
  48.2 0.2 collective-permute-done.1
  48.4 1.0 %collective-permute-start.12 = (bf16[512,128]{1,0:T(8,128)(2,1)S(1)}, bf16[512,128]{1,0:T(8,128)(2,1)S(1)}, u32[]{:S(2)}, u32[]{:S(2)}) collective-permute-start(bf16[512,128]{1,0:T(8,128)(2,1)S(1)} %copy-done.3), channel_id=1, source_target_pairs={{0,15},{1,14},{2,13},{3,12},{4,11},{5,10},{6,9},{7,8},{8,7},{9,6},... | collective-permute-start | bytes 393224 | tf_op jit(solution)/shard_map/ppermute | solution.py:324
  49.5 0.1 fusion
  49.6 0.1 multiply_add_fusion.2
  49.7 0.2 slice_reduce_fusion.2
  49.8 0.1 select_select_fusion.2
  49.9 0.0 collective-permute-done.8
  49.9 0.1 collective-permute-start.2
  50.0 0.7 constant_dynamic-update-slice_fusion.4
  50.7 5.7 %collective-permute-done.9 = bf16[512,128]{1,0:T(8,128)(2,1)S(1)} collective-permute-done((bf16[512,128]{1,0:T(8,128)(2,1)S(1)}, bf16[512,128]{1,0:T(8,128)(2,1)S(1)}, u32[]{:S(2)}, u32[]{:S(2)}) %collective-permute-start.9) | collective-permute-done | bytes 131104 | tf_op jit(solution)/shard_map/ppermute | solution.py:324
  56.4 0.0 collective-permute-start.3
  56.4 0.7 constant_dynamic-update-slice_fusion.3
  57.0 1.0 %collective-permute-done.10 = bf16[512,128]{1,0:T(8,128)(2,1)S(1)} collective-permute-done((bf16[512,128]{1,0:T(8,128)(2,1)S(1)}, bf16[512,128]{1,0:T(8,128)(2,1)S(1)}, u32[]{:S(2)}, u32[]{:S(2)}) %collective-permute-start.10) | collective-permute-done | bytes 131104 | tf_op jit(solution)/shard_map/ppermute | solution.py:324
  58.1 1.1 %collective-permute-start.4 = (f32[8,8,128]{2,1,0:T(8,128)S(1)}, f32[8,8,128]{2,1,0:T(8,128)S(1)}, u32[]{:S(2)}, u32[]{:S(2)}) collective-permute-start(f32[8,8,128]{2,1,0:T(8,128)S(1)} %select_select_fusion.2), channel_id=1, source_target_pairs={{0,12},{1,13},{2,14},{3,15},{4,8},{5,9},{6,10},{7,11},{8,4},{9,5},... | collective-permute-start | bytes 98312 | tf_op jit(solution)/shard_map/ppermute | solution.py:324
  59.2 0.7 constant_dynamic-update-slice_fusion.2
  59.9 5.1 %all-to-all-done.1 = bf16[8,512,128]{2,1,0:T(8,128)(2,1)S(1)} async-done(((bf16[8,512,128]{2,1,0:T(8,128)(2,1)}), bf16[8,512,128]{2,1,0:T(8,128)(2,1)S(1)}, u32[]{:S(2)}, u32[]{:S(2)}) %all-to-all-start.1) | async-done | bytes 1048608 | tf_op jit(solution)/shard_map/all_to_all | solution.py:338
  65.0 1.0 %constant_dynamic-update-slice_fusion.1 = bf16[8192,128]{1,0:T(8,128)(2,1)} fusion(bf16[8192,128]{1,0:T(8,128)(2,1)} %constant_dynamic-update-slice_fusion.2, bf16[4096,128]{1,0:T(8,128)(2,1)S(1)} %bitcast.17, s32[]{:T(128)S(6)} %select_n.82), kind=kLoop, calls=%fused_computation.28 | loop fusion | bytes 2097156 | tf_op jit(solution)/shard_map/dynamic_update_slice | solution.py:359
  66.0 0.0 collective-permute-done.11
  66.0 0.7 constant_dynamic-update-slice_fusion
  66.7 0.0 collective-permute-done.2
  66.7 0.0 collective-permute-done.3
  66.7 0.0 collective-permute-done.4
  66.7 0.1 fusion.1
  66.8 0.1 multiply_add_fusion.1
  66.9 0.2 slice_reduce_fusion.1
  67.1 0.1 select_select_fusion.1
  67.2 0.2 slice_reduce_fusion
  67.3 0.1 broadcast_divide_fusion
  67.4 0.7 %collective-permute-start.13 = (f32[8,8,128]{2,1,0:T(8,128)S(1)}, f32[8,8,128]{2,1,0:T(8,128)S(1)}, u32[]{:S(2)}, u32[]{:S(2)}) collective-permute-start(f32[8,8,128]{2,1,0:T(8,128)S(1)} %broadcast_divide_fusion), channel_id=1, source_target_pairs={{0,1},{1,0},{2,3},{3,2},{4,5},{5,4},{6,7},{7,6},{8,9},{9,8},{10,11... | collective-permute-start | bytes 98312 | tf_op jit(solution)/shard_map/ppermute | solution.py:324
  68.2 0.0 collective-permute-done.12
  68.2 0.7 bitcast_dynamic-update-slice_fusion
  68.8 0.2 collective-permute-done.13
  69.0 0.1 broadcast_select_fusion.1
  69.1 0.7 %pad_maximum_fusion = f32[16,8,64]{2,1,0:T(8,128)} fusion(f32[8,8,128]{2,1,0:T(8,128)S(1)} %get-tuple-element.49, f32[8,8,128]{2,1,0:T(8,128)S(1)} %get-tuple-element.48), kind=kLoop, calls=%fused_computation.1 | loop fusion | flops 8192 | bytes 98304 | tf_op jit(solution)/shard_map/concatenate | solution.py:365
  (16 shorter events, 0.1 us)
Async XLA Ops:
  5.8 14.3 %all-to-all-start = ((f32[16,4,128]{2,1,0:T(4,128)}), f32[16,4,128]{2,1,0:T(4,128)S(1)}, u32[]{:S(2)}, u32[]{:S(2)}) async-start(f32[16,4,128]{2,1,0:T(4,128)} %bitcast.2), calls=%async_computation | async-start | bytes 65536 | tf_op jit(solution)/shard_map/all_to_all | solution.py:329
  13.2 28.3 %collective-permute-start.5 = (bf16[512,128]{1,0:T(8,128)(2,1)}, bf16[512,128]{1,0:T(8,128)(2,1)S(1)}, u32[]{:S(2)}, u32[]{:S(2)}) collective-permute-start(bf16[512,128]{1,0:T(8,128)(2,1)} %get-tuple-element.21.refs_0_), channel_id=1, source_target_pairs={{0,8},{1,9},{2,10},{3,11},{4,12},{5,13},{6,14},{7,15},{8,0},{9,1},... | collective-permute-start | bytes 393224 | tf_op jit(solution)/shard_map/ppermute | solution.py:324
  16.0 26.5 %collective-permute-start.6 = (bf16[512,128]{1,0:T(8,128)(2,1)}, bf16[512,128]{1,0:T(8,128)(2,1)S(1)}, u32[]{:S(2)}, u32[]{:S(2)}) collective-permute-start(bf16[512,128]{1,0:T(8,128)(2,1)} %get-tuple-element.24.refs_1_), channel_id=1, source_target_pairs={{0,9},{1,8},{2,11},{3,10},{4,13},{5,12},{6,15},{7,14},{8,1},{9,0},... | collective-permute-start | bytes 393224 | tf_op jit(solution)/shard_map/ppermute | solution.py:324
  16.0 31.1 %collective-permute-start.7 = (bf16[512,128]{1,0:T(8,128)(2,1)}, bf16[512,128]{1,0:T(8,128)(2,1)S(1)}, u32[]{:S(2)}, u32[]{:S(2)}) collective-permute-start(bf16[512,128]{1,0:T(8,128)(2,1)} %get-tuple-element.25.refs_2_), channel_id=1, source_target_pairs={{0,10},{1,11},{2,8},{3,9},{4,14},{5,15},{6,12},{7,13},{8,2},{9,3},... | collective-permute-start | bytes 393224 | tf_op jit(solution)/shard_map/ppermute | solution.py:324
  20.1 0.6 copy-start.2
  20.7 11.4 %copy-start.1 = (bf16[512,128]{1,0:T(8,128)(2,1)S(1)}, bf16[512,128]{1,0:T(8,128)(2,1)}, u32[]{:S(2)}) copy-start(bf16[512,128]{1,0:T(8,128)(2,1)} %get-tuple-element.28.refs_3_) | copy-start | bytes 393220
  32.0 5.8 %copy-start.6 = (bf16[512,128]{1,0:T(8,128)(2,1)S(1)}, bf16[512,128]{1,0:T(8,128)(2,1)}, u32[]{:S(2)}) copy-start(bf16[512,128]{1,0:T(8,128)(2,1)} %get-tuple-element.29) | copy-start | bytes 393220
  32.0 8.6 %copy-start = (f32[16,8,128]{2,1,0:T(8,128)S(1)}, f32[16,8,128]{2,1,0:T(8,128)}, u32[]{:S(2)}) copy-start(f32[16,8,128]{2,1,0:T(8,128)} %get-tuple-element.26) | copy-start | bytes 196612
  32.0 9.6 %copy-start.5 = (bf16[512,128]{1,0:T(8,128)(2,1)S(1)}, bf16[512,128]{1,0:T(8,128)(2,1)}, u32[]{:S(2)}) copy-start(bf16[512,128]{1,0:T(8,128)(2,1)} %get-tuple-element.30) | copy-start | bytes 393220
  32.0 10.5 %copy-start.4 = (bf16[512,128]{1,0:T(8,128)(2,1)S(1)}, bf16[512,128]{1,0:T(8,128)(2,1)}, u32[]{:S(2)}) copy-start(bf16[512,128]{1,0:T(8,128)(2,1)} %get-tuple-element.32) | copy-start | bytes 393220
  32.0 5.8 %collective-permute-start = (f32[16,8,128]{2,1,0:T(8,128)}, f32[16,8,128]{2,1,0:T(8,128)S(1)}, u32[]{:S(2)}, u32[]{:S(2)}) collective-permute-start(f32[16,8,128]{2,1,0:T(8,128)} %get-tuple-element.26), channel_id=1, source_target_pairs={{0,2},{1,3},{2,0},{3,1},{4,6},{5,7},{6,4},{7,5},{8,10},{9,11},{10,... | collective-permute-start | bytes 196616 | tf_op jit(solution)/shard_map/ppermute | solution.py:324
  32.2 17.7 %collective-permute-start.8 = (bf16[512,128]{1,0:T(8,128)(2,1)S(1)}, bf16[512,128]{1,0:T(8,128)(2,1)S(1)}, u32[]{:S(2)}, u32[]{:S(2)}) collective-permute-start(bf16[512,128]{1,0:T(8,128)(2,1)S(1)} %copy-done.1), channel_id=1, source_target_pairs={{0,11},{1,10},{2,9},{3,8},{4,15},{5,14},{6,13},{7,12},{8,3},{9,2},... | collective-permute-start | bytes 393224 | tf_op jit(solution)/shard_map/ppermute | solution.py:324
  33.2 15.3 %copy-start.3 = (bf16[512,128]{1,0:T(8,128)(2,1)S(1)}, bf16[512,128]{1,0:T(8,128)(2,1)}, u32[]{:S(2)}) copy-start(bf16[512,128]{1,0:T(8,128)(2,1)} %get-tuple-element.34) | copy-start | bytes 393220
  33.2 31.8 %all-to-all-start.1 = ((bf16[8,512,128]{2,1,0:T(8,128)(2,1)}), bf16[8,512,128]{2,1,0:T(8,128)(2,1)S(1)}, u32[]{:S(2)}, u32[]{:S(2)}) async-start(bf16[8,512,128]{2,1,0:T(8,128)(2,1)} %bitcast.18), calls=%async_computation.1 | async-start | bytes 2097152 | tf_op jit(solution)/shard_map/all_to_all | solution.py:338
  37.8 18.6 %collective-permute-start.9 = (bf16[512,128]{1,0:T(8,128)(2,1)S(1)}, bf16[512,128]{1,0:T(8,128)(2,1)S(1)}, u32[]{:S(2)}, u32[]{:S(2)}) collective-permute-start(bf16[512,128]{1,0:T(8,128)(2,1)S(1)} %copy-done.6), channel_id=1, source_target_pairs={{0,12},{1,13},{2,14},{3,15},{4,8},{5,9},{6,10},{7,11},{8,4},{9,5},... | collective-permute-start | bytes 393224 | tf_op jit(solution)/shard_map/ppermute | solution.py:324
  41.6 16.5 %collective-permute-start.10 = (bf16[512,128]{1,0:T(8,128)(2,1)S(1)}, bf16[512,128]{1,0:T(8,128)(2,1)S(1)}, u32[]{:S(2)}, u32[]{:S(2)}) collective-permute-start(bf16[512,128]{1,0:T(8,128)(2,1)S(1)} %copy-done.5), channel_id=1, source_target_pairs={{0,13},{1,12},{2,15},{3,14},{4,9},{5,8},{6,11},{7,10},{8,5},{9,4},... | collective-permute-start | bytes 393224 | tf_op jit(solution)/shard_map/ppermute | solution.py:324
  42.5 23.5 %collective-permute-start.11 = (bf16[512,128]{1,0:T(8,128)(2,1)S(1)}, bf16[512,128]{1,0:T(8,128)(2,1)S(1)}, u32[]{:S(2)}, u32[]{:S(2)}) collective-permute-start(bf16[512,128]{1,0:T(8,128)(2,1)S(1)} %copy-done.4), channel_id=1, source_target_pairs={{0,14},{1,15},{2,12},{3,13},{4,10},{5,11},{6,8},{7,9},{8,6},{9,7},... | collective-permute-start | bytes 393224 | tf_op jit(solution)/shard_map/ppermute | solution.py:324
  47.2 1.2 %collective-permute-start.1 = (f32[8,8,128]{2,1,0:T(8,128)S(1)}, f32[8,8,128]{2,1,0:T(8,128)S(1)}, u32[]{:S(2)}, u32[]{:S(2)}) collective-permute-start(f32[8,8,128]{2,1,0:T(8,128)S(1)} %get-tuple-element.51), channel_id=1, source_target_pairs={{0,1},{1,0},{2,3},{3,2},{4,5},{5,4},{6,7},{7,6},{8,9},{9,8},{10,11... | collective-permute-start | bytes 98312 | tf_op jit(solution)/shard_map/ppermute | solution.py:324
  48.4 19.7 %collective-permute-start.12 = (bf16[512,128]{1,0:T(8,128)(2,1)S(1)}, bf16[512,128]{1,0:T(8,128)(2,1)S(1)}, u32[]{:S(2)}, u32[]{:S(2)}) collective-permute-start(bf16[512,128]{1,0:T(8,128)(2,1)S(1)} %copy-done.3), channel_id=1, source_target_pairs={{0,15},{1,14},{2,13},{3,12},{4,11},{5,10},{6,9},{7,8},{8,7},{9,6},... | collective-permute-start | bytes 393224 | tf_op jit(solution)/shard_map/ppermute | solution.py:324
  49.9 16.8 %collective-permute-start.2 = (f32[8,8,128]{2,1,0:T(8,128)S(1)}, f32[8,8,128]{2,1,0:T(8,128)S(1)}, u32[]{:S(2)}, u32[]{:S(2)}) collective-permute-start(f32[8,8,128]{2,1,0:T(8,128)S(1)} %select_select_fusion.2), channel_id=1, source_target_pairs={{0,4},{1,5},{2,6},{3,7},{4,0},{5,1},{6,2},{7,3},{8,12},{9,13},{10,... | collective-permute-start | bytes 98312 | tf_op jit(solution)/shard_map/ppermute | solution.py:324
  56.4 10.3 %collective-permute-start.3 = (f32[8,8,128]{2,1,0:T(8,128)S(1)}, f32[8,8,128]{2,1,0:T(8,128)S(1)}, u32[]{:S(2)}, u32[]{:S(2)}) collective-permute-start(f32[8,8,128]{2,1,0:T(8,128)S(1)} %select_select_fusion.2), channel_id=1, source_target_pairs={{0,8},{1,9},{2,10},{3,11},{4,12},{5,13},{6,14},{7,15},{8,0},{9,1},... | collective-permute-start | bytes 98312 | tf_op jit(solution)/shard_map/ppermute | solution.py:324
  58.1 8.6 %collective-permute-start.4 = (f32[8,8,128]{2,1,0:T(8,128)S(1)}, f32[8,8,128]{2,1,0:T(8,128)S(1)}, u32[]{:S(2)}, u32[]{:S(2)}) collective-permute-start(f32[8,8,128]{2,1,0:T(8,128)S(1)} %select_select_fusion.2), channel_id=1, source_target_pairs={{0,12},{1,13},{2,14},{3,15},{4,8},{5,9},{6,10},{7,11},{8,4},{9,5},... | collective-permute-start | bytes 98312 | tf_op jit(solution)/shard_map/ppermute | solution.py:324
  67.4 1.6 %collective-permute-start.13 = (f32[8,8,128]{2,1,0:T(8,128)S(1)}, f32[8,8,128]{2,1,0:T(8,128)S(1)}, u32[]{:S(2)}, u32[]{:S(2)}) collective-permute-start(f32[8,8,128]{2,1,0:T(8,128)S(1)} %broadcast_divide_fusion), channel_id=1, source_target_pairs={{0,1},{1,0},{2,3},{3,2},{4,5},{5,4},{6,7},{7,6},{8,9},{9,8},{10,11... | collective-permute-start | bytes 98312 | tf_op jit(solution)/shard_map/ppermute | solution.py:324

commit v4 on v3

--- a/solution.py
+++ b/solution.py
@@ -147,13 +147,14 @@
 
 
 def across_kernel(axes, flip, tokens_ref, gain_ref, key_hbm, value_hbm, *refs):
-    heads = len(refs) - 6
-    out_refs, (token_ref, key_ref, value_ref, made_ref, loads, stores) = refs[:heads], refs[heads:]
+    heads = len(refs) - 5
+    out_refs, (token_ref, weight_ref, made_ref, loads, stores) = refs[:heads], refs[heads:]
     upper, lower, column = (lax.axis_index(axis) for axis in axes)
     seq = (upper * lax.axis_size(axes[1]) + lower) ^ flip
     pieces, rows = token_ref.shape[:2]
     moves = [(tokens_ref.at[seq, pl.ds(i * rows, rows)], token_ref.at[i]) for i in range(pieces)]
-    moves += [(key_hbm, key_ref), (value_hbm, value_ref)]
+    wide = key_hbm.shape[1]
+    moves += [(key_hbm, weight_ref.at[:, pl.ds(0, wide)]), (value_hbm, weight_ref.at[:, pl.ds(wide, wide)])]
     copies = [
         pltpu.make_async_copy(source, target, loads.at[i]) for i, (source, target) in enumerate(moves)
     ]
@@ -164,16 +165,15 @@
         copies[i].wait()
         normed.append(normalize(token_ref[i], gain_ref[...]))
     copies[pieces].wait()
-    keys = [jnp.dot(value, key_ref[...], preferred_element_type=F32) for value in normed]
     copies[pieces + 1].wait()
     writes = []
     for i in range(pieces):
-        values = jnp.dot(normed[i], value_ref[...], preferred_element_type=F32)
+        made = jnp.dot(normed[i], weight_ref[...], preferred_element_type=F32)
         part = slice(i * rows, (i + 1) * rows)
         for head in range(heads):
-            lanes = slice(head * HD, (head + 1) * HD)
-            both = jnp.concatenate([keys[i][:, lanes], values[:, lanes]], axis=-1)
-            made_ref[head, part] = both.astype(BF16)
+            k = made[:, head * HD : (head + 1) * HD]
+            v = made[:, wide + head * HD : wide + (head + 1) * HD]
+            made_ref[head, part] = jnp.concatenate([k, v], axis=-1).astype(BF16)
         for j, out_ref in enumerate(out_refs):
             source = made_ref.at[column ^ j, pl.ds(i * rows, rows)]
             target = out_ref.at[pl.ds(i * rows, rows)]
@@ -195,8 +195,7 @@
         out_shape=[jax.ShapeDtypeStruct((positions, 2 * HD), BF16)] * heads,
         scratch_shapes=[
             pltpu.VMEM((pieces, positions // pieces, width), BF16),
-            pltpu.VMEM(w_key.shape, BF16),
-            pltpu.VMEM(w_value.shape, BF16),
+            pltpu.VMEM((width, 2 * w_key.shape[1]), BF16),
             pltpu.VMEM((heads, positions, 2 * HD), BF16),
             pltpu.SemaphoreType.DMA((pieces + 2,)),
             pltpu.SemaphoreType.DMA((pieces, heads)),
@@ -324,12 +323,11 @@
         return lax.ppermute(value, everyone, pairs)
 
     first = make_across(everyone, half, tokens, *weights)
-    arrived_first = [swap(first[0], half, 0)]
     gates = after(cum_gate.reshape(devices, positions // LANES, LANES), first[0])
     gates = lax.all_to_all(gates, everyone, split_axis=0, concat_axis=0, tiled=True)
-    arrived_first += [swap(first[j], half, j) for j in range(1, heads - 1)]
-    last, gates = lax.optimization_barrier((first[-1], gates))
-    arrived_first.append(swap(last, half, heads - 1))
+    ready, gates = lax.optimization_barrier((first[3], gates))
+    blocks = [ready if j == 3 else block for j, block in enumerate(first)]
+    arrived_first = [swap(block, half, j) for j, block in enumerate(blocks)]
     queries = new_query.reshape(devices, group, HD)
     rest = make_rest(everyone, tokens, *weights, queries, gates, first)
     second, near, tile, cache = rest
@@ -338,11 +336,15 @@
     arrived_near = lax.all_to_all(near, ("lo", "tp"), split_axis=0, concat_axis=0, tiled=True)
     rows = devices * positions
 
-    def placed(cache, blocks, k, columns):
-        for j in columns:
-            start = ((plane ^ k) * heads + (column ^ j)) * positions
-            cache = lax.dynamic_update_slice(cache, blocks[j], (start, 0))
-        return cache
+    def placed(cache, blocks, k):
+        for bit in range(heads.bit_length() - 1):
+            swapped = ((column >> bit) & 1) == 1
+            blocks = [
+                jnp.where(swapped, blocks[head ^ (1 << bit)], block)
+                for head, block in enumerate(blocks)
+            ]
+        start = (plane ^ k) * heads * positions
+        return lax.dynamic_update_slice(cache, jnp.concatenate(blocks), (start, 0))
 
     columns = [1 << bit for bit in reversed(range(1, heads.bit_length() - 1))]
     for j in columns:
@@ -352,18 +354,15 @@
     tile = jnp.where(odd, high, low)
     tile = merge([tile, swap(jnp.where(odd, low, high), 0, 1)])
     others = [swap(tile, k, 0) for k in range(1, seqs)]
-    early = max(heads - 2, 0)
-    cache = placed(cache, arrived_first, half, range(heads))
-    cache = placed(cache, arrived_second, half + 1, range(early))
+    cache = placed(cache, arrived_first, half)
     near_rows = arrived_near.reshape(half * heads * positions, 2 * HD)
     cache = lax.dynamic_update_slice(cache, near_rows, (near_first * heads * positions, 0))
-    cache = placed(cache, arrived_second, half + 1, range(early, heads - 1))
-    others, cache = lax.optimization_barrier((others, cache))
     tile = merge([tile] + others)
     tile = tile / tile[..., 1:2]
     other = swap(tile, 0, 1)
-    first_read = jnp.concatenate([jnp.where(odd, other, tile), jnp.where(odd, tile, other)])[..., HD:]
-    cache = placed(cache, arrived_second, half + 1, range(heads - 1, heads))
+    pair = [jnp.where(odd, other, tile), jnp.where(odd, tile, other)]
+    first_read = jnp.concatenate(pair)[..., HD:]
+    cache = placed(cache, arrived_second, half + 1)
     return cache.reshape(1, 1, rows, 2 * HD), first_read.reshape(seqs, query_heads, HD)
 
 
@@ -386,7 +385,7 @@
         heads = w_key.shape[1] // HD
         alone = sp_count == seqs and tp_count == heads
         even = power_of_two(seqs) and power_of_two(heads) and positions % LANES == 0
-        body = read_beside if alone and even else functools.partial(read_after, sp_axes)
+        body = read_beside if alone and even and seqs // 2 == 2 else functools.partial(read_after, sp_axes)
         return body(tokens, norm_gain.reshape(1, width), w_key, w_value, new_query, cum_gate)
 
     sp = sp_axes if isinstance(sp_axes, tuple) else (sp_axes,)

time: 70.1 us -> 98.2 us (1.40)
  starting transfers between devices: 28.7 us -> 50.3 us
  waiting for transfers between devices: 14 us -> 22.6 us
  local copies, waits for them, and re-layouts: 8.16 us -> 2.83 us
  other arithmetic: 1.79 us -> 5.24 us
    ppermute x14, starting transfers between devices: 17.6 us -> 39.3 us  [swap(): return lax.ppermute(value, everyone, pairs)]
    ppermute x14, waiting for transfers between devices: 8.07 us -> 15.9 us  [swap(): return lax.ppermute(value, everyone, pairs)]
    all_to_all x1, waiting for transfers between devices: 0.8 us -> 6.63 us  [read_beside(): lax.all_to_all(gates, everyone, split_axis=0, concat_axis=0, tiled=True)]
    dynamic_update_slice x8 -> x0, local copies, waits for them, and re-layouts: 5.32 us -> none  [placed(): cache = lax.dynamic_update_slice(cache, blocks[j], (start, 0))]
    all_to_all x1, waiting for transfers between devices: 5.1 us -> 0.01 us  [read_beside(): lax.all_to_all(near, ('lo', 'tp'), split_axis=0, concat_axis=0, tiled=True)]
    dynamic_update_slice x0 -> x2, other arithmetic: none -> 1.65 us  [placed(): return lax.dynamic_update_slice(cache, jnp.concatenate(blocks), (start, 0))]
  transfers between devices with their start and end apart: 16 -> 16, of which waited for: 7 -> 7; matrix products, arithmetic and copies ran while one was open for 12% -> 3% of each run, Pallas kernels for 16% -> 0%
where the time goes in v4:
time: 98.2 us; the launch traced here: 97.8 us
  starting transfers between devices  50.3 us (51%)
  waiting for transfers between devices  22.6 us (23%)
  Pallas kernels  16 us (16%)
  other arithmetic  5.24 us (5%)
  local copies, waits for them, and re-layouts  2.83 us (3%)
    ppermute x14, starting transfers between devices, swap(): return lax.ppermute(value, everyone, pairs)  39.3 us
    ppermute x14, waiting for transfers between devices, swap(): return lax.ppermute(value, everyone, pairs)  15.9 us
    pallas_call x1, Pallas kernels, make_rest(): pl.pallas_call(functools.partial(rest_kernel, axes, heads), grid=(near +...  11 us
    all_to_all x1, starting transfers between devices, read_beside(): lax.all_to_all(gates, everyone, split_axis=0, concat_axis=0, tiled=True)  7.43 us
    all_to_all x1, waiting for transfers between devices, read_beside(): lax.all_to_all(gates, everyone, split_axis=0, concat_axis=0, tiled=True)  6.63 us
    pallas_call x1, Pallas kernels, make_across(): pl.pallas_call(functools.partial(across_kernel, axes, flip), in_specs=[an...  5 us
    all_to_all x1, starting transfers between devices, read_beside(): lax.all_to_all(near, ('lo', 'tp'), split_axis=0, concat_axis=0, tiled=True)  3.56 us
  transfers between devices with their start and end apart: 16, of which 7 were waited for; matrix products, arithmetic and copies ran while one was open for 3% of the time, Pallas kernels for 0%

profile of v4, /device:TPU:0, one launch (start us, length us, event | category | flops | bytes accessed | tf_op | source)
XLA Modules:
  0.0 97.8 jit_solution(6239407525982962812)
XLA Ops:
  0.6 5.0 %across.1 = (bf16[512,128]{1,0:T(8,128)(2,1)}, bf16[512,128]{1,0:T(8,128)(2,1)}, bf16[512,128]{1,0:T(8,128)(2,1)}, bf16[512,128]{1,0:T(8,128)(2,1)}) custom-call(bf16[4,512,2048]{2,1,0:T(8,128)(2,1)} %tokens_ref.3, f32[1,2048]{1,0:T(1,128)} %bitcast.31, bf16[2048,256]{1,0:T(8,128)(2,1)} %key_ref.1, bf16[2048,256]{1,0:T(8,128)(2,1)} %value_ref.1), custom_call_target="tpu_custom_call" | custom-call | tf_op jit(solution)/shard_map/across/pallas_call | solution.py:191
  5.6 7.4 %all-to-all-start = ((f32[16,4,128]{2,1,0:T(4,128)}), f32[16,4,128]{2,1,0:T(4,128)S(1)}, u32[]{:S(2)}, u32[]{:S(2)}) async-start(f32[16,4,128]{2,1,0:T(4,128)} %bitcast.2), calls=%async_computation | async-start | bytes 65536 | tf_op jit(solution)/shard_map/all_to_all | solution.py:327
  13.1 6.6 %all-to-all-done.gate_ref = f32[16,4,128]{2,1,0:T(4,128)S(1)} async-done(((f32[16,4,128]{2,1,0:T(4,128)}), f32[16,4,128]{2,1,0:T(4,128)S(1)}, u32[]{:S(2)}, u32[]{:S(2)}) %all-to-all-start) | async-done | bytes 32800 | tf_op jit(solution)/shard_map/all_to_all | solution.py:327
  19.7 0.6 copy-done.4
  20.3 11.0 %rest.1 = (bf16[512,128]{1,0:T(8,128)(2,1)}, bf16[512,128]{1,0:T(8,128)(2,1)}, bf16[512,128]{1,0:T(8,128)(2,1)}, bf16[512,128]{1,0:T(8,128)(2,1)}, bf16[2,4,512,...) custom-call(bf16[4,512,2048]{2,1,0:T(8,128)(2,1)} %tokens_ref.3, f32[1,2048]{1,0:T(1,128)} %bitcast.32, ...), custom_call_target="tpu_custom_call" | custom-call | tf_op jit(solution)/shard_map/rest/pallas_call | solution.py:269
  31.3 0.0 copy-start.2
  31.3 0.0 copy-start.1
  31.3 0.0 copy-start
  31.3 0.4 collective-permute-start.8
  31.8 4.1 %collective-permute-done.8 = f32[16,8,128]{2,1,0:T(8,128)S(1)} collective-permute-done((f32[16,8,128]{2,1,0:T(8,128)}, f32[16,8,128]{2,1,0:T(8,128)S(1)}, u32[]{:S(2)}, u32[]{:S(2)}) %collective-permute-start.8) | collective-permute-done | bytes 65568 | tf_op jit(solution)/shard_map/ppermute | solution.py:323
  35.9 0.9 subtract_exponential_fusion.1
  36.7 0.2 copy.34
  36.9 0.2 copy.33
  37.1 0.2 copy.32
  37.2 1.0 multiply_add_fusion
  38.2 0.1 slice.69
  38.3 0.2 copy.35
  38.4 0.1 select_select_fusion
  38.6 0.1 collective-permute-start.9
  38.7 0.0 copy-done.3
  38.7 0.5 collective-permute-start.3
  39.2 2.0 %collective-permute-start.4 = (bf16[512,128]{1,0:T(8,128)(2,1)}, bf16[512,128]{1,0:T(8,128)(2,1)S(1)}, u32[]{:S(2)}, u32[]{:S(2)}) collective-permute-start(bf16[512,128]{1,0:T(8,128)(2,1)} %get-tuple-element.25), channel_id=1, source_target_pairs={{0,15},{1,14},{2,13},{3,12},{4,11},{5,10},{6,9},{7,8},{8,7},{9,6},... | collective-permute-start | bytes 393224 | tf_op jit(solution)/shard_map/ppermute | solution.py:323
  41.2 2.5 %collective-permute-start.5 = (bf16[512,128]{1,0:T(8,128)(2,1)}, bf16[512,128]{1,0:T(8,128)(2,1)S(1)}, u32[]{:S(2)}, u32[]{:S(2)}) collective-permute-start(bf16[512,128]{1,0:T(8,128)(2,1)} %get-tuple-element.26), channel_id=1, source_target_pairs={{0,14},{1,15},{2,12},{3,13},{4,10},{5,11},{6,8},{7,9},{8,6},{9,7},... | collective-permute-start | bytes 393224 | tf_op jit(solution)/shard_map/ppermute | solution.py:323
  43.7 1.9 %collective-permute-start.6 = (bf16[512,128]{1,0:T(8,128)(2,1)}, bf16[512,128]{1,0:T(8,128)(2,1)S(1)}, u32[]{:S(2)}, u32[]{:S(2)}) collective-permute-start(bf16[512,128]{1,0:T(8,128)(2,1)} %get-tuple-element.27), channel_id=1, source_target_pairs={{0,13},{1,12},{2,15},{3,14},{4,9},{5,8},{6,11},{7,10},{8,5},{9,4},... | collective-permute-start | bytes 393224 | tf_op jit(solution)/shard_map/ppermute | solution.py:323
  45.6 3.6 %all-to-all-start.1 = ((bf16[8,512,128]{2,1,0:T(8,128)(2,1)}), bf16[8,512,128]{2,1,0:T(8,128)(2,1)S(1)}, u32[]{:S(2)}, u32[]{:S(2)}) async-start(bf16[8,512,128]{2,1,0:T(8,128)(2,1)} %bitcast.24), calls=%async_computation.1 | async-start | bytes 2097152 | tf_op jit(solution)/shard_map/all_to_all | solution.py:336
  49.1 0.0 collective-permute-done.9
  49.1 0.0 copy-done.5
  49.2 1.6 %collective-permute-start.7 = (bf16[512,128]{1,0:T(8,128)(2,1)S(1)}, bf16[512,128]{1,0:T(8,128)(2,1)S(1)}, u32[]{:S(2)}, u32[]{:S(2)}) collective-permute-start(bf16[512,128]{1,0:T(8,128)(2,1)S(1)} %copy-done.5), channel_id=1, source_target_pairs={{0,12},{1,13},{2,14},{3,15},{4,8},{5,9},{6,10},{7,11},{8,4},{9,5},... | collective-permute-start | bytes 393224 | tf_op jit(solution)/shard_map/ppermute | solution.py:323
  50.8 0.1 fusion.2
  50.9 0.1 multiply_add_fusion.2
  51.0 0.2 slice_reduce_fusion.2
  51.1 0.1 select_select_fusion.2
  51.2 0.0 collective-permute-done.4
  51.2 10.3 %collective-permute-start.1 = (bf16[512,128]{1,0:T(8,128)(2,1)S(1)}, bf16[512,128]{1,0:T(8,128)(2,1)S(1)}, u32[]{:S(2)}, u32[]{:S(2)}) collective-permute-start(bf16[512,128]{1,0:T(8,128)(2,1)S(1)} %copy-done.2), channel_id=1, source_target_pairs={{0,10},{1,11},{2,8},{3,9},{4,14},{5,15},{6,12},{7,13},{8,2},{9,3},... | collective-permute-start | bytes 393224 | tf_op jit(solution)/shard_map/ppermute | solution.py:323
  61.5 0.0 collective-permute-done.5
  61.5 3.9 %collective-permute-start.2 = (bf16[512,128]{1,0:T(8,128)(2,1)S(1)}, bf16[512,128]{1,0:T(8,128)(2,1)S(1)}, u32[]{:S(2)}, u32[]{:S(2)}) collective-permute-start(bf16[512,128]{1,0:T(8,128)(2,1)S(1)} %copy-done.1), channel_id=1, source_target_pairs={{0,9},{1,8},{2,11},{3,10},{4,13},{5,12},{6,15},{7,14},{8,1},{9,0},... | collective-permute-start | bytes 393224 | tf_op jit(solution)/shard_map/ppermute | solution.py:323
  65.4 0.0 collective-permute-done.6
  65.4 11.5 %collective-permute-start = (bf16[512,128]{1,0:T(8,128)(2,1)S(1)}, bf16[512,128]{1,0:T(8,128)(2,1)S(1)}, u32[]{:S(2)}, u32[]{:S(2)}) collective-permute-start(bf16[512,128]{1,0:T(8,128)(2,1)S(1)} %copy-done), channel_id=1, source_target_pairs={{0,11},{1,10},{2,9},{3,8},{4,15},{5,14},{6,13},{7,12},{8,3},{9,2},... | collective-permute-start | bytes 393224 | tf_op jit(solution)/shard_map/ppermute | solution.py:323
  76.9 0.0 collective-permute-done.7
  76.9 3.4 %collective-permute-start.10 = (f32[8,8,128]{2,1,0:T(8,128)S(1)}, f32[8,8,128]{2,1,0:T(8,128)S(1)}, u32[]{:S(2)}, u32[]{:S(2)}) collective-permute-start(f32[8,8,128]{2,1,0:T(8,128)S(1)} %select_select_fusion.2), channel_id=1, source_target_pairs={{0,4},{1,5},{2,6},{3,7},{4,0},{5,1},{6,2},{7,3},{8,12},{9,13},{10,... | collective-permute-start | bytes 98312 | tf_op jit(solution)/shard_map/ppermute | solution.py:323
  80.4 0.0 collective-permute-done.3
  80.4 0.2 collective-permute-start.11
  80.6 5.9 %collective-permute-done.1 = bf16[512,128]{1,0:T(8,128)(2,1)S(1)} collective-permute-done((bf16[512,128]{1,0:T(8,128)(2,1)S(1)}, bf16[512,128]{1,0:T(8,128)(2,1)S(1)}, u32[]{:S(2)}, u32[]{:S(2)}) %collective-permute-start.1) | collective-permute-done | bytes 131104 | tf_op jit(solution)/shard_map/ppermute | solution.py:323
  86.5 1.0 %collective-permute-start.12 = (f32[8,8,128]{2,1,0:T(8,128)S(1)}, f32[8,8,128]{2,1,0:T(8,128)S(1)}, u32[]{:S(2)}, u32[]{:S(2)}) collective-permute-start(f32[8,8,128]{2,1,0:T(8,128)S(1)} %select_select_fusion.2), channel_id=1, source_target_pairs={{0,12},{1,13},{2,14},{3,15},{4,8},{5,9},{6,10},{7,11},{8,4},{9,5},... | collective-permute-start | bytes 98312 | tf_op jit(solution)/shard_map/ppermute | solution.py:323
  87.5 1.2 %collective-permute-done.2 = bf16[512,128]{1,0:T(8,128)(2,1)S(1)} collective-permute-done((bf16[512,128]{1,0:T(8,128)(2,1)S(1)}, bf16[512,128]{1,0:T(8,128)(2,1)S(1)}, u32[]{:S(2)}, u32[]{:S(2)}) %collective-permute-start.2) | collective-permute-done | bytes 131104 | tf_op jit(solution)/shard_map/ppermute | solution.py:323
  88.8 3.5 %collective-permute-done = bf16[512,128]{1,0:T(8,128)(2,1)S(1)} collective-permute-done((bf16[512,128]{1,0:T(8,128)(2,1)S(1)}, bf16[512,128]{1,0:T(8,128)(2,1)S(1)}, u32[]{:S(2)}, u32[]{:S(2)}) %collective-permute-start) | collective-permute-done | bytes 131104 | tf_op jit(solution)/shard_map/ppermute | solution.py:323
  92.3 0.1 broadcast_select_fusion.15
  92.3 0.0 collective-permute-done.10
  92.4 0.7 collective-permute-done.11
  93.1 0.0 collective-permute-done.12
  93.1 0.1 fusion.3
  93.2 0.1 multiply_add_fusion.1
  93.3 0.2 slice_reduce_fusion.1
  93.5 0.1 select_select_fusion.1
  93.6 0.2 slice_reduce_fusion
  93.7 0.1 broadcast_divide_fusion
  93.8 0.1 collective-permute-start.13
  93.9 0.8 fusion
  94.8 0.4 collective-permute-done.13
  95.1 0.1 broadcast_select_fusion.17
  95.2 0.7 pad_maximum_fusion
  95.9 0.0 all-to-all-done.1
  95.9 1.0 %constant_dynamic-update-slice_fusion = bf16[1,1,8192,128]{3,2,1,0:T(8,128)(2,1)} fusion(bf16[1,1,8192,128]{3,2,1,0:T(8,128)(2,1)} %fusion, bf16[1,1,4096,128]{3,2,1,0:T(8,128)(2,1)S(1)} %bitcast.23, s32[]{:T(128)S(6)} %select_n.132), kind=kLoop, calls=%fused_computation.46 | loop fusion | bytes 2097156 | tf_op jit(solution)/shard_map/dynamic_update_slice | solution.py:359
  97.0 0.8 fusion.1
  (10 shorter events, 0.1 us)
Async XLA Ops:
  5.6 14.1 %all-to-all-start = ((f32[16,4,128]{2,1,0:T(4,128)}), f32[16,4,128]{2,1,0:T(4,128)S(1)}, u32[]{:S(2)}, u32[]{:S(2)}) async-start(f32[16,4,128]{2,1,0:T(4,128)} %bitcast.2), calls=%async_computation | async-start | bytes 65536 | tf_op jit(solution)/shard_map/all_to_all | solution.py:327
  19.7 0.6 copy-start.4
  20.3 18.4 %copy-start.3 = (bf16[512,128]{1,0:T(8,128)(2,1)S(1)}, bf16[512,128]{1,0:T(8,128)(2,1)}, u32[]{:S(2)}) copy-start(bf16[512,128]{1,0:T(8,128)(2,1)} %get-tuple-element.17.refs_0_) | copy-start | bytes 393220
  31.3 17.8 %copy-start.5 = (bf16[512,128]{1,0:T(8,128)(2,1)S(1)}, bf16[512,128]{1,0:T(8,128)(2,1)}, u32[]{:S(2)}) copy-start(bf16[512,128]{1,0:T(8,128)(2,1)} %get-tuple-element.28) | copy-start | bytes 393220
  31.3 19.9 %copy-start.2 = (bf16[512,128]{1,0:T(8,128)(2,1)S(1)}, bf16[512,128]{1,0:T(8,128)(2,1)}, u32[]{:S(2)}) copy-start(bf16[512,128]{1,0:T(8,128)(2,1)} %get-tuple-element.21.refs_2_) | copy-start | bytes 393220
  31.3 30.2 %copy-start.1 = (bf16[512,128]{1,0:T(8,128)(2,1)S(1)}, bf16[512,128]{1,0:T(8,128)(2,1)}, u32[]{:S(2)}) copy-start(bf16[512,128]{1,0:T(8,128)(2,1)} %get-tuple-element.20.refs_1_) | copy-start | bytes 393220
  31.3 34.1 %copy-start = (bf16[512,128]{1,0:T(8,128)(2,1)S(1)}, bf16[512,128]{1,0:T(8,128)(2,1)}, u32[]{:S(2)}) copy-start(bf16[512,128]{1,0:T(8,128)(2,1)} %get-tuple-element.23.refs_3_) | copy-start | bytes 393220
  31.3 4.5 %collective-permute-start.8 = (f32[16,8,128]{2,1,0:T(8,128)}, f32[16,8,128]{2,1,0:T(8,128)S(1)}, u32[]{:S(2)}, u32[]{:S(2)}) collective-permute-start(f32[16,8,128]{2,1,0:T(8,128)} %get-tuple-element.29), channel_id=1, source_target_pairs={{0,2},{1,3},{2,0},{3,1},{4,6},{5,7},{6,4},{7,5},{8,10},{9,11},{10,... | collective-permute-start | bytes 196616 | tf_op jit(solution)/shard_map/ppermute | solution.py:323
  38.6 10.6 %collective-permute-start.9 = (f32[8,8,128]{2,1,0:T(8,128)S(1)}, f32[8,8,128]{2,1,0:T(8,128)S(1)}, u32[]{:S(2)}, u32[]{:S(2)}) collective-permute-start(f32[8,8,128]{2,1,0:T(8,128)S(1)} %get-tuple-element.51), channel_id=1, source_target_pairs={{0,1},{1,0},{2,3},{3,2},{4,5},{5,4},{6,7},{7,6},{8,9},{9,8},{10,11... | collective-permute-start | bytes 98312 | tf_op jit(solution)/shard_map/ppermute | solution.py:323
  38.7 41.7 %collective-permute-start.3 = (bf16[512,128]{1,0:T(8,128)(2,1)S(1)}, bf16[512,128]{1,0:T(8,128)(2,1)S(1)}, u32[]{:S(2)}, u32[]{:S(2)}) collective-permute-start(bf16[512,128]{1,0:T(8,128)(2,1)S(1)} %copy-done.3), channel_id=1, source_target_pairs={{0,8},{1,9},{2,10},{3,11},{4,12},{5,13},{6,14},{7,15},{8,0},{9,1},... | collective-permute-start | bytes 393224 | tf_op jit(solution)/shard_map/ppermute | solution.py:323
  39.2 12.0 %collective-permute-start.4 = (bf16[512,128]{1,0:T(8,128)(2,1)}, bf16[512,128]{1,0:T(8,128)(2,1)S(1)}, u32[]{:S(2)}, u32[]{:S(2)}) collective-permute-start(bf16[512,128]{1,0:T(8,128)(2,1)} %get-tuple-element.25), channel_id=1, source_target_pairs={{0,15},{1,14},{2,13},{3,12},{4,11},{5,10},{6,9},{7,8},{8,7},{9,6},... | collective-permute-start | bytes 393224 | tf_op jit(solution)/shard_map/ppermute | solution.py:323
  41.2 20.3 %collective-permute-start.5 = (bf16[512,128]{1,0:T(8,128)(2,1)}, bf16[512,128]{1,0:T(8,128)(2,1)S(1)}, u32[]{:S(2)}, u32[]{:S(2)}) collective-permute-start(bf16[512,128]{1,0:T(8,128)(2,1)} %get-tuple-element.26), channel_id=1, source_target_pairs={{0,14},{1,15},{2,12},{3,13},{4,10},{5,11},{6,8},{7,9},{8,6},{9,7},... | collective-permute-start | bytes 393224 | tf_op jit(solution)/shard_map/ppermute | solution.py:323
  43.7 21.8 %collective-permute-start.6 = (bf16[512,128]{1,0:T(8,128)(2,1)}, bf16[512,128]{1,0:T(8,128)(2,1)S(1)}, u32[]{:S(2)}, u32[]{:S(2)}) collective-permute-start(bf16[512,128]{1,0:T(8,128)(2,1)} %get-tuple-element.27), channel_id=1, source_target_pairs={{0,13},{1,12},{2,15},{3,14},{4,9},{5,8},{6,11},{7,10},{8,5},{9,4},... | collective-permute-start | bytes 393224 | tf_op jit(solution)/shard_map/ppermute | solution.py:323
  45.6 50.4 %all-to-all-start.1 = ((bf16[8,512,128]{2,1,0:T(8,128)(2,1)}), bf16[8,512,128]{2,1,0:T(8,128)(2,1)S(1)}, u32[]{:S(2)}, u32[]{:S(2)}) async-start(bf16[8,512,128]{2,1,0:T(8,128)(2,1)} %bitcast.24), calls=%async_computation.1 | async-start | bytes 2097152 | tf_op jit(solution)/shard_map/all_to_all | solution.py:336
  49.2 27.8 %collective-permute-start.7 = (bf16[512,128]{1,0:T(8,128)(2,1)S(1)}, bf16[512,128]{1,0:T(8,128)(2,1)S(1)}, u32[]{:S(2)}, u32[]{:S(2)}) collective-permute-start(bf16[512,128]{1,0:T(8,128)(2,1)S(1)} %copy-done.5), channel_id=1, source_target_pairs={{0,12},{1,13},{2,14},{3,15},{4,8},{5,9},{6,10},{7,11},{8,4},{9,5},... | collective-permute-start | bytes 393224 | tf_op jit(solution)/shard_map/ppermute | solution.py:323
  51.2 35.3 %collective-permute-start.1 = (bf16[512,128]{1,0:T(8,128)(2,1)S(1)}, bf16[512,128]{1,0:T(8,128)(2,1)S(1)}, u32[]{:S(2)}, u32[]{:S(2)}) collective-permute-start(bf16[512,128]{1,0:T(8,128)(2,1)S(1)} %copy-done.2), channel_id=1, source_target_pairs={{0,10},{1,11},{2,8},{3,9},{4,14},{5,15},{6,12},{7,13},{8,2},{9,3},... | collective-permute-start | bytes 393224 | tf_op jit(solution)/shard_map/ppermute | solution.py:323
  61.5 27.2 %collective-permute-start.2 = (bf16[512,128]{1,0:T(8,128)(2,1)S(1)}, bf16[512,128]{1,0:T(8,128)(2,1)S(1)}, u32[]{:S(2)}, u32[]{:S(2)}) collective-permute-start(bf16[512,128]{1,0:T(8,128)(2,1)S(1)} %copy-done.1), channel_id=1, source_target_pairs={{0,9},{1,8},{2,11},{3,10},{4,13},{5,12},{6,15},{7,14},{8,1},{9,0},... | collective-permute-start | bytes 393224 | tf_op jit(solution)/shard_map/ppermute | solution.py:323
  65.4 26.9 %collective-permute-start = (bf16[512,128]{1,0:T(8,128)(2,1)S(1)}, bf16[512,128]{1,0:T(8,128)(2,1)S(1)}, u32[]{:S(2)}, u32[]{:S(2)}) collective-permute-start(bf16[512,128]{1,0:T(8,128)(2,1)S(1)} %copy-done), channel_id=1, source_target_pairs={{0,11},{1,10},{2,9},{3,8},{4,15},{5,14},{6,13},{7,12},{8,3},{9,2},... | collective-permute-start | bytes 393224 | tf_op jit(solution)/shard_map/ppermute | solution.py:323
  76.9 15.4 %collective-permute-start.10 = (f32[8,8,128]{2,1,0:T(8,128)S(1)}, f32[8,8,128]{2,1,0:T(8,128)S(1)}, u32[]{:S(2)}, u32[]{:S(2)}) collective-permute-start(f32[8,8,128]{2,1,0:T(8,128)S(1)} %select_select_fusion.2), channel_id=1, source_target_pairs={{0,4},{1,5},{2,6},{3,7},{4,0},{5,1},{6,2},{7,3},{8,12},{9,13},{10,... | collective-permute-start | bytes 98312 | tf_op jit(solution)/shard_map/ppermute | solution.py:323
  80.4 12.7 %collective-permute-start.11 = (f32[8,8,128]{2,1,0:T(8,128)S(1)}, f32[8,8,128]{2,1,0:T(8,128)S(1)}, u32[]{:S(2)}, u32[]{:S(2)}) collective-permute-start(f32[8,8,128]{2,1,0:T(8,128)S(1)} %select_select_fusion.2), channel_id=1, source_target_pairs={{0,8},{1,9},{2,10},{3,11},{4,12},{5,13},{6,14},{7,15},{8,0},{9,1},... | collective-permute-start | bytes 98312 | tf_op jit(solution)/shard_map/ppermute | solution.py:323
  86.5 6.6 %collective-permute-start.12 = (f32[8,8,128]{2,1,0:T(8,128)S(1)}, f32[8,8,128]{2,1,0:T(8,128)S(1)}, u32[]{:S(2)}, u32[]{:S(2)}) collective-permute-start(f32[8,8,128]{2,1,0:T(8,128)S(1)} %select_select_fusion.2), channel_id=1, source_target_pairs={{0,12},{1,13},{2,14},{3,15},{4,8},{5,9},{6,10},{7,11},{8,4},{9,5},... | collective-permute-start | bytes 98312 | tf_op jit(solution)/shard_map/ppermute | solution.py:323
  93.8 1.3 %collective-permute-start.13 = (f32[8,8,128]{2,1,0:T(8,128)S(1)}, f32[8,8,128]{2,1,0:T(8,128)S(1)}, u32[]{:S(2)}, u32[]{:S(2)}) collective-permute-start(f32[8,8,128]{2,1,0:T(8,128)S(1)} %broadcast_divide_fusion), channel_id=1, source_target_pairs={{0,1},{1,0},{2,3},{3,2},{4,5},{5,4},{6,7},{7,6},{8,9},{9,8},{10,11... | collective-permute-start | bytes 98312 | tf_op jit(solution)/shard_map/ppermute | solution.py:323

commit v5 on v4

--- a/solution.py
+++ b/solution.py
@@ -346,6 +346,10 @@
         start = (plane ^ k) * heads * positions
         return lax.dynamic_update_slice(cache, jnp.concatenate(blocks), (start, 0))
 
+    def placed_alone(cache, block, k, j):
+        start = ((plane ^ k) * heads + (column ^ j)) * positions
+        return lax.dynamic_update_slice(cache, block, (start, 0))
+
     columns = [1 << bit for bit in reversed(range(1, heads.bit_length() - 1))]
     for j in columns:
         tile = merge([tile, swap(tile, 0, j)])
@@ -355,6 +359,8 @@
     tile = merge([tile, swap(jnp.where(odd, low, high), 0, 1)])
     others = [swap(tile, k, 0) for k in range(1, seqs)]
     cache = placed(cache, arrived_first, half)
+    for j, block in enumerate(arrived_second[:-1]):
+        cache = placed_alone(cache, block, half + 1, j)
     near_rows = arrived_near.reshape(half * heads * positions, 2 * HD)
     cache = lax.dynamic_update_slice(cache, near_rows, (near_first * heads * positions, 0))
     tile = merge([tile] + others)
@@ -362,7 +368,7 @@
     other = swap(tile, 0, 1)
     pair = [jnp.where(odd, other, tile), jnp.where(odd, tile, other)]
     first_read = jnp.concatenate(pair)[..., HD:]
-    cache = placed(cache, arrived_second, half + 1)
+    cache = placed_alone(cache, arrived_second[-1], half + 1, heads - 1)
     return cache.reshape(1, 1, rows, 2 * HD), first_read.reshape(seqs, query_heads, HD)
 
 

time: 98.2 us -> 94.8 us (0.965)
  starting transfers between devices: 50.3 us -> 36.9 us
  waiting for transfers between devices: 22.6 us -> 30.5 us
  local copies, waits for them, and re-layouts: 2.83 us -> 5.49 us
    ppermute x14, starting transfers between devices: 39.3 us -> 25.9 us  [swap(): return lax.ppermute(value, everyone, pairs)]
    ppermute x14, waiting for transfers between devices: 15.9 us -> 23.9 us  [swap(): return lax.ppermute(value, everyone, pairs)]
    dynamic_update_slice x0 -> x4, local copies, waits for them, and re-layouts: none -> 2.66 us  [placed_alone(): return lax.dynamic_update_slice(cache, block, (start, 0))]
  transfers between devices with their start and end apart: 16 -> 16, of which waited for: 7 -> 10; matrix products, arithmetic and copies ran while one was open for 3% -> 6% of each run, Pallas kernels for 0% -> 0%
where the time goes in v5:
time: 94.8 us; the launch traced here: 94.4 us
  starting transfers between devices  36.9 us (39%)
  waiting for transfers between devices  30.5 us (32%)
  Pallas kernels  16.3 us (17%)
  local copies, waits for them, and re-layouts  5.49 us (6%)
  other arithmetic  4.36 us (5%)
    ppermute x14, starting transfers between devices, swap(): return lax.ppermute(value, everyone, pairs)  25.9 us
    ppermute x14, waiting for transfers between devices, swap(): return lax.ppermute(value, everyone, pairs)  23.9 us
    pallas_call x1, Pallas kernels, make_rest(): pl.pallas_call(functools.partial(rest_kernel, axes, heads), grid=(near +...  11.3 us
    all_to_all x1, starting transfers between devices, read_beside(): lax.all_to_all(gates, everyone, split_axis=0, concat_axis=0, tiled=True)  7.43 us
    all_to_all x1, waiting for transfers between devices, read_beside(): lax.all_to_all(gates, everyone, split_axis=0, concat_axis=0, tiled=True)  6.63 us
    pallas_call x1, Pallas kernels, make_across(): pl.pallas_call(functools.partial(across_kernel, axes, flip), in_specs=[an...  5.01 us
    all_to_all x1, starting transfers between devices, read_beside(): lax.all_to_all(near, ('lo', 'tp'), split_axis=0, concat_axis=0, tiled=True)  3.56 us
    dynamic_update_slice x4, local copies, waits for them, and re-layouts, placed_alone(): return lax.dynamic_update_slice(cache, block, (start, 0))  2.66 us
  transfers between devices with their start and end apart: 16, of which 10 were waited for; matrix products, arithmetic and copies ran while one was open for 6% of the time, Pallas kernels for 0%

profile of v5, /device:TPU:0, one launch (start us, length us, event | category | flops | bytes accessed | tf_op | source)
XLA Modules:
  0.0 94.4 jit_solution(3176556514698363446)
XLA Ops:
  0.6 5.0 %across.1 = (bf16[512,128]{1,0:T(8,128)(2,1)}, bf16[512,128]{1,0:T(8,128)(2,1)}, bf16[512,128]{1,0:T(8,128)(2,1)}, bf16[512,128]{1,0:T(8,128)(2,1)}) custom-call(bf16[4,512,2048]{2,1,0:T(8,128)(2,1)} %tokens_ref.3, f32[1,2048]{1,0:T(1,128)} %bitcast.35, bf16[2048,256]{1,0:T(8,128)(2,1)} %key_ref.1, bf16[2048,256]{1,0:T(8,128)(2,1)} %value_ref.1), custom_call_target="tpu_custom_call" | custom-call | tf_op jit(solution)/shard_map/across/pallas_call | solution.py:191
  5.6 7.4 %all-to-all-start = ((f32[16,4,128]{2,1,0:T(4,128)}), f32[16,4,128]{2,1,0:T(4,128)S(1)}, u32[]{:S(2)}, u32[]{:S(2)}) async-start(f32[16,4,128]{2,1,0:T(4,128)} %bitcast.2), calls=%async_computation | async-start | bytes 65536 | tf_op jit(solution)/shard_map/all_to_all | solution.py:327
  13.1 6.6 %all-to-all-done.gate_ref = f32[16,4,128]{2,1,0:T(4,128)S(1)} async-done(((f32[16,4,128]{2,1,0:T(4,128)}), f32[16,4,128]{2,1,0:T(4,128)S(1)}, u32[]{:S(2)}, u32[]{:S(2)}) %all-to-all-start) | async-done | bytes 32800 | tf_op jit(solution)/shard_map/all_to_all | solution.py:327
  19.7 0.6 copy-done.4
  20.3 11.3 %rest.1 = (bf16[512,128]{1,0:T(8,128)(2,1)}, bf16[512,128]{1,0:T(8,128)(2,1)}, bf16[512,128]{1,0:T(8,128)(2,1)}, bf16[512,128]{1,0:T(8,128)(2,1)}, bf16[2,4,512,...) custom-call(bf16[4,512,2048]{2,1,0:T(8,128)(2,1)} %tokens_ref.3, f32[1,2048]{1,0:T(1,128)} %bitcast.36, ...), custom_call_target="tpu_custom_call" | custom-call | tf_op jit(solution)/shard_map/rest/pallas_call | solution.py:269
  31.6 0.0 copy-start.7
  31.6 0.4 collective-permute-start.8
  32.0 4.1 %collective-permute-done.8 = f32[16,8,128]{2,1,0:T(8,128)S(1)} collective-permute-done((f32[16,8,128]{2,1,0:T(8,128)}, f32[16,8,128]{2,1,0:T(8,128)S(1)}, u32[]{:S(2)}, u32[]{:S(2)}) %collective-permute-start.8) | collective-permute-done | bytes 65568 | tf_op jit(solution)/shard_map/ppermute | solution.py:323
  36.2 0.9 subtract_exponential_fusion.1
  37.0 0.2 copy.34
  37.2 0.2 copy.33
  37.4 0.2 copy.32
  37.5 1.0 %multiply_add_fusion = f32[16,8,128]{2,1,0:T(8,128)S(1)} fusion(f32[16,8,128]{2,1,0:T(8,128)S(1)} %collective-permute-done.8, f32[16,8,128]{2,1,0:T(8,128)} %get-tuple-element.29, f32[16,8]{1,0:T(8,128)S(1)} %bitcast.33, f32[16,8]{1,0:T(8,128)S(1)} %bitcast.34), kind=kLoop, calls=%fused_computation.16 | loop fusion | flops 49152 | bytes 197632 | tf_op jit(solution)/shard_map/add | solution.py:90
  38.5 0.1 slice.69
  38.6 0.2 copy.35
  38.7 0.1 select_select_fusion
  38.9 0.1 collective-permute-start.9
  39.0 0.4 collective-permute-start.3
  39.3 0.0 copy-done.2
  39.3 2.4 %collective-permute-start.1 = (bf16[512,128]{1,0:T(8,128)(2,1)S(1)}, bf16[512,128]{1,0:T(8,128)(2,1)S(1)}, u32[]{:S(2)}, u32[]{:S(2)}) collective-permute-start(bf16[512,128]{1,0:T(8,128)(2,1)S(1)} %copy-done.2), channel_id=1, source_target_pairs={{0,10},{1,11},{2,8},{3,9},{4,14},{5,15},{6,12},{7,13},{8,2},{9,3},... | collective-permute-start | bytes 393224 | tf_op jit(solution)/shard_map/ppermute | solution.py:323
  41.7 0.0 collective-permute-start.2
  41.8 0.0 copy-done
  41.8 3.7 %collective-permute-start = (bf16[512,128]{1,0:T(8,128)(2,1)S(1)}, bf16[512,128]{1,0:T(8,128)(2,1)S(1)}, u32[]{:S(2)}, u32[]{:S(2)}) collective-permute-start(bf16[512,128]{1,0:T(8,128)(2,1)S(1)} %copy-done), channel_id=1, source_target_pairs={{0,11},{1,10},{2,9},{3,8},{4,15},{5,14},{6,13},{7,12},{8,3},{9,2},... | collective-permute-start | bytes 393224 | tf_op jit(solution)/shard_map/ppermute | solution.py:323
  45.5 3.6 %all-to-all-start.1 = ((bf16[8,512,128]{2,1,0:T(8,128)(2,1)}), bf16[8,512,128]{2,1,0:T(8,128)(2,1)S(1)}, u32[]{:S(2)}, u32[]{:S(2)}) async-start(bf16[8,512,128]{2,1,0:T(8,128)(2,1)} %bitcast.28), calls=%async_computation.1 | async-start | bytes 2097152 | tf_op jit(solution)/shard_map/all_to_all | solution.py:336
  49.1 0.0 collective-permute-done.9
  49.1 1.7 %collective-permute-start.4 = (bf16[512,128]{1,0:T(8,128)(2,1)S(1)}, bf16[512,128]{1,0:T(8,128)(2,1)S(1)}, u32[]{:S(2)}, u32[]{:S(2)}) collective-permute-start(bf16[512,128]{1,0:T(8,128)(2,1)S(1)} %copy-done.8), channel_id=1, source_target_pairs={{0,12},{1,13},{2,14},{3,15},{4,8},{5,9},{6,10},{7,11},{8,4},{9,5},... | collective-permute-start | bytes 393224 | tf_op jit(solution)/shard_map/ppermute | solution.py:323
  50.8 0.1 fusion.1
  50.9 0.1 multiply_add_fusion.2
  51.0 0.2 slice_reduce_fusion.2
  51.2 0.1 select_select_fusion.2
  51.3 5.6 %collective-permute-done.3 = bf16[512,128]{1,0:T(8,128)(2,1)S(1)} collective-permute-done((bf16[512,128]{1,0:T(8,128)(2,1)S(1)}, bf16[512,128]{1,0:T(8,128)(2,1)S(1)}, u32[]{:S(2)}, u32[]{:S(2)}) %collective-permute-start.3) | collective-permute-done | bytes 131104 | tf_op jit(solution)/shard_map/ppermute | solution.py:323
  56.8 0.0 collective-permute-start.5
  56.8 2.9 %collective-permute-done.1 = bf16[512,128]{1,0:T(8,128)(2,1)S(1)} collective-permute-done((bf16[512,128]{1,0:T(8,128)(2,1)S(1)}, bf16[512,128]{1,0:T(8,128)(2,1)S(1)}, u32[]{:S(2)}, u32[]{:S(2)}) %collective-permute-start.1) | collective-permute-done | bytes 131104 | tf_op jit(solution)/shard_map/ppermute | solution.py:323
  59.7 2.1 %collective-permute-start.6 = (bf16[512,128]{1,0:T(8,128)(2,1)S(1)}, bf16[512,128]{1,0:T(8,128)(2,1)S(1)}, u32[]{:S(2)}, u32[]{:S(2)}) collective-permute-start(bf16[512,128]{1,0:T(8,128)(2,1)S(1)} %copy-done.6), channel_id=1, source_target_pairs={{0,14},{1,15},{2,12},{3,13},{4,10},{5,11},{6,8},{7,9},{8,6},{9,7},... | collective-permute-start | bytes 393224 | tf_op jit(solution)/shard_map/ppermute | solution.py:323
  61.9 0.5 collective-permute-done.2
  62.4 1.4 %collective-permute-start.7 = (bf16[512,128]{1,0:T(8,128)(2,1)S(1)}, bf16[512,128]{1,0:T(8,128)(2,1)S(1)}, u32[]{:S(2)}, u32[]{:S(2)}) collective-permute-start(bf16[512,128]{1,0:T(8,128)(2,1)S(1)} %copy-done.5), channel_id=1, source_target_pairs={{0,15},{1,14},{2,13},{3,12},{4,11},{5,10},{6,9},{7,8},{8,7},{9,6},... | collective-permute-start | bytes 393224 | tf_op jit(solution)/shard_map/ppermute | solution.py:323
  63.8 2.0 %collective-permute-done = bf16[512,128]{1,0:T(8,128)(2,1)S(1)} collective-permute-done((bf16[512,128]{1,0:T(8,128)(2,1)S(1)}, bf16[512,128]{1,0:T(8,128)(2,1)S(1)}, u32[]{:S(2)}, u32[]{:S(2)}) %collective-permute-start) | collective-permute-done | bytes 131104 | tf_op jit(solution)/shard_map/ppermute | solution.py:323
  65.8 0.0 collective-permute-start.10
  65.8 0.8 fusion
  66.7 1.9 %collective-permute-done.4 = bf16[512,128]{1,0:T(8,128)(2,1)S(1)} collective-permute-done((bf16[512,128]{1,0:T(8,128)(2,1)S(1)}, bf16[512,128]{1,0:T(8,128)(2,1)S(1)}, u32[]{:S(2)}, u32[]{:S(2)}) %collective-permute-start.4) | collective-permute-done | bytes 131104 | tf_op jit(solution)/shard_map/ppermute | solution.py:323
  68.6 11.1 %collective-permute-start.11 = (f32[8,8,128]{2,1,0:T(8,128)S(1)}, f32[8,8,128]{2,1,0:T(8,128)S(1)}, u32[]{:S(2)}, u32[]{:S(2)}) collective-permute-start(f32[8,8,128]{2,1,0:T(8,128)S(1)} %select_select_fusion.2), channel_id=1, source_target_pairs={{0,8},{1,9},{2,10},{3,11},{4,12},{5,13},{6,14},{7,15},{8,0},{9,1},... | collective-permute-start | bytes 98312 | tf_op jit(solution)/shard_map/ppermute | solution.py:323
  79.7 0.7 bitcast_dynamic-update-slice_fusion.3
  80.3 0.0 collective-permute-done.5
  80.3 2.5 %collective-permute-start.12 = (f32[8,8,128]{2,1,0:T(8,128)S(1)}, f32[8,8,128]{2,1,0:T(8,128)S(1)}, u32[]{:S(2)}, u32[]{:S(2)}) collective-permute-start(f32[8,8,128]{2,1,0:T(8,128)S(1)} %select_select_fusion.2), channel_id=1, source_target_pairs={{0,12},{1,13},{2,14},{3,15},{4,8},{5,9},{6,10},{7,11},{8,4},{9,5},... | collective-permute-start | bytes 98312 | tf_op jit(solution)/shard_map/ppermute | solution.py:323
  82.9 0.7 bitcast_dynamic-update-slice_fusion.2
  83.5 3.7 %collective-permute-done.10 = f32[8,8,128]{2,1,0:T(8,128)S(1)} collective-permute-done((f32[8,8,128]{2,1,0:T(8,128)S(1)}, f32[8,8,128]{2,1,0:T(8,128)S(1)}, u32[]{:S(2)}, u32[]{:S(2)}) %collective-permute-start.10) | collective-permute-done | bytes 32800 | tf_op jit(solution)/shard_map/ppermute | solution.py:323
  87.2 2.6 %collective-permute-done.11 = f32[8,8,128]{2,1,0:T(8,128)S(1)} collective-permute-done((f32[8,8,128]{2,1,0:T(8,128)S(1)}, f32[8,8,128]{2,1,0:T(8,128)S(1)}, u32[]{:S(2)}, u32[]{:S(2)}) %collective-permute-start.11) | collective-permute-done | bytes 32800 | tf_op jit(solution)/shard_map/ppermute | solution.py:323
  89.8 0.0 collective-permute-done.12
  89.8 0.1 fusion.2
  90.0 0.1 multiply_add_fusion.1
  90.1 0.2 slice_reduce_fusion.1
  90.2 0.1 select_select_fusion.1
  90.3 0.2 slice_reduce_fusion
  90.5 0.1 broadcast_divide_fusion
  90.6 0.1 collective-permute-start.13
  90.7 0.0 collective-permute-done.6
  90.7 0.7 bitcast_dynamic-update-slice_fusion.1
  91.3 0.5 collective-permute-done.13
  91.9 0.1 broadcast_select_fusion.9
  92.0 0.7 pad_maximum_fusion
  92.7 0.0 all-to-all-done.1
  92.7 1.0 %constant_dynamic-update-slice_fusion = bf16[1,1,8192,128]{3,2,1,0:T(8,128)(2,1)} fusion(bf16[1,1,8192,128]{3,2,1,0:T(8,128)(2,1)} %bitcast_dynamic-update-slice_fusion.1, bf16[1,1,4096,128]{3,2,1,0:T(8,128)(2,1)S(1)} %bitcast.27, s32[]{:T(128)S(6)} %select_n.112), kind=kLoop, calls=%fused_computation.40 | loop fusion | bytes 2097156 | tf_op jit(solution)/shard_map/dynamic_update_slice | solution.py:365
  93.7 0.0 collective-permute-done.7
  93.7 0.7 bitcast_dynamic-update-slice_fusion
  (18 shorter events, 0.1 us)
Async XLA Ops:
  5.6 14.1 %all-to-all-start = ((f32[16,4,128]{2,1,0:T(4,128)}), f32[16,4,128]{2,1,0:T(4,128)S(1)}, u32[]{:S(2)}, u32[]{:S(2)}) async-start(f32[16,4,128]{2,1,0:T(4,128)} %bitcast.2), calls=%async_computation | async-start | bytes 65536 | tf_op jit(solution)/shard_map/all_to_all | solution.py:327
  19.7 0.6 copy-start.4
  20.3 18.6 %copy-start.3 = (bf16[512,128]{1,0:T(8,128)(2,1)S(1)}, bf16[512,128]{1,0:T(8,128)(2,1)}, u32[]{:S(2)}) copy-start(bf16[512,128]{1,0:T(8,128)(2,1)} %get-tuple-element.17.refs_0_) | copy-start | bytes 393220
  20.3 19.0 %copy-start.2 = (bf16[512,128]{1,0:T(8,128)(2,1)S(1)}, bf16[512,128]{1,0:T(8,128)(2,1)}, u32[]{:S(2)}) copy-start(bf16[512,128]{1,0:T(8,128)(2,1)} %get-tuple-element.21.refs_2_) | copy-start | bytes 393220
  20.3 21.4 %copy-start.1 = (bf16[512,128]{1,0:T(8,128)(2,1)S(1)}, bf16[512,128]{1,0:T(8,128)(2,1)}, u32[]{:S(2)}) copy-start(bf16[512,128]{1,0:T(8,128)(2,1)} %get-tuple-element.20.refs_1_) | copy-start | bytes 393220
  20.3 21.5 %copy-start = (bf16[512,128]{1,0:T(8,128)(2,1)S(1)}, bf16[512,128]{1,0:T(8,128)(2,1)}, u32[]{:S(2)}) copy-start(bf16[512,128]{1,0:T(8,128)(2,1)} %get-tuple-element.23.refs_3_) | copy-start | bytes 393220
  31.6 17.5 %copy-start.8 = (bf16[512,128]{1,0:T(8,128)(2,1)S(1)}, bf16[512,128]{1,0:T(8,128)(2,1)}, u32[]{:S(2)}) copy-start(bf16[512,128]{1,0:T(8,128)(2,1)} %get-tuple-element.24) | copy-start | bytes 393220
  31.6 25.2 %copy-start.7 = (bf16[512,128]{1,0:T(8,128)(2,1)S(1)}, bf16[512,128]{1,0:T(8,128)(2,1)}, u32[]{:S(2)}) copy-start(bf16[512,128]{1,0:T(8,128)(2,1)} %get-tuple-element.25) | copy-start | bytes 393220
  31.6 28.1 %copy-start.6 = (bf16[512,128]{1,0:T(8,128)(2,1)S(1)}, bf16[512,128]{1,0:T(8,128)(2,1)}, u32[]{:S(2)}) copy-start(bf16[512,128]{1,0:T(8,128)(2,1)} %get-tuple-element.26) | copy-start | bytes 393220
  31.6 30.8 %copy-start.5 = (bf16[512,128]{1,0:T(8,128)(2,1)S(1)}, bf16[512,128]{1,0:T(8,128)(2,1)}, u32[]{:S(2)}) copy-start(bf16[512,128]{1,0:T(8,128)(2,1)} %get-tuple-element.28) | copy-start | bytes 393220
  31.6 4.5 %collective-permute-start.8 = (f32[16,8,128]{2,1,0:T(8,128)}, f32[16,8,128]{2,1,0:T(8,128)S(1)}, u32[]{:S(2)}, u32[]{:S(2)}) collective-permute-start(f32[16,8,128]{2,1,0:T(8,128)} %get-tuple-element.29), channel_id=1, source_target_pairs={{0,2},{1,3},{2,0},{3,1},{4,6},{5,7},{6,4},{7,5},{8,10},{9,11},{10,... | collective-permute-start | bytes 196616 | tf_op jit(solution)/shard_map/ppermute | solution.py:323
  38.9 10.2 %collective-permute-start.9 = (f32[8,8,128]{2,1,0:T(8,128)S(1)}, f32[8,8,128]{2,1,0:T(8,128)S(1)}, u32[]{:S(2)}, u32[]{:S(2)}) collective-permute-start(f32[8,8,128]{2,1,0:T(8,128)S(1)} %get-tuple-element.47), channel_id=1, source_target_pairs={{0,1},{1,0},{2,3},{3,2},{4,5},{5,4},{6,7},{7,6},{8,9},{9,8},{10,11... | collective-permute-start | bytes 98312 | tf_op jit(solution)/shard_map/ppermute | solution.py:323
  39.0 17.9 %collective-permute-start.3 = (bf16[512,128]{1,0:T(8,128)(2,1)S(1)}, bf16[512,128]{1,0:T(8,128)(2,1)S(1)}, u32[]{:S(2)}, u32[]{:S(2)}) collective-permute-start(bf16[512,128]{1,0:T(8,128)(2,1)S(1)} %copy-done.3), channel_id=1, source_target_pairs={{0,8},{1,9},{2,10},{3,11},{4,12},{5,13},{6,14},{7,15},{8,0},{9,1},... | collective-permute-start | bytes 393224 | tf_op jit(solution)/shard_map/ppermute | solution.py:323
  39.3 20.4 %collective-permute-start.1 = (bf16[512,128]{1,0:T(8,128)(2,1)S(1)}, bf16[512,128]{1,0:T(8,128)(2,1)S(1)}, u32[]{:S(2)}, u32[]{:S(2)}) collective-permute-start(bf16[512,128]{1,0:T(8,128)(2,1)S(1)} %copy-done.2), channel_id=1, source_target_pairs={{0,10},{1,11},{2,8},{3,9},{4,14},{5,15},{6,12},{7,13},{8,2},{9,3},... | collective-permute-start | bytes 393224 | tf_op jit(solution)/shard_map/ppermute | solution.py:323
  41.7 20.7 %collective-permute-start.2 = (bf16[512,128]{1,0:T(8,128)(2,1)S(1)}, bf16[512,128]{1,0:T(8,128)(2,1)S(1)}, u32[]{:S(2)}, u32[]{:S(2)}) collective-permute-start(bf16[512,128]{1,0:T(8,128)(2,1)S(1)} %copy-done.1), channel_id=1, source_target_pairs={{0,9},{1,8},{2,11},{3,10},{4,13},{5,12},{6,15},{7,14},{8,1},{9,0},... | collective-permute-start | bytes 393224 | tf_op jit(solution)/shard_map/ppermute | solution.py:323
  41.8 24.0 %collective-permute-start = (bf16[512,128]{1,0:T(8,128)(2,1)S(1)}, bf16[512,128]{1,0:T(8,128)(2,1)S(1)}, u32[]{:S(2)}, u32[]{:S(2)}) collective-permute-start(bf16[512,128]{1,0:T(8,128)(2,1)S(1)} %copy-done), channel_id=1, source_target_pairs={{0,11},{1,10},{2,9},{3,8},{4,15},{5,14},{6,13},{7,12},{8,3},{9,2},... | collective-permute-start | bytes 393224 | tf_op jit(solution)/shard_map/ppermute | solution.py:323
  45.5 47.2 %all-to-all-start.1 = ((bf16[8,512,128]{2,1,0:T(8,128)(2,1)}), bf16[8,512,128]{2,1,0:T(8,128)(2,1)S(1)}, u32[]{:S(2)}, u32[]{:S(2)}) async-start(bf16[8,512,128]{2,1,0:T(8,128)(2,1)} %bitcast.28), calls=%async_computation.1 | async-start | bytes 2097152 | tf_op jit(solution)/shard_map/all_to_all | solution.py:336
  49.1 19.5 %collective-permute-start.4 = (bf16[512,128]{1,0:T(8,128)(2,1)S(1)}, bf16[512,128]{1,0:T(8,128)(2,1)S(1)}, u32[]{:S(2)}, u32[]{:S(2)}) collective-permute-start(bf16[512,128]{1,0:T(8,128)(2,1)S(1)} %copy-done.8), channel_id=1, source_target_pairs={{0,12},{1,13},{2,14},{3,15},{4,8},{5,9},{6,10},{7,11},{8,4},{9,5},... | collective-permute-start | bytes 393224 | tf_op jit(solution)/shard_map/ppermute | solution.py:323
  56.8 23.5 %collective-permute-start.5 = (bf16[512,128]{1,0:T(8,128)(2,1)S(1)}, bf16[512,128]{1,0:T(8,128)(2,1)S(1)}, u32[]{:S(2)}, u32[]{:S(2)}) collective-permute-start(bf16[512,128]{1,0:T(8,128)(2,1)S(1)} %copy-done.7), channel_id=1, source_target_pairs={{0,13},{1,12},{2,15},{3,14},{4,9},{5,8},{6,11},{7,10},{8,5},{9,4},... | collective-permute-start | bytes 393224 | tf_op jit(solution)/shard_map/ppermute | solution.py:323
  59.7 30.9 %collective-permute-start.6 = (bf16[512,128]{1,0:T(8,128)(2,1)S(1)}, bf16[512,128]{1,0:T(8,128)(2,1)S(1)}, u32[]{:S(2)}, u32[]{:S(2)}) collective-permute-start(bf16[512,128]{1,0:T(8,128)(2,1)S(1)} %copy-done.6), channel_id=1, source_target_pairs={{0,14},{1,15},{2,12},{3,13},{4,10},{5,11},{6,8},{7,9},{8,6},{9,7},... | collective-permute-start | bytes 393224 | tf_op jit(solution)/shard_map/ppermute | solution.py:323
  62.4 31.3 %collective-permute-start.7 = (bf16[512,128]{1,0:T(8,128)(2,1)S(1)}, bf16[512,128]{1,0:T(8,128)(2,1)S(1)}, u32[]{:S(2)}, u32[]{:S(2)}) collective-permute-start(bf16[512,128]{1,0:T(8,128)(2,1)S(1)} %copy-done.5), channel_id=1, source_target_pairs={{0,15},{1,14},{2,13},{3,12},{4,11},{5,10},{6,9},{7,8},{8,7},{9,6},... | collective-permute-start | bytes 393224 | tf_op jit(solution)/shard_map/ppermute | solution.py:323
  65.8 21.4 %collective-permute-start.10 = (f32[8,8,128]{2,1,0:T(8,128)S(1)}, f32[8,8,128]{2,1,0:T(8,128)S(1)}, u32[]{:S(2)}, u32[]{:S(2)}) collective-permute-start(f32[8,8,128]{2,1,0:T(8,128)S(1)} %select_select_fusion.2), channel_id=1, source_target_pairs={{0,4},{1,5},{2,6},{3,7},{4,0},{5,1},{6,2},{7,3},{8,12},{9,13},{10,... | collective-permute-start | bytes 98312 | tf_op jit(solution)/shard_map/ppermute | solution.py:323
  68.6 21.2 %collective-permute-start.11 = (f32[8,8,128]{2,1,0:T(8,128)S(1)}, f32[8,8,128]{2,1,0:T(8,128)S(1)}, u32[]{:S(2)}, u32[]{:S(2)}) collective-permute-start(f32[8,8,128]{2,1,0:T(8,128)S(1)} %select_select_fusion.2), channel_id=1, source_target_pairs={{0,8},{1,9},{2,10},{3,11},{4,12},{5,13},{6,14},{7,15},{8,0},{9,1},... | collective-permute-start | bytes 98312 | tf_op jit(solution)/shard_map/ppermute | solution.py:323
  80.3 9.5 %collective-permute-start.12 = (f32[8,8,128]{2,1,0:T(8,128)S(1)}, f32[8,8,128]{2,1,0:T(8,128)S(1)}, u32[]{:S(2)}, u32[]{:S(2)}) collective-permute-start(f32[8,8,128]{2,1,0:T(8,128)S(1)} %select_select_fusion.2), channel_id=1, source_target_pairs={{0,12},{1,13},{2,14},{3,15},{4,8},{5,9},{6,10},{7,11},{8,4},{9,5},... | collective-permute-start | bytes 98312 | tf_op jit(solution)/shard_map/ppermute | solution.py:323
  90.6 1.3 %collective-permute-start.13 = (f32[8,8,128]{2,1,0:T(8,128)S(1)}, f32[8,8,128]{2,1,0:T(8,128)S(1)}, u32[]{:S(2)}, u32[]{:S(2)}) collective-permute-start(f32[8,8,128]{2,1,0:T(8,128)S(1)} %broadcast_divide_fusion), channel_id=1, source_target_pairs={{0,1},{1,0},{2,3},{3,2},{4,5},{5,4},{6,7},{7,6},{8,9},{9,8},{10,11... | collective-permute-start | bytes 98312 | tf_op jit(solution)/shard_map/ppermute | solution.py:323

commit v6 on v5

--- a/solution.py
+++ b/solution.py
@@ -232,9 +232,19 @@
 
 def rest_kernel(axes, heads, tokens_ref, gain_ref, key_ref, value_ref, query_ref, gate_ref, *refs):
     first_refs, refs = refs[:heads], refs[heads:]
-    second_refs, (near_ref, tile_ref, _, made_ref) = refs[:heads], refs[heads:]
+    second_refs, (near_ref, tile_ref, _, made_ref, first_ref, loads) = refs[:heads], refs[heads:]
     step = pl.program_id(0)
     plane, near_first, column, half = planes(axes)
+    copies = [
+        pltpu.make_async_copy(source, first_ref.at[j], loads.at[j])
+        for j, source in enumerate(first_refs)
+    ]
+
+    @pl.when(step == 0)
+    def _():
+        for copy in copies:
+            copy.start()
+
     made = heads_made(normalize(tokens_ref[0], gain_ref[...]), key_ref, value_ref)
     seq = jnp.where(step == 0, plane ^ (half + 1), near_first + step - 1)
     slots = [seq * heads + head for head in range(heads)]
@@ -246,8 +256,13 @@
             made_ref[head] = both
         for j in range(heads):
             second_refs[j][...] = made_ref[column ^ j]
+
+    @pl.when(step == pl.num_programs(0) - 1)
+    def _():
+        for copy in copies:
+            copy.wait()
         slots = [(plane ^ half) * heads + (column ^ j) for j in range(heads)]
-        read_sequence(slots, [ref[...] for ref in first_refs], query_ref, gate_ref, tile_ref)
+        read_sequence(slots, [first_ref[j] for j in range(heads)], query_ref, gate_ref, tile_ref)
 
     @pl.when(step > 0)
     def _():
@@ -277,14 +292,18 @@
             pl.BlockSpec(queries.shape, fixed(3)),
             pl.BlockSpec(gates.shape, fixed(3)),
         ]
-        + [pl.BlockSpec((positions, 2 * HD), fixed(2))] * heads,
+        + [pl.BlockSpec(memory_space=pl.ANY)] * heads,
         out_specs=[pl.BlockSpec((positions, 2 * HD), fixed(2))] * heads
         + [
             pl.BlockSpec((1, heads, positions, 2 * HD), lambda i: (jnp.maximum(i - 1, 0), 0, 0, 0)),
             pl.BlockSpec(tile_shape, fixed(3)),
             pl.BlockSpec(memory_space=pl.ANY),
         ],
-        scratch_shapes=[pltpu.VMEM((heads, positions, 2 * HD), BF16)],
+        scratch_shapes=[
+            pltpu.VMEM((heads, positions, 2 * HD), BF16),
+            pltpu.VMEM((heads, positions, 2 * HD), BF16),
+            pltpu.SemaphoreType.DMA((heads,)),
+        ],
         out_shape=[jax.ShapeDtypeStruct((positions, 2 * HD), BF16)] * heads
         + [
             jax.ShapeDtypeStruct((near, heads, positions, 2 * HD), BF16),

time: 94.8 us -> 94.4 us (level)
  no operation moved by 1% of the time
where the time goes in v6:
time: 94.4 us; the launch traced here: 94 us
  starting transfers between devices  36.7 us (39%)
  waiting for transfers between devices  30.8 us (33%)
  Pallas kernels  15.8 us (17%)
  local copies, waits for them, and re-layouts  5.49 us (6%)
  other arithmetic  4.36 us (5%)
    ppermute x14, starting transfers between devices, swap(): return lax.ppermute(value, everyone, pairs)  25.8 us
    ppermute x14, waiting for transfers between devices, swap(): return lax.ppermute(value, everyone, pairs)  24.1 us
    pallas_call x1, Pallas kernels, make_rest(): pl.pallas_call(functools.partial(rest_kernel, axes, heads), grid=(near +...  10.8 us
    all_to_all x1, starting transfers between devices, read_beside(): lax.all_to_all(gates, everyone, split_axis=0, concat_axis=0, tiled=True)  7.43 us
    all_to_all x1, waiting for transfers between devices, read_beside(): lax.all_to_all(gates, everyone, split_axis=0, concat_axis=0, tiled=True)  6.63 us
    pallas_call x1, Pallas kernels, make_across(): pl.pallas_call(functools.partial(across_kernel, axes, flip), in_specs=[an...  5.01 us
    all_to_all x1, starting transfers between devices, read_beside(): lax.all_to_all(near, ('lo', 'tp'), split_axis=0, concat_axis=0, tiled=True)  3.56 us
    dynamic_update_slice x4, local copies, waits for them, and re-layouts, placed_alone(): return lax.dynamic_update_slice(cache, block, (start, 0))  2.66 us
  transfers between devices with their start and end apart: 16, of which 10 were waited for; matrix products, arithmetic and copies ran while one was open for 6% of the time, Pallas kernels for 0%

profile of v6, /device:TPU:0, one launch (start us, length us, event | category | flops | bytes accessed | tf_op | source)
XLA Modules:
  0.0 94.0 jit_solution(988792720468542969)
XLA Ops:
  0.6 5.0 %across.1 = (bf16[512,128]{1,0:T(8,128)(2,1)}, bf16[512,128]{1,0:T(8,128)(2,1)}, bf16[512,128]{1,0:T(8,128)(2,1)}, bf16[512,128]{1,0:T(8,128)(2,1)}) custom-call(bf16[4,512,2048]{2,1,0:T(8,128)(2,1)} %tokens_ref.3, f32[1,2048]{1,0:T(1,128)} %bitcast.35, bf16[2048,256]{1,0:T(8,128)(2,1)} %key_ref.1, bf16[2048,256]{1,0:T(8,128)(2,1)} %value_ref.1), custom_call_target="tpu_custom_call" | custom-call | tf_op jit(solution)/shard_map/across/pallas_call | solution.py:191
  5.6 7.4 %all-to-all-start = ((f32[16,4,128]{2,1,0:T(4,128)}), f32[16,4,128]{2,1,0:T(4,128)S(1)}, u32[]{:S(2)}, u32[]{:S(2)}) async-start(f32[16,4,128]{2,1,0:T(4,128)} %bitcast.2), calls=%async_computation | async-start | bytes 65536 | tf_op jit(solution)/shard_map/all_to_all | solution.py:346
  13.1 6.6 %all-to-all-done.gate_ref = f32[16,4,128]{2,1,0:T(4,128)S(1)} async-done(((f32[16,4,128]{2,1,0:T(4,128)}), f32[16,4,128]{2,1,0:T(4,128)S(1)}, u32[]{:S(2)}, u32[]{:S(2)}) %all-to-all-start) | async-done | bytes 32800 | tf_op jit(solution)/shard_map/all_to_all | solution.py:346
  19.7 0.6 copy-done.4
  20.3 10.8 %rest.1 = (bf16[512,128]{1,0:T(8,128)(2,1)}, bf16[512,128]{1,0:T(8,128)(2,1)}, bf16[512,128]{1,0:T(8,128)(2,1)}, bf16[512,128]{1,0:T(8,128)(2,1)}, bf16[2,4,512,...) custom-call(bf16[4,512,2048]{2,1,0:T(8,128)(2,1)} %tokens_ref.3, f32[1,2048]{1,0:T(1,128)} %bitcast.36, ...), custom_call_target="tpu_custom_call" | custom-call | tf_op jit(solution)/shard_map/rest/pallas_call | solution.py:284
  31.1 0.0 copy-start.8
  31.1 0.0 copy-start.7
  31.1 0.4 collective-permute-start.8
  31.6 4.1 %collective-permute-done.8 = f32[16,8,128]{2,1,0:T(8,128)S(1)} collective-permute-done((f32[16,8,128]{2,1,0:T(8,128)}, f32[16,8,128]{2,1,0:T(8,128)S(1)}, u32[]{:S(2)}, u32[]{:S(2)}) %collective-permute-start.8) | collective-permute-done | bytes 65568 | tf_op jit(solution)/shard_map/ppermute | solution.py:342
  35.7 0.9 subtract_exponential_fusion.1
  36.5 0.2 copy.34
  36.7 0.2 copy.33
  36.9 0.2 copy.32
  37.1 1.0 %multiply_add_fusion = f32[16,8,128]{2,1,0:T(8,128)S(1)} fusion(f32[16,8,128]{2,1,0:T(8,128)S(1)} %collective-permute-done.8, f32[16,8,128]{2,1,0:T(8,128)} %get-tuple-element.29, f32[16,8]{1,0:T(8,128)S(1)} %bitcast.33, f32[16,8]{1,0:T(8,128)S(1)} %bitcast.34), kind=kLoop, calls=%fused_computation.16 | loop fusion | flops 49152 | bytes 197632 | tf_op jit(solution)/shard_map/add | solution.py:90
  38.0 0.1 slice.69
  38.1 0.2 copy.35
  38.3 0.1 select_select_fusion
  38.4 0.1 collective-permute-start.9
  38.5 0.5 collective-permute-start.3
  39.0 2.3 %collective-permute-start.1 = (bf16[512,128]{1,0:T(8,128)(2,1)S(1)}, bf16[512,128]{1,0:T(8,128)(2,1)S(1)}, u32[]{:S(2)}, u32[]{:S(2)}) collective-permute-start(bf16[512,128]{1,0:T(8,128)(2,1)S(1)} %copy-done.2), channel_id=1, source_target_pairs={{0,10},{1,11},{2,8},{3,9},{4,14},{5,15},{6,12},{7,13},{8,2},{9,3},... | collective-permute-start | bytes 393224 | tf_op jit(solution)/shard_map/ppermute | solution.py:342
  41.3 0.0 copy-done.1
  41.3 0.1 collective-permute-start.2
  41.4 3.6 %collective-permute-start = (bf16[512,128]{1,0:T(8,128)(2,1)S(1)}, bf16[512,128]{1,0:T(8,128)(2,1)S(1)}, u32[]{:S(2)}, u32[]{:S(2)}) collective-permute-start(bf16[512,128]{1,0:T(8,128)(2,1)S(1)} %copy-done), channel_id=1, source_target_pairs={{0,11},{1,10},{2,9},{3,8},{4,15},{5,14},{6,13},{7,12},{8,3},{9,2},... | collective-permute-start | bytes 393224 | tf_op jit(solution)/shard_map/ppermute | solution.py:342
  45.0 3.6 %all-to-all-start.1 = ((bf16[8,512,128]{2,1,0:T(8,128)(2,1)}), bf16[8,512,128]{2,1,0:T(8,128)(2,1)S(1)}, u32[]{:S(2)}, u32[]{:S(2)}) async-start(bf16[8,512,128]{2,1,0:T(8,128)(2,1)} %bitcast.28), calls=%async_computation.1 | async-start | bytes 2097152 | tf_op jit(solution)/shard_map/all_to_all | solution.py:355
  48.6 0.0 collective-permute-done.9
  48.6 1.8 %collective-permute-start.4 = (bf16[512,128]{1,0:T(8,128)(2,1)S(1)}, bf16[512,128]{1,0:T(8,128)(2,1)S(1)}, u32[]{:S(2)}, u32[]{:S(2)}) collective-permute-start(bf16[512,128]{1,0:T(8,128)(2,1)S(1)} %copy-done.8), channel_id=1, source_target_pairs={{0,12},{1,13},{2,14},{3,15},{4,8},{5,9},{6,10},{7,11},{8,4},{9,5},... | collective-permute-start | bytes 393224 | tf_op jit(solution)/shard_map/ppermute | solution.py:342
  50.5 0.1 fusion.1
  50.6 0.1 multiply_add_fusion.2
  50.6 0.2 slice_reduce_fusion.2
  50.8 0.1 select_select_fusion.2
  50.9 5.6 %collective-permute-done.3 = bf16[512,128]{1,0:T(8,128)(2,1)S(1)} collective-permute-done((bf16[512,128]{1,0:T(8,128)(2,1)S(1)}, bf16[512,128]{1,0:T(8,128)(2,1)S(1)}, u32[]{:S(2)}, u32[]{:S(2)}) %collective-permute-start.3) | collective-permute-done | bytes 131104 | tf_op jit(solution)/shard_map/ppermute | solution.py:342
  56.5 0.0 collective-permute-start.5
  56.5 2.9 %collective-permute-done.1 = bf16[512,128]{1,0:T(8,128)(2,1)S(1)} collective-permute-done((bf16[512,128]{1,0:T(8,128)(2,1)S(1)}, bf16[512,128]{1,0:T(8,128)(2,1)S(1)}, u32[]{:S(2)}, u32[]{:S(2)}) %collective-permute-start.1) | collective-permute-done | bytes 131104 | tf_op jit(solution)/shard_map/ppermute | solution.py:342
  59.4 2.0 %collective-permute-start.6 = (bf16[512,128]{1,0:T(8,128)(2,1)S(1)}, bf16[512,128]{1,0:T(8,128)(2,1)S(1)}, u32[]{:S(2)}, u32[]{:S(2)}) collective-permute-start(bf16[512,128]{1,0:T(8,128)(2,1)S(1)} %copy-done.6), channel_id=1, source_target_pairs={{0,14},{1,15},{2,12},{3,13},{4,10},{5,11},{6,8},{7,9},{8,6},{9,7},... | collective-permute-start | bytes 393224 | tf_op jit(solution)/shard_map/ppermute | solution.py:342
  61.4 0.6 collective-permute-done.2
  62.0 1.2 %collective-permute-start.7 = (bf16[512,128]{1,0:T(8,128)(2,1)S(1)}, bf16[512,128]{1,0:T(8,128)(2,1)S(1)}, u32[]{:S(2)}, u32[]{:S(2)}) collective-permute-start(bf16[512,128]{1,0:T(8,128)(2,1)S(1)} %copy-done.5), channel_id=1, source_target_pairs={{0,15},{1,14},{2,13},{3,12},{4,11},{5,10},{6,9},{7,8},{8,7},{9,6},... | collective-permute-start | bytes 393224 | tf_op jit(solution)/shard_map/ppermute | solution.py:342
  63.2 1.9 %collective-permute-done = bf16[512,128]{1,0:T(8,128)(2,1)S(1)} collective-permute-done((bf16[512,128]{1,0:T(8,128)(2,1)S(1)}, bf16[512,128]{1,0:T(8,128)(2,1)S(1)}, u32[]{:S(2)}, u32[]{:S(2)}) %collective-permute-start) | collective-permute-done | bytes 131104 | tf_op jit(solution)/shard_map/ppermute | solution.py:342
  65.1 0.0 collective-permute-start.10
  65.2 0.8 fusion
  66.0 2.2 %collective-permute-done.4 = bf16[512,128]{1,0:T(8,128)(2,1)S(1)} collective-permute-done((bf16[512,128]{1,0:T(8,128)(2,1)S(1)}, bf16[512,128]{1,0:T(8,128)(2,1)S(1)}, u32[]{:S(2)}, u32[]{:S(2)}) %collective-permute-start.4) | collective-permute-done | bytes 131104 | tf_op jit(solution)/shard_map/ppermute | solution.py:342
  68.2 11.0 %collective-permute-start.11 = (f32[8,8,128]{2,1,0:T(8,128)S(1)}, f32[8,8,128]{2,1,0:T(8,128)S(1)}, u32[]{:S(2)}, u32[]{:S(2)}) collective-permute-start(f32[8,8,128]{2,1,0:T(8,128)S(1)} %select_select_fusion.2), channel_id=1, source_target_pairs={{0,8},{1,9},{2,10},{3,11},{4,12},{5,13},{6,14},{7,15},{8,0},{9,1},... | collective-permute-start | bytes 98312 | tf_op jit(solution)/shard_map/ppermute | solution.py:342
  79.2 0.7 bitcast_dynamic-update-slice_fusion.3
  79.9 0.0 collective-permute-done.5
  79.9 2.6 %collective-permute-start.12 = (f32[8,8,128]{2,1,0:T(8,128)S(1)}, f32[8,8,128]{2,1,0:T(8,128)S(1)}, u32[]{:S(2)}, u32[]{:S(2)}) collective-permute-start(f32[8,8,128]{2,1,0:T(8,128)S(1)} %select_select_fusion.2), channel_id=1, source_target_pairs={{0,12},{1,13},{2,14},{3,15},{4,8},{5,9},{6,10},{7,11},{8,4},{9,5},... | collective-permute-start | bytes 98312 | tf_op jit(solution)/shard_map/ppermute | solution.py:342
  82.5 0.7 bitcast_dynamic-update-slice_fusion.2
  83.2 3.6 %collective-permute-done.10 = f32[8,8,128]{2,1,0:T(8,128)S(1)} collective-permute-done((f32[8,8,128]{2,1,0:T(8,128)S(1)}, f32[8,8,128]{2,1,0:T(8,128)S(1)}, u32[]{:S(2)}, u32[]{:S(2)}) %collective-permute-start.10) | collective-permute-done | bytes 32800 | tf_op jit(solution)/shard_map/ppermute | solution.py:342
  86.8 2.7 %collective-permute-done.11 = f32[8,8,128]{2,1,0:T(8,128)S(1)} collective-permute-done((f32[8,8,128]{2,1,0:T(8,128)S(1)}, f32[8,8,128]{2,1,0:T(8,128)S(1)}, u32[]{:S(2)}, u32[]{:S(2)}) %collective-permute-start.11) | collective-permute-done | bytes 32800 | tf_op jit(solution)/shard_map/ppermute | solution.py:342
  89.5 0.0 collective-permute-done.12
  89.5 0.1 fusion.2
  89.6 0.1 multiply_add_fusion.1
  89.7 0.2 slice_reduce_fusion.1
  89.9 0.1 select_select_fusion.1
  90.0 0.2 slice_reduce_fusion
  90.1 0.1 broadcast_divide_fusion
  90.2 0.1 collective-permute-start.13
  90.3 0.0 collective-permute-done.6
  90.3 0.7 bitcast_dynamic-update-slice_fusion.1
  91.0 0.5 collective-permute-done.13
  91.5 0.1 broadcast_select_fusion.9
  91.6 0.7 pad_maximum_fusion
  92.3 0.0 all-to-all-done.1
  92.3 1.0 %constant_dynamic-update-slice_fusion = bf16[1,1,8192,128]{3,2,1,0:T(8,128)(2,1)} fusion(bf16[1,1,8192,128]{3,2,1,0:T(8,128)(2,1)} %bitcast_dynamic-update-slice_fusion.1, bf16[1,1,4096,128]{3,2,1,0:T(8,128)(2,1)S(1)} %bitcast.27, s32[]{:T(128)S(6)} %select_n.112), kind=kLoop, calls=%fused_computation.40 | loop fusion | bytes 2097156 | tf_op jit(solution)/shard_map/dynamic_update_slice | solution.py:384
  93.3 0.0 collective-permute-done.7
  93.3 0.7 bitcast_dynamic-update-slice_fusion
  (18 shorter events, 0.1 us)
Async XLA Ops:
  5.6 14.1 %all-to-all-start = ((f32[16,4,128]{2,1,0:T(4,128)}), f32[16,4,128]{2,1,0:T(4,128)S(1)}, u32[]{:S(2)}, u32[]{:S(2)}) async-start(f32[16,4,128]{2,1,0:T(4,128)} %bitcast.2), calls=%async_computation | async-start | bytes 65536 | tf_op jit(solution)/shard_map/all_to_all | solution.py:346
  19.7 0.6 copy-start.4
  20.3 18.2 %copy-start.3 = (bf16[512,128]{1,0:T(8,128)(2,1)S(1)}, bf16[512,128]{1,0:T(8,128)(2,1)}, u32[]{:S(2)}) copy-start(bf16[512,128]{1,0:T(8,128)(2,1)} %get-tuple-element.17.refs_0_) | copy-start | bytes 393220
  20.3 18.6 %copy-start.2 = (bf16[512,128]{1,0:T(8,128)(2,1)S(1)}, bf16[512,128]{1,0:T(8,128)(2,1)}, u32[]{:S(2)}) copy-start(bf16[512,128]{1,0:T(8,128)(2,1)} %get-tuple-element.21.refs_2_) | copy-start | bytes 393220
  20.3 21.0 %copy-start.1 = (bf16[512,128]{1,0:T(8,128)(2,1)S(1)}, bf16[512,128]{1,0:T(8,128)(2,1)}, u32[]{:S(2)}) copy-start(bf16[512,128]{1,0:T(8,128)(2,1)} %get-tuple-element.20.refs_1_) | copy-start | bytes 393220
  20.3 21.1 %copy-start = (bf16[512,128]{1,0:T(8,128)(2,1)S(1)}, bf16[512,128]{1,0:T(8,128)(2,1)}, u32[]{:S(2)}) copy-start(bf16[512,128]{1,0:T(8,128)(2,1)} %get-tuple-element.23.refs_3_) | copy-start | bytes 393220
  31.1 17.5 %copy-start.8 = (bf16[512,128]{1,0:T(8,128)(2,1)S(1)}, bf16[512,128]{1,0:T(8,128)(2,1)}, u32[]{:S(2)}) copy-start(bf16[512,128]{1,0:T(8,128)(2,1)} %get-tuple-element.24) | copy-start | bytes 393220
  31.1 25.3 %copy-start.7 = (bf16[512,128]{1,0:T(8,128)(2,1)S(1)}, bf16[512,128]{1,0:T(8,128)(2,1)}, u32[]{:S(2)}) copy-start(bf16[512,128]{1,0:T(8,128)(2,1)} %get-tuple-element.25) | copy-start | bytes 393220
  31.1 28.3 %copy-start.6 = (bf16[512,128]{1,0:T(8,128)(2,1)S(1)}, bf16[512,128]{1,0:T(8,128)(2,1)}, u32[]{:S(2)}) copy-start(bf16[512,128]{1,0:T(8,128)(2,1)} %get-tuple-element.26) | copy-start | bytes 393220
  31.1 30.9 %copy-start.5 = (bf16[512,128]{1,0:T(8,128)(2,1)S(1)}, bf16[512,128]{1,0:T(8,128)(2,1)}, u32[]{:S(2)}) copy-start(bf16[512,128]{1,0:T(8,128)(2,1)} %get-tuple-element.28) | copy-start | bytes 393220
  31.1 4.5 %collective-permute-start.8 = (f32[16,8,128]{2,1,0:T(8,128)}, f32[16,8,128]{2,1,0:T(8,128)S(1)}, u32[]{:S(2)}, u32[]{:S(2)}) collective-permute-start(f32[16,8,128]{2,1,0:T(8,128)} %get-tuple-element.29), channel_id=1, source_target_pairs={{0,2},{1,3},{2,0},{3,1},{4,6},{5,7},{6,4},{7,5},{8,10},{9,11},{10,... | collective-permute-start | bytes 196616 | tf_op jit(solution)/shard_map/ppermute | solution.py:342
  38.4 10.2 %collective-permute-start.9 = (f32[8,8,128]{2,1,0:T(8,128)S(1)}, f32[8,8,128]{2,1,0:T(8,128)S(1)}, u32[]{:S(2)}, u32[]{:S(2)}) collective-permute-start(f32[8,8,128]{2,1,0:T(8,128)S(1)} %get-tuple-element.47), channel_id=1, source_target_pairs={{0,1},{1,0},{2,3},{3,2},{4,5},{5,4},{6,7},{7,6},{8,9},{9,8},{10,11... | collective-permute-start | bytes 98312 | tf_op jit(solution)/shard_map/ppermute | solution.py:342
  38.5 18.0 %collective-permute-start.3 = (bf16[512,128]{1,0:T(8,128)(2,1)S(1)}, bf16[512,128]{1,0:T(8,128)(2,1)S(1)}, u32[]{:S(2)}, u32[]{:S(2)}) collective-permute-start(bf16[512,128]{1,0:T(8,128)(2,1)S(1)} %copy-done.3), channel_id=1, source_target_pairs={{0,8},{1,9},{2,10},{3,11},{4,12},{5,13},{6,14},{7,15},{8,0},{9,1},... | collective-permute-start | bytes 393224 | tf_op jit(solution)/shard_map/ppermute | solution.py:342
  39.0 20.4 %collective-permute-start.1 = (bf16[512,128]{1,0:T(8,128)(2,1)S(1)}, bf16[512,128]{1,0:T(8,128)(2,1)S(1)}, u32[]{:S(2)}, u32[]{:S(2)}) collective-permute-start(bf16[512,128]{1,0:T(8,128)(2,1)S(1)} %copy-done.2), channel_id=1, source_target_pairs={{0,10},{1,11},{2,8},{3,9},{4,14},{5,15},{6,12},{7,13},{8,2},{9,3},... | collective-permute-start | bytes 393224 | tf_op jit(solution)/shard_map/ppermute | solution.py:342
  41.3 20.7 %collective-permute-start.2 = (bf16[512,128]{1,0:T(8,128)(2,1)S(1)}, bf16[512,128]{1,0:T(8,128)(2,1)S(1)}, u32[]{:S(2)}, u32[]{:S(2)}) collective-permute-start(bf16[512,128]{1,0:T(8,128)(2,1)S(1)} %copy-done.1), channel_id=1, source_target_pairs={{0,9},{1,8},{2,11},{3,10},{4,13},{5,12},{6,15},{7,14},{8,1},{9,0},... | collective-permute-start | bytes 393224 | tf_op jit(solution)/shard_map/ppermute | solution.py:342
  41.4 23.7 %collective-permute-start = (bf16[512,128]{1,0:T(8,128)(2,1)S(1)}, bf16[512,128]{1,0:T(8,128)(2,1)S(1)}, u32[]{:S(2)}, u32[]{:S(2)}) collective-permute-start(bf16[512,128]{1,0:T(8,128)(2,1)S(1)} %copy-done), channel_id=1, source_target_pairs={{0,11},{1,10},{2,9},{3,8},{4,15},{5,14},{6,13},{7,12},{8,3},{9,2},... | collective-permute-start | bytes 393224 | tf_op jit(solution)/shard_map/ppermute | solution.py:342
  45.0 47.3 %all-to-all-start.1 = ((bf16[8,512,128]{2,1,0:T(8,128)(2,1)}), bf16[8,512,128]{2,1,0:T(8,128)(2,1)S(1)}, u32[]{:S(2)}, u32[]{:S(2)}) async-start(bf16[8,512,128]{2,1,0:T(8,128)(2,1)} %bitcast.28), calls=%async_computation.1 | async-start | bytes 2097152 | tf_op jit(solution)/shard_map/all_to_all | solution.py:355
  48.6 19.6 %collective-permute-start.4 = (bf16[512,128]{1,0:T(8,128)(2,1)S(1)}, bf16[512,128]{1,0:T(8,128)(2,1)S(1)}, u32[]{:S(2)}, u32[]{:S(2)}) collective-permute-start(bf16[512,128]{1,0:T(8,128)(2,1)S(1)} %copy-done.8), channel_id=1, source_target_pairs={{0,12},{1,13},{2,14},{3,15},{4,8},{5,9},{6,10},{7,11},{8,4},{9,5},... | collective-permute-start | bytes 393224 | tf_op jit(solution)/shard_map/ppermute | solution.py:342
  56.5 23.4 %collective-permute-start.5 = (bf16[512,128]{1,0:T(8,128)(2,1)S(1)}, bf16[512,128]{1,0:T(8,128)(2,1)S(1)}, u32[]{:S(2)}, u32[]{:S(2)}) collective-permute-start(bf16[512,128]{1,0:T(8,128)(2,1)S(1)} %copy-done.7), channel_id=1, source_target_pairs={{0,13},{1,12},{2,15},{3,14},{4,9},{5,8},{6,11},{7,10},{8,5},{9,4},... | collective-permute-start | bytes 393224 | tf_op jit(solution)/shard_map/ppermute | solution.py:342
  59.4 30.9 %collective-permute-start.6 = (bf16[512,128]{1,0:T(8,128)(2,1)S(1)}, bf16[512,128]{1,0:T(8,128)(2,1)S(1)}, u32[]{:S(2)}, u32[]{:S(2)}) collective-permute-start(bf16[512,128]{1,0:T(8,128)(2,1)S(1)} %copy-done.6), channel_id=1, source_target_pairs={{0,14},{1,15},{2,12},{3,13},{4,10},{5,11},{6,8},{7,9},{8,6},{9,7},... | collective-permute-start | bytes 393224 | tf_op jit(solution)/shard_map/ppermute | solution.py:342
  62.0 31.3 %collective-permute-start.7 = (bf16[512,128]{1,0:T(8,128)(2,1)S(1)}, bf16[512,128]{1,0:T(8,128)(2,1)S(1)}, u32[]{:S(2)}, u32[]{:S(2)}) collective-permute-start(bf16[512,128]{1,0:T(8,128)(2,1)S(1)} %copy-done.5), channel_id=1, source_target_pairs={{0,15},{1,14},{2,13},{3,12},{4,11},{5,10},{6,9},{7,8},{8,7},{9,6},... | collective-permute-start | bytes 393224 | tf_op jit(solution)/shard_map/ppermute | solution.py:342
  65.1 21.6 %collective-permute-start.10 = (f32[8,8,128]{2,1,0:T(8,128)S(1)}, f32[8,8,128]{2,1,0:T(8,128)S(1)}, u32[]{:S(2)}, u32[]{:S(2)}) collective-permute-start(f32[8,8,128]{2,1,0:T(8,128)S(1)} %select_select_fusion.2), channel_id=1, source_target_pairs={{0,4},{1,5},{2,6},{3,7},{4,0},{5,1},{6,2},{7,3},{8,12},{9,13},{10,... | collective-permute-start | bytes 98312 | tf_op jit(solution)/shard_map/ppermute | solution.py:342
  68.2 21.2 %collective-permute-start.11 = (f32[8,8,128]{2,1,0:T(8,128)S(1)}, f32[8,8,128]{2,1,0:T(8,128)S(1)}, u32[]{:S(2)}, u32[]{:S(2)}) collective-permute-start(f32[8,8,128]{2,1,0:T(8,128)S(1)} %select_select_fusion.2), channel_id=1, source_target_pairs={{0,8},{1,9},{2,10},{3,11},{4,12},{5,13},{6,14},{7,15},{8,0},{9,1},... | collective-permute-start | bytes 98312 | tf_op jit(solution)/shard_map/ppermute | solution.py:342
  79.9 9.6 %collective-permute-start.12 = (f32[8,8,128]{2,1,0:T(8,128)S(1)}, f32[8,8,128]{2,1,0:T(8,128)S(1)}, u32[]{:S(2)}, u32[]{:S(2)}) collective-permute-start(f32[8,8,128]{2,1,0:T(8,128)S(1)} %select_select_fusion.2), channel_id=1, source_target_pairs={{0,12},{1,13},{2,14},{3,15},{4,8},{5,9},{6,10},{7,11},{8,4},{9,5},... | collective-permute-start | bytes 98312 | tf_op jit(solution)/shard_map/ppermute | solution.py:342
  90.2 1.3 %collective-permute-start.13 = (f32[8,8,128]{2,1,0:T(8,128)S(1)}, f32[8,8,128]{2,1,0:T(8,128)S(1)}, u32[]{:S(2)}, u32[]{:S(2)}) collective-permute-start(f32[8,8,128]{2,1,0:T(8,128)S(1)} %broadcast_divide_fusion), channel_id=1, source_target_pairs={{0,1},{1,0},{2,3},{3,2},{4,5},{5,4},{6,7},{7,6},{8,9},{9,8},{10,11... | collective-permute-start | bytes 98312 | tf_op jit(solution)/shard_map/ppermute | solution.py:342
